TPU v7x, 256 devices: a whole 4x4x8 slice. The times are simulated.
256 devices in a mesh: fs: 32 (over z, x), tp: 8 (over y, core).
Axes of the slice: x: 4, y: 4, z: 8, core: 2. Of those that a mesh axis runs over, the one named last changes fastest.
Arguments:
- later_rows: bfloat16 [32768, 2048], P(('fs', 'tp')), may hold values from -6 to 6
- earlier_rows: bfloat16 [32768, 2048], P(('fs', 'tp')), may hold values from -6 to 6
- cotangent: bfloat16 [32768, 2048], P(('fs', 'tp')), may hold values from -24 to 24
- up_weight: bfloat16 [2048, 4096], P('fs', 'tp'), may hold values from -0.125 to 0.125
- down_weight: bfloat16 [2048, 4096], P('fs', 'tp'), may hold values from -0.09375 to 0.09375
- up_total: float32 [2048, 4096], P('fs', 'tp'), may hold values from -6 to 6
- down_total: float32 [2048, 4096], P('fs', 'tp'), may hold values from -6 to 6
Outputs:
- later_out: bfloat16 [32768, 2048], P(('fs', 'tp'))
- earlier_grad: bfloat16 [32768, 2048], P(('fs', 'tp'))
- up_updated: float32 [2048, 4096], P('fs', 'tp')
- down_updated: float32 [2048, 4096], P('fs', 'tp')
All inputs are finite; a program needn't handle non-finite values.
Results may differ from a plain program's by a relative error of at most 0.015.
Values may be sent and summed in bfloat16 or wider, within the bound.
No kernel may reach another device: no remote copies, remote signals or barrier semaphores. Data moves between devices by JAX's collectives and lax.ppermute only.
A program may use at most 128 MiB of HBM per device.

v0:
```python
import math

import jax
import jax.numpy as jnp
from jax import lax
from jax.sharding import Mesh
from jax.sharding import PartitionSpec as P

FS = ("fs_0", "fs_1")
FS_TP = ("fs_0", "fs_1", "tp")


def side_by_side(arrays, axis, dim, along):
    ends, at = ([], 0)
    for a in arrays[:-1]:
        at += a.shape[along]
        ends.append(at)
    both = jnp.concatenate(arrays, axis=along)
    return tuple(jnp.split(lax.all_gather(both, axis, axis=dim, tiled=True), ends, axis=along))


def in_blocks(x, dim, length):
    before, after = (x.shape[:dim], x.shape[dim + 1 :])
    return jnp.moveaxis(x.reshape(*before, length, -1, *after), dim, 0)


def sum_at_owner(x, axis, dim):
    length = lax.axis_size(axis)
    tiles = lax.all_to_all(in_blocks(x, dim, length), axis, 0, 0, tiled=True)
    return jnp.sum(tiles.astype(jnp.float32), axis=0)


def sum_by_axis(terms, axes):
    subtotal = terms.astype(jnp.bfloat16)
    for axis in axes:
        subtotal = lax.psum_scatter(subtotal, axis, scatter_dimension=0, tiled=True)
    return subtotal.astype(jnp.float32)


def contract_last(left, right):
    return lax.dot_general(
        left, right, (((1,), (1,)), ((), ())), preferred_element_type=jnp.float32
    )


def body(later_rows, earlier_rows, cotangent, up_weight, down_weight, up_total, down_total):
    rows_dev = later_rows.shape[0]
    total_rows = rows_dev * lax.axis_size(FS) * lax.axis_size("tp")
    factor = 1.0 / math.sqrt(total_rows)
    up_full, down_full = side_by_side((up_weight, down_weight), FS, 0, 1)

    def fetch():
        return (up_full, down_full)

    def to_owner(term):
        return sum_at_owner(term.astype(jnp.bfloat16), "tp", 0)

    def grad_owner(group, right):
        return sum_by_axis(
            lax.dot_general(
                group, right, (((0,), (0,)), ((), ())), preferred_element_type=jnp.float32
            ),
            FS,
        )

    up_whole, down_whole = fetch()
    group = lax.all_gather(later_rows, "tp", axis=0, tiled=True)
    relu_part = jnp.maximum(jnp.dot(group, up_whole, preferred_element_type=jnp.float32), 0.0)
    hidden = (relu_part * relu_part).astype(jnp.bfloat16)
    partial_value = contract_last(hidden, down_whole)
    later_out = to_owner(partial_value).astype(jnp.bfloat16)
    up_whole, down_whole = fetch()
    saved_group, cot_group = side_by_side((earlier_rows, cotangent), "tp", 0, 1)
    relu_part = jnp.maximum(jnp.dot(saved_group, up_whole, preferred_element_type=jnp.float32), 0.0)
    hidden = (relu_part * relu_part).astype(jnp.bfloat16)
    hidden_grad = jnp.dot(cot_group, down_whole, preferred_element_type=jnp.float32)
    pre_grad = (2.0 * relu_part * hidden_grad).astype(jnp.bfloat16)
    input_partial = contract_last(pre_grad, up_whole)
    earlier_grad = to_owner(input_partial).astype(jnp.bfloat16)
    down_updated = down_total + grad_owner(cot_group, hidden) * factor
    up_updated = up_total + grad_owner(saved_group, pre_grad) * factor
    earlier_grad, up_updated, down_updated = (earlier_grad, up_updated, down_updated)
    return (later_out, earlier_grad, up_updated, down_updated)


def solution(mesh):
    finer = Mesh(mesh.devices.reshape(8, 4, mesh.shape["tp"]), ("fs_0", "fs_1", "tp"))
    placed = (
        P(FS_TP, None),
        P(FS_TP, None),
        P(FS_TP, None),
        P(FS, "tp"),
        P(FS, "tp"),
        P(FS, "tp"),
        P(FS, "tp"),
    )
    return jax.shard_map(
        body,
        mesh=finer,
        in_specs=placed,
        out_specs=(P(FS_TP, None), P(FS_TP, None), P(FS, "tp"), P(FS, "tp")),
        check_vma=False,
    )
```

profile of v0, /device:TPU:8, one launch (start us, length us, event | category | flops | bytes accessed | tf_op | source)
XLA Modules:
  0.0 330.6 jit_solution(11753121503092980763)
XLA Ops:
  7.2 1.5 pad_maximum_fusion.1
  8.8 0.0 all-gather.8.cloned.1.call-start
  8.8 2.3 pad_maximum_fusion
  11.2 0.7 all-gather.6.cloned.1.call-update
  11.9 83.9 %all-gather.4.cloned.1.call-done = bf16[2048,1024]{1,0:T(8,128)(2,1)} async-done(((bf16[64,1024]{1,0:T(8,128)(2,1)}), bf16[2048,1024]{1,0:T(8,128)(2,1)}) %all-gather.4.cloned.1.call-update) | async-done | bytes 4194320 | tf_op jit(solution)/shard_map/all_gather | solution.py:19
  95.8 50.1 %all-gather.8.cloned.1.call-done = bf16[1024,4096]{1,0:T(8,128)(2,1)} async-done(((bf16[128,4096]{1,0:T(8,128)(2,1)}), bf16[1024,4096]{1,0:T(8,128)(2,1)}) %all-gather.8.cloned.1.call-update) | async-done | bytes 8388624 | tf_op jit(solution)/shard_map/all_gather | solution.py:19
  145.9 5.3 %fusion.6 = f32[1024,512]{1,0:T(8,128)S(1)} fusion(bf16[1024,4096]{1,0:T(8,128)(2,1)} %all-gather.8.cloned.1.call-done, bf16[2048,1024]{1,0:T(8,128)(2,1)} %all-gather.4.cloned.1.call-done), kind=kOutput, calls=%fused_computation.8 | convolution fusion | flops 2147483648 | bytes 8388608 | tf_op jit(solution)/shard_map/dot_general | solution.py:74
  151.2 3.7 %fusion.11 = bf16[2048,512]{1,0:T(8,128)(2,1)} fusion(bf16[1024,4096]{1,0:T(8,128)(2,1)S(1)} %copy-done.2, f32[1024,512]{1,0:T(8,128)S(1)} %fusion.6), kind=kOutput, calls=%fused_computation.11 | convolution fusion | flops 2150105088 | bytes 8388608 | tf_op jit(solution)/shard_map/dot_general | solution.py:60
  155.0 27.4 %all-gather.6.cloned.1.call-done = bf16[1024,2048]{1,0:T(8,128)(2,1)} async-done(((bf16[128,2048]{1,0:T(8,128)(2,1)}), bf16[1024,2048]{1,0:T(8,128)(2,1)}) %all-gather.6.cloned.1.call-update) | async-done | bytes 4194320 | tf_op jit(solution)/shard_map/all_gather | solution.py:67
  182.4 10.0 %convolution_convert_fusion.1 = bf16[1024,2048]{1,0:T(8,128)(2,1)} fusion(bf16[2048,1024]{1,0:T(8,128)(2,1)} %all-gather.4.cloned.1.call-done, bf16[1024,2048]{1,0:T(8,128)(2,1)} %all-gather.6.cloned.1.call-done), kind=kOutput, calls=%fused_computation.1 | convolution fusion | flops 4298637312 | bytes 12582912 | tf_op jit(solution)/shard_map/dot_general | solution.py:41
  192.4 6.0 %all-to-all-start = ((bf16[8,128,2048]{2,1,0:T(8,128)(2,1)}), bf16[8,128,2048]{2,1,0:T(8,128)(2,1)}, u32[]{:S(2)}, u32[]{:S(2)}) async-start(bf16[8,128,2048]{2,1,0:T(8,128)(2,1)} %bitcast.6), calls=%async_computation | async-start | bytes 8388608 | tf_op jit(solution)/shard_map/all_to_all | solution.py:29
  198.4 5.2 %multiply_convert_fusion.1 = bf16[1024,512]{1,0:T(8,128)(2,1)S(1)} fusion(f32[1024,512]{1,0:T(8,128)S(1)} %fusion.6, bf16[2048,1024]{1,0:T(8,128)(2,1)} %all-gather.4.cloned.1.call-done, bf16[1024,4096]{1,0:T(8,128)(2,1)} %all-gather.8.cloned.1.call-done), kind=kOutput, calls=%fused_computation.13 | convolution fusion | flops 2149580800 | bytes 9437184 | tf_op jit(solution)/shard_map/dot_general | solution.py:76
  203.6 6.0 %fusion.8 = bf16[2048,512]{1,0:T(8,128)(2,1)} fusion(bf16[1024,512]{1,0:T(8,128)(2,1)S(1)} %multiply_convert_fusion.1, bf16[1024,4096]{1,0:T(8,128)(2,1)} %all-gather.8.cloned.1.call-done), kind=kOutput, calls=%fused_computation.10 | convolution fusion | flops 2148532224 | bytes 7340032 | tf_op jit(solution)/shard_map/dot_general | solution.py:60
  209.6 5.9 %convolution_convert_fusion = bf16[1024,2048]{1,0:T(8,128)(2,1)} fusion(bf16[1024,512]{1,0:T(8,128)(2,1)S(1)} %multiply_convert_fusion.1, bf16[2048,1024]{1,0:T(8,128)(2,1)} %all-gather.4.cloned.1.call-done), kind=kOutput, calls=%fused_computation | convolution fusion | flops 2149580800 | bytes 7340032 | tf_op jit(solution)/shard_map/dot_general | solution.py:41
  215.5 31.2 %all-to-all-done = bf16[8,128,2048]{2,1,0:T(8,128)(2,1)} async-done(((bf16[8,128,2048]{2,1,0:T(8,128)(2,1)}), bf16[8,128,2048]{2,1,0:T(8,128)(2,1)}, u32[]{:S(2)}, u32[]{:S(2)}) %all-to-all-start) | async-done | bytes 4194336 | tf_op jit(solution)/shard_map/all_to_all | solution.py:29
  246.7 5.9 %all-to-all-start.1 = ((bf16[8,128,2048]{2,1,0:T(8,128)(2,1)}), bf16[8,128,2048]{2,1,0:T(8,128)(2,1)}, u32[]{:S(2)}, u32[]{:S(2)}) async-start(bf16[8,128,2048]{2,1,0:T(8,128)(2,1)} %bitcast.5), calls=%async_computation.1 | async-start | bytes 8388608 | tf_op jit(solution)/shard_map/all_to_all | solution.py:29
  252.6 0.6 reduce-scatter.11.cloned.1.call-update
  253.2 18.8 %reduce-scatter.5.cloned.1.call-done = bf16[256,512]{1,0:T(8,128)(2,1)} async-done(((bf16[2048,512]{1,0:T(8,128)(2,1)}), bf16[256,512]{1,0:T(8,128)(2,1)}) %reduce-scatter.5.cloned.1.call-update) | async-done | bytes 262160 | tf_op jit(solution)/shard_map/reduce_scatter | solution.py:36
  272.0 3.9 %reduce_sum.24 = bf16[128,2048]{1,0:T(8,128)(2,1)} reduce(bf16[8,128,2048]{2,1,0:T(8,128)(2,1)} %all-to-all-done, bf16[]{:T(256)} %constant.3.clone.1), dimensions={0}, to_apply=%region_0.0 | reduce | flops 1835008 | bytes 4718594 | tf_op jit(solution)/shard_map/reduce_sum | solution.py:30
  275.9 25.0 %all-to-all-done.1 = bf16[8,128,2048]{2,1,0:T(8,128)(2,1)} async-done(((bf16[8,128,2048]{2,1,0:T(8,128)(2,1)}), bf16[8,128,2048]{2,1,0:T(8,128)(2,1)}, u32[]{:S(2)}, u32[]{:S(2)}) %all-to-all-start.1) | async-done | bytes 4194336 | tf_op jit(solution)/shard_map/all_to_all | solution.py:29
  300.9 3.8 %reduce_sum.25 = bf16[128,2048]{1,0:T(8,128)(2,1)} reduce(bf16[8,128,2048]{2,1,0:T(8,128)(2,1)} %all-to-all-done.1, bf16[]{:T(256)} %constant.3.clone.1), dimensions={0}, to_apply=%region_1.0 | reduce | flops 1835008 | bytes 4718594 | tf_op jit(solution)/shard_map/reduce_sum | solution.py:30
  304.8 1.5 multiply_add_fusion
  306.3 16.0 %reduce-scatter.7.cloned.1.call-done = bf16[64,512]{1,0:T(8,128)(2,1)} async-done(((bf16[256,512]{1,0:T(8,128)(2,1)}), bf16[64,512]{1,0:T(8,128)(2,1)}) %reduce-scatter.7.cloned.1.call-update) | async-done | bytes 65552 | tf_op jit(solution)/shard_map/reduce_scatter | solution.py:36
  322.3 1.5 multiply_add_fusion.1
  (19 shorter events, 0.3 us)
Async XLA Ops:
  7.2 88.6 %all-gather.4.cloned.1.call-start = ((), (), s32[]{:S(2)}) async-start(), calls=%async_computation.6 | async-start | bytes 4325376 | tf_op jit(solution)/shard_map/all_gather | solution.py:19
  8.8 137.1 %all-gather.8.cloned.1.call-start = ((), (), s32[]{:S(2)}) async-start(), calls=%async_computation.8 | async-start | bytes 9437184 | tf_op jit(solution)/shard_map/all_gather | solution.py:19
  11.1 171.2 %all-gather.6.cloned.1.call-start = ((), (), s32[]{:S(2)}) async-start(), calls=%async_computation.7 | async-start | bytes 4718592 | tf_op jit(solution)/shard_map/all_gather | solution.py:67
  11.9 240.7 %reduce-scatter.9.cloned.1.call-start = ((), (), s32[]{:S(2)}) async-start(), calls=%async_computation.11 | async-start | bytes 2359296 | tf_op jit(solution)/shard_map/reduce_scatter | solution.py:36
  145.9 5.3 %copy-start.2 = (bf16[1024,4096]{1,0:T(8,128)(2,1)S(1)}, bf16[1024,4096]{1,0:T(8,128)(2,1)}, u32[]{:S(2)}) copy-start(bf16[1024,4096]{1,0:T(8,128)(2,1)} %all-gather.8.cloned.1.call-done) | copy-start | bytes 25165828
  192.4 54.3 %all-to-all-start = ((bf16[8,128,2048]{2,1,0:T(8,128)(2,1)}), bf16[8,128,2048]{2,1,0:T(8,128)(2,1)}, u32[]{:S(2)}, u32[]{:S(2)}) async-start(bf16[8,128,2048]{2,1,0:T(8,128)(2,1)} %bitcast.6), calls=%async_computation | async-start | bytes 8388608 | tf_op jit(solution)/shard_map/all_to_all | solution.py:29
  198.4 73.6 %reduce-scatter.5.cloned.1.call-start = ((), (), s32[]{:S(2)}) async-start(), calls=%async_computation.9 | async-start | bytes 2359296 | tf_op jit(solution)/shard_map/reduce_scatter | solution.py:36
  246.7 54.2 %all-to-all-start.1 = ((bf16[8,128,2048]{2,1,0:T(8,128)(2,1)}), bf16[8,128,2048]{2,1,0:T(8,128)(2,1)}, u32[]{:S(2)}, u32[]{:S(2)}) async-start(bf16[8,128,2048]{2,1,0:T(8,128)(2,1)} %bitcast.5), calls=%async_computation.1 | async-start | bytes 8388608 | tf_op jit(solution)/shard_map/all_to_all | solution.py:29
  252.6 52.2 %reduce-scatter.11.cloned.1.call-start = ((), (), s32[]{:S(2)}) async-start(), calls=%async_computation.12 | async-start | bytes 327680 | tf_op jit(solution)/shard_map/reduce_scatter | solution.py:36
  253.2 69.1 %reduce-scatter.7.cloned.1.call-start = ((), (), s32[]{:S(2)}) async-start(), calls=%async_computation.10 | async-start | bytes 327680 | tf_op jit(solution)/shard_map/reduce_scatter | solution.py:36
  272.0 32.8 %copy-start = (f32[64,512]{1,0:T(8,128)S(1)}, f32[64,512]{1,0:T(8,128)}, u32[]{:S(2)}) copy-start(f32[64,512]{1,0:T(8,128)} %param.13) | copy-start | bytes 393220
  272.0 50.3 %copy-start.1 = (f32[64,512]{1,0:T(8,128)S(1)}, f32[64,512]{1,0:T(8,128)}, u32[]{:S(2)}) copy-start(f32[64,512]{1,0:T(8,128)} %param.12) | copy-start | bytes 393220
Sparse Core Ops, SparseCore 0:
  11.1 84.6 all-gather.3
  97.6 48.1 all-gather.7
  147.8 34.5 all-gather.5
  184.8 43.4 reduce-scatter.8
  230.7 41.2 reduce-scatter.4
  274.3 22.1 reduce-scatter.10
  299.1 23.1 reduce-scatter.6
where the time goes:
time: 331 us
  waiting for transfers between devices  254 us (77%)
  matrix products  36.1 us (11%)
  other arithmetic  14.6 us (4%)
  between operations  14.2 us (4%)
  starting transfers between devices  12.1 us (4%)
    all_gather x2, waiting for transfers between devices, side_by_side(): lax.all_gather(both, axis, axis=dim, tiled=True)  134 us
    all_to_all x2, waiting for transfers between devices, sum_at_owner(): tiles = lax.all_to_all(in_blocks(x, dim, length), axis, 0, 0, tiled=True)  56.2 us
    reduce_scatter x4, waiting for transfers between devices, sum_by_axis(): subtotal = lax.psum_scatter(subtotal, axis, scatter_dimension=0, tiled=True)  34.8 us
    all_gather x1, waiting for transfers between devices, body(): group = lax.all_gather(later_rows, 'tp', axis=0, tiled=True)  27.4 us
    dot_general x2, matrix products, contract_last(): lax.dot_general(left, right, (((1,), (1,)), ((), ())), preferred_element_...  15.9 us
    all_to_all x2, starting transfers between devices, sum_at_owner(): tiles = lax.all_to_all(in_blocks(x, dim, length), axis, 0, 0, tiled=True)  11.9 us
    dot_general x2, matrix products, grad_owner(): lax.dot_general(group, right, (((0,), (0,)), ((), ())), preferred_element...  9.68 us
    reduce_sum x2, other arithmetic, sum_at_owner(): return jnp.sum(tiles.astype(jnp.float32), axis=0)  7.73 us
  transfers between devices with their start and end apart: 9, of which 7 were waited for; matrix products, arithmetic and copies ran while one was open for 14% of the time, Pallas kernels for 0%

commit v1 on v0

v1 whole, which is shorter than its diff:
```python
import math

import jax
import jax.numpy as jnp
from jax import lax
from jax.sharding import Mesh
from jax.sharding import PartitionSpec as P

FS = ("z", "x")
ALL = ("z", "x", "y", "c")
F32 = jnp.float32
BF16 = jnp.bfloat16


def shift(x, axis, by):
    n = lax.axis_size(axis)
    return lax.ppermute(x, axis, [(i, (i + by) % n) for i in range(n)])


def gather_tokens(x):
    half = x.shape[0] // 2
    behind, ahead = shift(x, "y", 1), shift(x, "y", -1)
    far_lo, far_hi = shift(behind[:half], "y", 1), shift(ahead[half:], "y", -1)
    mine = jnp.concatenate([x, behind, ahead, far_lo, far_hi], axis=0)
    return jnp.concatenate([mine, shift(mine, "c", 1)], axis=0)


def plus(a, b):
    return (a.astype(F32) + b.astype(F32)).astype(BF16)


def scatter_tokens(partial):
    mine, partners = jnp.split(partial, 2, axis=0)
    mine = plus(mine, shift(partners, "c", 1))
    rows = mine.shape[0] // 4
    half = rows // 2
    own, behind, ahead, far = (mine[i * rows : (i + 1) * rows] for i in range(4))
    from_behind = shift(far[:half], "y", 1)
    from_ahead = shift(far[half:], "y", -1)
    ahead = jnp.concatenate([plus(ahead[:half], from_behind), ahead[half:]], axis=0)
    behind = jnp.concatenate([behind[:half], plus(behind[half:], from_ahead)], axis=0)
    a, b = shift(ahead, "y", 1), shift(behind, "y", -1)
    return (own.astype(F32) + a.astype(F32) + b.astype(F32)).astype(BF16)


def exchange_sum(term, axis, dim):
    tiles = lax.all_to_all(term, axis, dim, dim, tiled=True)
    return jnp.sum(tiles.astype(F32), axis=dim)


def rows_times(left, right):
    return lax.dot_general(left, right, (((1,), (1,)), ((), ())), preferred_element_type=F32)


def over_tokens(left, right):
    return lax.dot_general(left, right, (((0,), (0,)), ((), ())), preferred_element_type=F32)


def body(later_rows, earlier_rows, cotangent, up_weight, down_weight, up_total, down_total):
    n_dev = math.prod(lax.axis_size(a) for a in ALL)
    factor = 1.0 / math.sqrt(later_rows.shape[0] * n_dev)
    up = lax.all_gather(up_weight, FS, axis=0, tiled=True)
    down = lax.all_gather(down_weight, FS, axis=0, tiled=True)
    saved = gather_tokens(earlier_rows)
    cot = gather_tokens(cotangent)
    later = gather_tokens(later_rows)

    relu = jnp.maximum(jnp.dot(saved, up, preferred_element_type=F32), 0.0)
    hidden = (relu * relu).astype(BF16)
    down_term = over_tokens(cot, hidden).astype(BF16)
    down_term = lax.psum_scatter(down_term, "z", scatter_dimension=0, tiled=True)
    down_term = lax.psum_scatter(down_term, "x", scatter_dimension=0, tiled=True)
    later_relu = jnp.maximum(jnp.dot(later, up, preferred_element_type=F32), 0.0)
    later_hidden = (later_relu * later_relu).astype(BF16)

    hidden_grad = jnp.dot(cot, down, preferred_element_type=F32)
    pre_grad = (2.0 * relu * hidden_grad).astype(BF16)
    up_term = over_tokens(saved, pre_grad).astype(BF16)
    nz, nx = lax.axis_size("z"), lax.axis_size("x")
    up_term = up_term.reshape(nz, nx, up_weight.shape[0], up_weight.shape[1])
    up_term = exchange_sum(up_term, "x", 1).astype(BF16)
    up_term = exchange_sum(up_term, "z", 0)

    later_out = scatter_tokens(rows_times(later_hidden, down).astype(BF16))
    earlier_grad = scatter_tokens(rows_times(pre_grad, up).astype(BF16))
    up_updated = up_total + up_term * factor
    down_updated = down_total + down_term.astype(F32) * factor
    return later_out, earlier_grad, up_updated, down_updated


def solution(mesh):
    n_tp = mesh.shape["tp"]
    finer = Mesh(mesh.devices.reshape(8, 4, n_tp // 2, 2), ALL)
    rows, weight = P(ALL, None), P(FS, ("y", "c"))
    return jax.shard_map(
        body,
        mesh=finer,
        in_specs=(rows, rows, rows, weight, weight, weight, weight),
        out_specs=(rows, rows, weight, weight),
        check_vma=False,
    )
```

time: 331 us -> 292 us (0.88)
  waiting for transfers between devices: 254 us -> 168 us
  local copies, waits for them, and re-layouts: 0.02 us -> 24.6 us
  starting transfers between devices: 12.1 us -> 35.4 us
    all_gather x3 -> x2, waiting for transfers between devices: 161 us -> 93.7 us  [the longest x1 71.2 us: body(): down = lax.all_gather(down_weight, FS, axis=0, tiled=True)]
    all_to_all x2, waiting for transfers between devices: 56.2 us -> 6.74 us  [exchange_sum(): tiles = lax.all_to_all(term, axis, dim, dim, tiled=True)]
    ppermute x0 -> x25, waiting for transfers between devices: none -> 32.3 us  [shift(): return lax.ppermute(x, axis, [(i, (i + by) % n) for i in range(n)])]
    ppermute x0 -> x25, starting transfers between devices: none -> 27.3 us  [shift(): return lax.ppermute(x, axis, [(i, (i + by) % n) for i in range(n)])]
    unnamed x6 -> x34, local copies, waits for them, and re-layouts: 0.02 us -> 13.1 us
    convert_element_type x0 -> x6, other arithmetic: none -> 10.6 us  [the longest x4 5.9 us: plus(): return (a.astype(F32) + b.astype(F32)).astype(BF16)]
    reduce_sum x2, other arithmetic: 7.73 us -> 1.33 us  [exchange_sum(): return jnp.sum(tiles.astype(F32), axis=dim)]
    split x0 -> x2, local copies, waits for them, and re-layouts: none -> 4.85 us  [scatter_tokens(): mine, partners = jnp.split(partial, 2, axis=0)]
  transfers between devices with their start and end apart: 9 -> 31, of which waited for: 7 -> 18; matrix products, arithmetic and copies ran while one was open for 14% -> 20% of each run, Pallas kernels for 0% -> 0%
where the time goes in v1:
time: 292 us; the launch traced here: 291 us
  waiting for transfers between devices  168 us (58%)
  starting transfers between devices  35.4 us (12%)
  matrix products  32.9 us (11%)
  local copies, waits for them, and re-layouts  24.6 us (8%)
  other arithmetic  16.7 us (6%)
  between operations  14.1 us (5%)
    all_gather x1, waiting for transfers between devices, body(): down = lax.all_gather(down_weight, FS, axis=0, tiled=True)  71.2 us
    ppermute x25, waiting for transfers between devices, shift(): return lax.ppermute(x, axis, [(i, (i + by) % n) for i in range(n)])  32.3 us
    ppermute x25, starting transfers between devices, shift(): return lax.ppermute(x, axis, [(i, (i + by) % n) for i in range(n)])  27.3 us
    all_gather x1, waiting for transfers between devices, body(): up = lax.all_gather(up_weight, FS, axis=0, tiled=True)  22.4 us
    reduce_scatter x1, waiting for transfers between devices, body(): lax.psum_scatter(down_term, 'x', scatter_dimension=0, tiled=True)  19.5 us
    reduce_scatter x1, waiting for transfers between devices, body(): lax.psum_scatter(down_term, 'z', scatter_dimension=0, tiled=True)  14.7 us
    unnamed x34, local copies, waits for them, and re-layouts  13.1 us
    dot_general x2, matrix products, rows_times(): lax.dot_general(left, right, (((1,), (1,)), ((), ())), preferred_element_...  12.3 us
  transfers between devices with their start and end apart: 31, of which 18 were waited for; matrix products, arithmetic and copies ran while one was open for 20% of the time, Pallas kernels for 0%

profile of v1, /device:TPU:8, one launch (start us, length us, event | category | flops | bytes accessed | tf_op | source)
XLA Modules:
  0.0 291.5 jit_solution(11379320285208974257)
XLA Ops:
  17.7 5.5 %collective-permute-done.10 = bf16[128,2048]{1,0:T(8,128)(2,1)S(1)} collective-permute-done((bf16[128,2048]{1,0:T(8,128)(2,1)}, bf16[128,2048]{1,0:T(8,128)(2,1)S(1)}, u32[]{:S(2)}, u32[]{:S(2)}) %collective-permute-start.10) | collective-permute-done | bytes 524320 | tf_op jit(solution)/shard_map/ppermute | solution.py:17
  23.2 3.2 %collective-permute-start.1 = (bf16[128,2048]{1,0:T(8,128)(2,1)S(1)}, bf16[128,2048]{1,0:T(8,128)(2,1)S(1)}, u32[]{:S(2)}, u32[]{:S(2)}) collective-permute-start(bf16[128,2048]{1,0:T(8,128)(2,1)S(1)} %copy-done.4), channel_id=1, source_target_pairs={{0,6},{2,0},{4,2},{6,4},{1,7},{3,1},{5,3},{7,5},{8,14},{10,8},{12,... | collective-permute-start | bytes 1572872 | tf_op jit(solution)/shard_map/ppermute | solution.py:17
  26.7 7.7 %collective-permute-done.15 = bf16[128,2048]{1,0:T(8,128)(2,1)S(1)} collective-permute-done((bf16[128,2048]{1,0:T(8,128)(2,1)}, bf16[128,2048]{1,0:T(8,128)(2,1)S(1)}, u32[]{:S(2)}, u32[]{:S(2)}) %collective-permute-start.15) | collective-permute-done | bytes 524320 | tf_op jit(solution)/shard_map/ppermute | solution.py:17
  34.4 3.2 %collective-permute-start.13 = (bf16[64,2048]{1,0:T(8,128)(2,1)S(1)}, bf16[64,2048]{1,0:T(8,128)(2,1)S(1)}, u32[]{:S(2)}, u32[]{:S(2)}) collective-permute-start(bf16[64,2048]{1,0:T(8,128)(2,1)S(1)} %slice.108), channel_id=1, source_target_pairs={{0,6},{2,0},{4,2},{6,4},{1,7},{3,1},{5,3},{7,5},{8,14},{10,8},{12,... | collective-permute-start | bytes 786440 | tf_op jit(solution)/shard_map/ppermute | solution.py:17
  39.6 6.1 %collective-permute-done = bf16[128,2048]{1,0:T(8,128)(2,1)S(1)} collective-permute-done((bf16[128,2048]{1,0:T(8,128)(2,1)}, bf16[128,2048]{1,0:T(8,128)(2,1)S(1)}, u32[]{:S(2)}, u32[]{:S(2)}) %collective-permute-start) | collective-permute-done | bytes 524320 | tf_op jit(solution)/shard_map/ppermute | solution.py:17
  45.6 3.2 %collective-permute-start.18 = (bf16[64,2048]{1,0:T(8,128)(2,1)S(1)}, bf16[64,2048]{1,0:T(8,128)(2,1)S(1)}, u32[]{:S(2)}, u32[]{:S(2)}) collective-permute-start(bf16[64,2048]{1,0:T(8,128)(2,1)S(1)} %slice.110), channel_id=1, source_target_pairs={{0,6},{2,0},{4,2},{6,4},{1,7},{3,1},{5,3},{7,5},{8,14},{10,8},{12,... | collective-permute-start | bytes 786440 | tf_op jit(solution)/shard_map/ppermute | solution.py:17
  51.3 3.2 %collective-permute-start.3 = (bf16[64,2048]{1,0:T(8,128)(2,1)S(1)}, bf16[64,2048]{1,0:T(8,128)(2,1)S(1)}, u32[]{:S(2)}, u32[]{:S(2)}) collective-permute-start(bf16[64,2048]{1,0:T(8,128)(2,1)S(1)} %slice.99), channel_id=1, source_target_pairs={{0,6},{2,0},{4,2},{6,4},{1,7},{3,1},{5,3},{7,5},{8,14},{10,8},{12,... | collective-permute-start | bytes 786440 | tf_op jit(solution)/shard_map/ppermute | solution.py:17
  69.0 22.4 %all-gather.3.cloned.1.call-done = bf16[2048,512]{1,0:T(8,128)(2,1)} async-done(((bf16[64,512]{1,0:T(8,128)(2,1)}), bf16[2048,512]{1,0:T(8,128)(2,1)}) %all-gather.3.cloned.1.call-update) | async-done | bytes 2097168 | tf_op jit(solution)/shard_map/all_gather | solution.py:62
  91.4 6.5 %fusion.5 = f32[1024,512]{1,0:T(8,128)} fusion(bf16[1024,2048]{1,0:T(8,128)(2,1)} %copy-done.7, bf16[2048,512]{1,0:T(8,128)(2,1)} %all-gather.3.cloned.1.call-done), kind=kOutput, calls=%fused_computation.60 | convolution fusion | flops 2147483648 | bytes 8388608 | tf_op jit(solution)/shard_map/dot_general | solution.py:68
  97.9 71.2 %all-gather.5.cloned.1.call-done = bf16[2048,512]{1,0:T(8,128)(2,1)} async-done(((bf16[64,512]{1,0:T(8,128)(2,1)}), bf16[2048,512]{1,0:T(8,128)(2,1)}) %all-gather.5.cloned.1.call-update) | async-done | bytes 2097168 | tf_op jit(solution)/shard_map/all_gather | solution.py:63
  169.1 5.8 %multiply_convert_fusion.1 = bf16[1024,512]{1,0:T(8,128)(2,1)S(1)} fusion(f32[1024,512]{1,0:T(8,128)} %fusion.5, bf16[1024,2048]{1,0:T(8,128)(2,1)} %constant_dynamic-update-slice_fusion.27, bf16[2048,512]{1,0:T(8,128)(2,1)} %all-gather.5.cloned.1.call-done), kind=kOutput, calls=%fused_computation.7 | convolution fusion | flops 2149580800 | bytes 9437184 | tf_op jit(solution)/shard_map/dot_general | solution.py:76
  174.9 2.4 convolution_convert_fusion
  181.7 2.4 convolution_convert_fusion.3
  185.8 3.6 %all-to-all-start = ((bf16[8,4,64,512]{3,2,0,1:T(8,128)(2,1)}), bf16[8,4,64,512]{3,2,0,1:T(8,128)(2,1)S(1)}, u32[]{:S(2)}, u32[]{:S(2)}) async-start(bf16[8,4,64,512]{3,2,0,1:T(8,128)(2,1)} %copy.12), calls=%async_computation | async-start | bytes 4194304 | tf_op jit(solution)/shard_map/all_to_all | solution.py:47
  189.5 9.9 %convolution_convert_fusion.1 = bf16[1024,2048]{1,0:T(8,128)(2,1)} fusion(bf16[2048,512]{1,0:T(8,128)(2,1)} %all-gather.5.cloned.1.call-done, bf16[1024,2048]{1,0:T(8,128)(2,1)} %constant_dynamic-update-slice_fusion.5, bf16[2048,512]{1,0:T(8,128)(2,1)} %all-gather.3.cloned.1.call-done), kind=kOutput, calls=%fused_computation.3 | convolution fusion | flops 4298637312 | bytes 12582912 | tf_op jit(solution)/shard_map/dot_general | solution.py:52
  199.4 3.3 %split.17 = bf16[512,2048]{1,0:T(8,128)(2,1)} slice(bf16[1024,2048]{1,0:T(8,128)(2,1)} %convolution_convert_fusion.1), slice={[512:1024], [0:2048]} | slice | bytes 4194304 | tf_op jit(solution)/shard_map/split | solution.py:33
  202.8 5.9 %convolution_convert_fusion.2 = bf16[2048,512]{1,0:T(8,128)(2,1)} fusion(bf16[1024,2048]{1,0:T(8,128)(2,1)} %constant_dynamic-update-slice_fusion.27, f32[1024,512]{1,0:T(8,128)S(1)} %copy-done.10), kind=kOutput, calls=%fused_computation.4 | convolution fusion | flops 2150105088 | bytes 8388608 | tf_op jit(solution)/shard_map/dot_general | solution.py:56
  208.7 6.7 %all-to-all-done = bf16[8,4,64,512]{3,2,0,1:T(8,128)(2,1)S(1)} async-done(((bf16[8,4,64,512]{3,2,0,1:T(8,128)(2,1)}), bf16[8,4,64,512]{3,2,0,1:T(8,128)(2,1)S(1)}, u32[]{:S(2)}, u32[]{:S(2)}) %all-to-all-start) | async-done | bytes 2097184 | tf_op jit(solution)/shard_map/all_to_all | solution.py:47
  216.7 4.3 %all-to-all-start.1 = ((bf16[8,64,512]{2,1,0:T(8,128)(2,1)}), bf16[8,64,512]{2,1,0:T(8,128)(2,1)S(1)}, u32[]{:S(2)}, u32[]{:S(2)}) async-start(bf16[8,64,512]{2,1,0:T(8,128)(2,1)} %reduce_sum.21), calls=%async_computation.1 | async-start | bytes 1048576 | tf_op jit(solution)/shard_map/all_to_all | solution.py:47
  221.1 3.3 %add_convert_fusion = bf16[512,2048]{1,0:T(8,128)(2,1)S(1)} fusion(bf16[512,2048]{1,0:T(8,128)(2,1)} %collective-permute-done.20, bf16[1024,2048]{1,0:T(8,128)(2,1)} %copy-done.2), kind=kLoop, calls=%fused_computation | loop fusion | flops 4194304 | bytes 6291456 | tf_op jit(solution)/shard_map/convert_element_type | solution.py:29
  226.5 2.4 add_convert_fusion.1
  244.5 14.7 %reduce-scatter.3.cloned.1.call-done = bf16[256,512]{1,0:T(8,128)(2,1)} async-done(((bf16[2048,512]{1,0:T(8,128)(2,1)}), bf16[256,512]{1,0:T(8,128)(2,1)}) %reduce-scatter.3.cloned.1.call-update) | async-done | bytes 262160 | tf_op jit(solution)/shard_map/reduce_scatter | solution.py:71
  261.5 2.4 add_convert_fusion.3
  263.9 19.5 %reduce-scatter.5.cloned.1.call-done = bf16[64,512]{1,0:T(8,128)(2,1)} async-done(((bf16[256,512]{1,0:T(8,128)(2,1)}), bf16[64,512]{1,0:T(8,128)(2,1)}) %reduce-scatter.5.cloned.1.call-update) | async-done | bytes 65552 | tf_op jit(solution)/shard_map/reduce_scatter | solution.py:72
  (113 shorter events, 58.3 us)
Async XLA Ops:
  7.2 84.2 %all-gather.3.cloned.1.call-start = ((), (), s32[]{:S(2)}) async-start(), calls=%async_computation.4 | async-start | bytes 2162688 | tf_op jit(solution)/shard_map/all_gather | solution.py:62
  7.9 161.2 %all-gather.5.cloned.1.call-start = ((), (), s32[]{:S(2)}) async-start(), calls=%async_computation.5 | async-start | bytes 2162688 | tf_op jit(solution)/shard_map/all_gather | solution.py:63
  8.0 15.2 %collective-permute-start.10 = (bf16[128,2048]{1,0:T(8,128)(2,1)}, bf16[128,2048]{1,0:T(8,128)(2,1)S(1)}, u32[]{:S(2)}, u32[]{:S(2)}) collective-permute-start(bf16[128,2048]{1,0:T(8,128)(2,1)} %param.8), channel_id=1, source_target_pairs={{0,2},{2,4},{4,6},{6,0},{1,3},{3,5},{5,7},{7,1},{8,10},{10,12},{12... | collective-permute-start | bytes 1572872 | tf_op jit(solution)/shard_map/ppermute | solution.py:17
  9.6 16.9 %collective-permute-start.11 = (bf16[128,2048]{1,0:T(8,128)(2,1)}, bf16[128,2048]{1,0:T(8,128)(2,1)S(1)}, u32[]{:S(2)}, u32[]{:S(2)}) collective-permute-start(bf16[128,2048]{1,0:T(8,128)(2,1)} %param.8), channel_id=1, source_target_pairs={{0,6},{2,0},{4,2},{6,4},{1,7},{3,1},{5,3},{7,5},{8,14},{10,8},{12,... | collective-permute-start | bytes 1572872 | tf_op jit(solution)/shard_map/ppermute | solution.py:17
  10.3 24.1 %collective-permute-start.15 = (bf16[128,2048]{1,0:T(8,128)(2,1)}, bf16[128,2048]{1,0:T(8,128)(2,1)S(1)}, u32[]{:S(2)}, u32[]{:S(2)}) collective-permute-start(bf16[128,2048]{1,0:T(8,128)(2,1)} %param.9), channel_id=1, source_target_pairs={{0,2},{2,4},{4,6},{6,0},{1,3},{3,5},{5,7},{7,1},{8,10},{10,12},{12... | collective-permute-start | bytes 1572872 | tf_op jit(solution)/shard_map/ppermute | solution.py:17
  11.6 26.9 %collective-permute-start.16 = (bf16[128,2048]{1,0:T(8,128)(2,1)}, bf16[128,2048]{1,0:T(8,128)(2,1)S(1)}, u32[]{:S(2)}, u32[]{:S(2)}) collective-permute-start(bf16[128,2048]{1,0:T(8,128)(2,1)} %param.9), channel_id=1, source_target_pairs={{0,6},{2,0},{4,2},{6,4},{1,7},{3,1},{5,3},{7,5},{8,14},{10,8},{12,... | collective-permute-start | bytes 1572872 | tf_op jit(solution)/shard_map/ppermute | solution.py:17
  13.4 32.2 %collective-permute-start = (bf16[128,2048]{1,0:T(8,128)(2,1)}, bf16[128,2048]{1,0:T(8,128)(2,1)S(1)}, u32[]{:S(2)}, u32[]{:S(2)}) collective-permute-start(bf16[128,2048]{1,0:T(8,128)(2,1)} %param.7), channel_id=1, source_target_pairs={{0,2},{2,4},{4,6},{6,0},{1,3},{3,5},{5,7},{7,1},{8,10},{10,12},{12... | collective-permute-start | bytes 1572872 | tf_op jit(solution)/shard_map/ppermute | solution.py:17
  23.2 26.6 %collective-permute-start.1 = (bf16[128,2048]{1,0:T(8,128)(2,1)S(1)}, bf16[128,2048]{1,0:T(8,128)(2,1)S(1)}, u32[]{:S(2)}, u32[]{:S(2)}) collective-permute-start(bf16[128,2048]{1,0:T(8,128)(2,1)S(1)} %copy-done.4), channel_id=1, source_target_pairs={{0,6},{2,0},{4,2},{6,4},{1,7},{3,1},{5,3},{7,5},{8,14},{10,8},{12,... | collective-permute-start | bytes 1572872 | tf_op jit(solution)/shard_map/ppermute | solution.py:17
  26.5 24.7 %collective-permute-start.12 = (bf16[64,2048]{1,0:T(8,128)(2,1)S(1)}, bf16[64,2048]{1,0:T(8,128)(2,1)S(1)}, u32[]{:S(2)}, u32[]{:S(2)}) collective-permute-start(bf16[64,2048]{1,0:T(8,128)(2,1)S(1)} %slice.107), channel_id=1, source_target_pairs={{0,2},{2,4},{4,6},{6,0},{1,3},{3,5},{5,7},{7,1},{8,10},{10,12},{12... | collective-permute-start | bytes 786440 | tf_op jit(solution)/shard_map/ppermute | solution.py:17
  34.4 20.1 %collective-permute-start.13 = (bf16[64,2048]{1,0:T(8,128)(2,1)S(1)}, bf16[64,2048]{1,0:T(8,128)(2,1)S(1)}, u32[]{:S(2)}, u32[]{:S(2)}) collective-permute-start(bf16[64,2048]{1,0:T(8,128)(2,1)S(1)} %slice.108), channel_id=1, source_target_pairs={{0,6},{2,0},{4,2},{6,4},{1,7},{3,1},{5,3},{7,5},{8,14},{10,8},{12,... | collective-permute-start | bytes 786440 | tf_op jit(solution)/shard_map/ppermute | solution.py:17
  38.6 18.3 %collective-permute-start.17 = (bf16[64,2048]{1,0:T(8,128)(2,1)S(1)}, bf16[64,2048]{1,0:T(8,128)(2,1)S(1)}, u32[]{:S(2)}, u32[]{:S(2)}) collective-permute-start(bf16[64,2048]{1,0:T(8,128)(2,1)S(1)} %slice.109), channel_id=1, source_target_pairs={{0,2},{2,4},{4,6},{6,0},{1,3},{3,5},{5,7},{7,1},{8,10},{10,12},{12... | collective-permute-start | bytes 786440 | tf_op jit(solution)/shard_map/ppermute | solution.py:17
  45.6 12.7 %collective-permute-start.18 = (bf16[64,2048]{1,0:T(8,128)(2,1)S(1)}, bf16[64,2048]{1,0:T(8,128)(2,1)S(1)}, u32[]{:S(2)}, u32[]{:S(2)}) collective-permute-start(bf16[64,2048]{1,0:T(8,128)(2,1)S(1)} %slice.110), channel_id=1, source_target_pairs={{0,6},{2,0},{4,2},{6,4},{1,7},{3,1},{5,3},{7,5},{8,14},{10,8},{12,... | collective-permute-start | bytes 786440 | tf_op jit(solution)/shard_map/ppermute | solution.py:17
  49.8 11.4 %collective-permute-start.2 = (bf16[64,2048]{1,0:T(8,128)(2,1)S(1)}, bf16[64,2048]{1,0:T(8,128)(2,1)S(1)}, u32[]{:S(2)}, u32[]{:S(2)}) collective-permute-start(bf16[64,2048]{1,0:T(8,128)(2,1)S(1)} %slice.98), channel_id=1, source_target_pairs={{0,2},{2,4},{4,6},{6,0},{1,3},{3,5},{5,7},{7,1},{8,10},{10,12},{12... | collective-permute-start | bytes 786440 | tf_op jit(solution)/shard_map/ppermute | solution.py:17
  51.3 11.3 %collective-permute-start.3 = (bf16[64,2048]{1,0:T(8,128)(2,1)S(1)}, bf16[64,2048]{1,0:T(8,128)(2,1)S(1)}, u32[]{:S(2)}, u32[]{:S(2)}) collective-permute-start(bf16[64,2048]{1,0:T(8,128)(2,1)S(1)} %slice.99), channel_id=1, source_target_pairs={{0,6},{2,0},{4,2},{6,4},{1,7},{3,1},{5,3},{7,5},{8,14},{10,8},{12,... | collective-permute-start | bytes 786440 | tf_op jit(solution)/shard_map/ppermute | solution.py:17
  180.5 40.6 %collective-permute-start.20 = (bf16[512,2048]{1,0:T(8,128)(2,1)}, bf16[512,2048]{1,0:T(8,128)(2,1)}, u32[]{:S(2)}, u32[]{:S(2)}) collective-permute-start(bf16[512,2048]{1,0:T(8,128)(2,1)} %split.19), channel_id=1, source_target_pairs={{0,1},{1,0},{2,3},{3,2},{4,5},{5,4},{6,7},{7,6},{8,9},{9,8},{10,11... | collective-permute-start | bytes 6291464 | tf_op jit(solution)/shard_map/ppermute | solution.py:17
  185.8 29.6 %all-to-all-start = ((bf16[8,4,64,512]{3,2,0,1:T(8,128)(2,1)}), bf16[8,4,64,512]{3,2,0,1:T(8,128)(2,1)S(1)}, u32[]{:S(2)}, u32[]{:S(2)}) async-start(bf16[8,4,64,512]{3,2,0,1:T(8,128)(2,1)} %copy.12), calls=%async_computation | async-start | bytes 4194304 | tf_op jit(solution)/shard_map/all_to_all | solution.py:47
  189.4 69.8 %reduce-scatter.3.cloned.1.call-start = ((), (), s32[]{:S(2)}) async-start(), calls=%async_computation.6 | async-start | bytes 2359296 | tf_op jit(solution)/shard_map/reduce_scatter | solution.py:71
  202.8 23.8 %collective-permute-start.5 = (bf16[512,2048]{1,0:T(8,128)(2,1)}, bf16[512,2048]{1,0:T(8,128)(2,1)}, u32[]{:S(2)}, u32[]{:S(2)}) collective-permute-start(bf16[512,2048]{1,0:T(8,128)(2,1)} %split.17), channel_id=1, source_target_pairs={{0,1},{1,0},{2,3},{3,2},{4,5},{5,4},{6,7},{7,6},{8,9},{9,8},{10,11... | collective-permute-start | bytes 6291464 | tf_op jit(solution)/shard_map/ppermute | solution.py:17
  216.7 27.1 %all-to-all-start.1 = ((bf16[8,64,512]{2,1,0:T(8,128)(2,1)}), bf16[8,64,512]{2,1,0:T(8,128)(2,1)S(1)}, u32[]{:S(2)}, u32[]{:S(2)}) async-start(bf16[8,64,512]{2,1,0:T(8,128)(2,1)} %reduce_sum.21), calls=%async_computation.1 | async-start | bytes 1048576 | tf_op jit(solution)/shard_map/all_to_all | solution.py:47
  221.0 62.4 %reduce-scatter.5.cloned.1.call-start = ((), (), s32[]{:S(2)}) async-start(), calls=%async_computation.7 | async-start | bytes 327680 | tf_op jit(solution)/shard_map/reduce_scatter | solution.py:72
  234.4 24.8 %collective-permute-start.22 = (bf16[128,2048]{1,0:T(8,128)(2,1)S(1)}, bf16[128,2048]{1,0:T(8,128)(2,1)}, u32[]{:S(2)}, u32[]{:S(2)}) collective-permute-start(bf16[128,2048]{1,0:T(8,128)(2,1)S(1)} %pad_maximum_fusion.2), channel_id=1, source_target_pairs={{0,2},{2,4},{4,6},{6,0},{1,3},{3,5},{5,7},{7,1},{8,10},{10,12},{12... | collective-permute-start | bytes 1572872 | tf_op jit(solution)/shard_map/ppermute | solution.py:17
  236.5 22.7 %collective-permute-start.24 = (bf16[128,2048]{1,0:T(8,128)(2,1)}, bf16[128,2048]{1,0:T(8,128)(2,1)}, u32[]{:S(2)}, u32[]{:S(2)}) collective-permute-start(bf16[128,2048]{1,0:T(8,128)(2,1)} %pad_maximum_fusion.3), channel_id=1, source_target_pairs={{0,6},{2,0},{4,2},{6,4},{1,7},{3,1},{5,3},{7,5},{8,14},{10,8},{12,... | collective-permute-start | bytes 1572872 | tf_op jit(solution)/shard_map/ppermute | solution.py:17
  240.8 20.7 %collective-permute-start.7 = (bf16[128,2048]{1,0:T(8,128)(2,1)}, bf16[128,2048]{1,0:T(8,128)(2,1)}, u32[]{:S(2)}, u32[]{:S(2)}) collective-permute-start(bf16[128,2048]{1,0:T(8,128)(2,1)} %pad_maximum_fusion), channel_id=1, source_target_pairs={{0,2},{2,4},{4,6},{6,0},{1,3},{3,5},{5,7},{7,1},{8,10},{10,12},{12... | collective-permute-start | bytes 1572872 | tf_op jit(solution)/shard_map/ppermute | solution.py:17
  242.8 18.7 %collective-permute-start.9 = (bf16[128,2048]{1,0:T(8,128)(2,1)}, bf16[128,2048]{1,0:T(8,128)(2,1)}, u32[]{:S(2)}, u32[]{:S(2)}) collective-permute-start(bf16[128,2048]{1,0:T(8,128)(2,1)} %pad_maximum_fusion.1), channel_id=1, source_target_pairs={{0,6},{2,0},{4,2},{6,4},{1,7},{3,1},{5,3},{7,5},{8,14},{10,8},{12,... | collective-permute-start | bytes 1572872 | tf_op jit(solution)/shard_map/ppermute | solution.py:17
  (18 other events, 209.6 us)
Sparse Core Ops, SparseCore 0:
  10.6 80.7 all-gather.2
  94.0 75.1 all-gather.4
  208.8 50.3 reduce-scatter.2
  261.5 21.8 reduce-scatter.4

commit v2 on v1

v2 whole, which is shorter than its diff:
```python
import math

import jax
import jax.numpy as jnp
from jax import lax
from jax.sharding import Mesh
from jax.sharding import PartitionSpec as P


FS = ("z", "x")
ALL = ("z", "x", "y", "c")
F32 = jnp.float32
BF16 = jnp.bfloat16


def shift(x, axis, by):
    n = lax.axis_size(axis)
    return lax.ppermute(x, axis, [(i, (i + by) % n) for i in range(n)])


def place(buffer, piece, slot, row):
    return lax.dynamic_update_slice(buffer, piece[:, None], (0, slot, row, 0))


def gather_tokens(arrays):
    own = jnp.stack(arrays)
    half = own.shape[1] // 2
    behind, ahead = shift(own, "y", 1), shift(own, "y", -1)
    far_lo, far_hi = shift(behind[:, :half], "y", 1), shift(ahead[:, half:], "y", -1)
    group = jnp.zeros((own.shape[0], 8, *own.shape[1:]), BF16)
    for piece, slot, row in (
        (own, 0, 0), (behind, 1, 0), (ahead, 2, 0), (far_lo, 3, 0), (far_hi, 3, half)
    ):
        partners = shift(piece, "c", 1)
        group = place(place(group, piece, slot, row), partners, slot + 4, row)
    return tuple(g.reshape(-1, g.shape[-1]) for g in group)


def plus(a, b):
    return (a.astype(F32) + b.astype(F32)).astype(BF16)


def scatter_tokens(partial):
    mine, partners = jnp.split(partial, 2, axis=0)
    partners = shift(partners, "c", 1)
    mine = plus(mine, partners)
    rows = mine.shape[0] // 4
    half = rows // 2
    own, behind, ahead, far = (mine[i * rows : (i + 1) * rows] for i in range(4))
    from_behind = shift(far[:half], "y", 1)
    from_ahead = shift(far[half:], "y", -1)
    ahead = jnp.concatenate([plus(ahead[:half], from_behind), ahead[half:]], axis=0)
    behind = jnp.concatenate([behind[:half], plus(behind[half:], from_ahead)], axis=0)
    a, b = shift(ahead, "y", 1), shift(behind, "y", -1)
    return (own.astype(F32) + a.astype(F32) + b.astype(F32)).astype(BF16)


def gather(x, axis):
    n = lax.axis_size(axis)
    return lax.all_to_all(jnp.broadcast_to(x[None], (n, *x.shape)), axis, 0, 0, tiled=True)


def exchange_sum(term, axis, dim):
    tiles = lax.all_to_all(term, axis, dim, dim, tiled=True)
    return jnp.sum(tiles.astype(F32), axis=dim)


def dot(left, right):
    return jnp.dot(left, right, preferred_element_type=F32)


def rows_times(left, right):
    return lax.dot_general(left, right, (((1,), (1,)), ((), ())), preferred_element_type=F32)


def over_tokens(left, right):
    return lax.dot_general(left, right, (((0,), (0,)), ((), ())), preferred_element_type=F32)


def body(later_rows, earlier_rows, cotangent, up_weight, down_weight, up_total, down_total):
    n_dev = math.prod(lax.axis_size(a) for a in ALL)
    nz, nx = lax.axis_size("z"), lax.axis_size("x")
    factor = 1.0 / math.sqrt(later_rows.shape[0] * n_dev)
    cols = up_weight.shape[1]
    up = gather(up_weight, "x").reshape(-1, cols)
    up = lax.all_gather(up, "z", axis=0, tiled=True)
    down = gather(down_weight, "z")
    down = gather(down, "x")
    down = jnp.swapaxes(down, 0, 1).reshape(-1, cols)
    saved, cot, later = gather_tokens((earlier_rows, cotangent, later_rows))

    relu = jnp.maximum(dot(saved, up), 0.0)
    hidden = (relu * relu).astype(BF16)
    down_term = over_tokens(cot, hidden).astype(BF16)
    down_term = lax.psum_scatter(down_term, "z", scatter_dimension=0, tiled=True)
    down_term = exchange_sum(down_term.reshape(-1, *down_weight.shape), "x", 0)
    hidden_grad = dot(cot, down)
    pre_grad = (2.0 * relu * hidden_grad).astype(BF16)
    up_term = over_tokens(saved, pre_grad).astype(BF16)
    up_term = up_term.reshape(nz, nx, *up_weight.shape)
    up_term = exchange_sum(up_term, "x", 1).astype(BF16)
    up_term = exchange_sum(up_term, "z", 0)
    later_relu = jnp.maximum(dot(later, up), 0.0)
    later_hidden = (later_relu * later_relu).astype(BF16)
    later_out = rows_times(later_hidden, down).astype(BF16)
    later_out = scatter_tokens(later_out)
    earlier_grad = rows_times(pre_grad, up).astype(BF16)
    earlier_grad = scatter_tokens(earlier_grad)
    up_updated = up_total + up_term * factor
    down_updated = down_total + down_term * factor
    return later_out, earlier_grad, up_updated, down_updated


def solution(mesh):
    n_tp = mesh.shape["tp"]
    finer = Mesh(mesh.devices.reshape(8, 4, n_tp // 2, 2), ALL)
    rows, weight = P(ALL, None), P(FS, ("y", "c"))
    return jax.shard_map(
        body,
        mesh=finer,
        in_specs=(rows, rows, rows, weight, weight, weight, weight),
        out_specs=(rows, rows, weight, weight),
        check_vma=False,
    )
```

time: 292 us -> 222 us (0.76)
  waiting for transfers between devices: 168 us -> 47.5 us
  local copies, waits for them, and re-layouts: 24.6 us -> 54.2 us
  blocking collectives: 0 us -> 24 us
  matrix products: 32.9 us -> 27.9 us
    all_gather x2 -> x1, waiting for transfers between devices: 93.7 us -> 0.01 us  [body(): up = lax.all_gather(up, 'z', axis=0, tiled=True)]
    dynamic_update_slice x0 -> x10, local copies, waits for them, and re-layouts: none -> 28.8 us  [place(): return lax.dynamic_update_slice(buffer, piece[:, None], (0, slot, row, 0))]
    all_to_all x0 -> x1, blocking collectives: none -> 24 us  [gather(): lax.all_to_all(jnp.broadcast_to(x[None], (n, *x.shape)), axis, 0, 0, tile...]
    reduce_scatter x1 -> x0, waiting for transfers between devices: 19.5 us -> none  [body(): lax.psum_scatter(down_term, 'x', scatter_dimension=0, tiled=True)]
    ppermute x25 -> x19, starting transfers between devices: 27.3 us -> 13.6 us  [shift(): return lax.ppermute(x, axis, [(i, (i + by) % n) for i in range(n)])]
    reduce_scatter x1, waiting for transfers between devices: 14.7 us -> 1.66 us  [body(): lax.psum_scatter(down_term, 'z', scatter_dimension=0, tiled=True)]
    unnamed x34 -> x28, local copies, waits for them, and re-layouts: 13.1 us -> 3.88 us
    another operation x0 -> x1, local copies, waits for them, and re-layouts: none -> 8.93 us  [gather_tokens(): return tuple((g.reshape(-1, g.shape[-1]) for g in group))]
  transfers between devices with their start and end apart: 31 -> 26, of which waited for: 18 -> 12; matrix products, arithmetic and copies ran while one was open for 20% -> 37% of each run, Pallas kernels for 0% -> 0%
where the time goes in v2:
time: 222 us; the launch traced here: 221 us
  local copies, waits for them, and re-layouts  54.2 us (24%)
  waiting for transfers between devices  47.5 us (21%)
  starting transfers between devices  34.2 us (15%)
  matrix products  27.9 us (13%)
  blocking collectives  24 us (11%)
  other arithmetic  19 us (9%)
  between operations  14.3 us (6%)
    dynamic_update_slice x10, local copies, waits for them, and re-layouts, place(): return lax.dynamic_update_slice(buffer, piece[:, None], (0, slot, row, 0))  28.8 us
    ppermute x19, waiting for transfers between devices, shift(): return lax.ppermute(x, axis, [(i, (i + by) % n) for i in range(n)])  27.1 us
    all_to_all x1, blocking collectives, gather(): lax.all_to_all(jnp.broadcast_to(x[None], (n, *x.shape)), axis, 0, 0, tile...  24 us
    ppermute x19, starting transfers between devices, shift(): return lax.ppermute(x, axis, [(i, (i + by) % n) for i in range(n)])  13.6 us
    all_to_all x3, starting transfers between devices, exchange_sum(): tiles = lax.all_to_all(term, axis, dim, dim, tiled=True)  12.6 us
    all_to_all x3, waiting for transfers between devices, exchange_sum(): tiles = lax.all_to_all(term, axis, dim, dim, tiled=True)  12.5 us
    dot_general x2, matrix products, rows_times(): lax.dot_general(left, right, (((1,), (1,)), ((), ())), preferred_element_...  12.3 us
    another operation x1, local copies, waits for them, and re-layouts, gather_tokens(): return tuple((g.reshape(-1, g.shape[-1]) for g in group))  8.93 us
  transfers between devices with their start and end apart: 26, of which 12 were waited for; matrix products, arithmetic and copies ran while one was open for 37% of the time, Pallas kernels for 0%

profile of v2, /device:TPU:8, one launch (start us, length us, event | category | flops | bytes accessed | tf_op | source)
XLA Modules:
  0.0 221.2 jit_solution(12706474844512983619)
XLA Ops:
  7.2 3.3 %pad_maximum_fusion = (bf16[3,128,2048]{2,1,0:T(8,128)(2,1)}, bf16[3,1,128,2048]{3,2,0,1:T(8,128)(2,1)}) fusion(bf16[1,128,2048]{2,1,0:T(8,128)(2,1)} %bitcast.53, bf16[1,128,2048]{2,1,0:T(8,128)(2,1)} %bitcast.54, bf16[1,128,2048]{2,1,0:T(8,128)(2,1)} %bitcast.55), kind=kLoop, calls=%fused_computation.9 | loop fusion | flops 1572864 | bytes 4718592 | tf_op jit(solution)/shard_map/stack | solution.py:26
  12.7 4.3 %all-to-all-start = ((bf16[4,64,512]{2,1,0:T(8,128)(2,1)}), bf16[4,64,512]{2,1,0:T(8,128)(2,1)S(1)}, u32[]{:S(2)}, u32[]{:S(2)}) async-start(bf16[4,64,512]{2,1,0:T(8,128)(2,1)} %broadcast_in_dim.59), calls=%async_computation | async-start | bytes 524288 | tf_op jit(solution)/shard_map/all_to_all | solution.py:60
  17.5 6.2 %all-to-all-done = bf16[4,64,512]{2,1,0:T(8,128)(2,1)S(1)} async-done(((bf16[4,64,512]{2,1,0:T(8,128)(2,1)}), bf16[4,64,512]{2,1,0:T(8,128)(2,1)S(1)}, u32[]{:S(2)}, u32[]{:S(2)}) %all-to-all-start) | async-done | bytes 262176 | tf_op jit(solution)/shard_map/all_to_all | solution.py:60
  23.8 24.0 %all_to_all.30 = bf16[8,64,512]{2,1,0:T(8,128)(2,1)S(1)} all-to-all(bf16[8,64,512]{2,1,0:T(8,128)(2,1)S(1)} %broadcast_in_dim.60), channel_id=1, replica_groups=mesh['z'=8,'x'=4,'y'=4,'c'=2] {'z'}, dimensions={0} | all-to-all | bytes 1048576 | tf_op jit(solution)/shard_map/all_to_all | solution.py:60
  49.4 3.6 %all-to-all-start.2 = ((bf16[4,8,64,512]{3,2,1,0:T(8,128)(2,1)}), bf16[4,8,64,512]{3,2,1,0:T(8,128)(2,1)S(1)}, u32[]{:S(2)}, u32[]{:S(2)}) async-start(bf16[4,8,64,512]{3,2,1,0:T(8,128)(2,1)} %broadcast_in_dim.61), calls=%async_computation.2 | async-start | bytes 4194304 | tf_op jit(solution)/shard_map/all_to_all | solution.py:60
  53.1 7.6 %dynamic_update_slice.30 = bf16[3,8,128,2048]{3,2,0,1:T(8,128)(2,1)} pad(bf16[3,1,128,2048]{3,2,0,1:T(8,128)(2,1)} %get-tuple-element.20, bf16[]{:T(256)} %constant.13.clone.1), padding=0_0x0_7x0_0x0_0 | pad | bytes 14155778 | tf_op jit(solution)/shard_map/dynamic_update_slice | solution.py:22
  65.3 2.8 %bitcast_dynamic-update-slice_fusion.4 = bf16[3,8,128,2048]{3,2,0,1:T(8,128)(2,1)} fusion(bf16[3,8,128,2048]{3,2,0,1:T(8,128)(2,1)} %dynamic_update_slice.30, bf16[3,128,2048]{2,1,0:T(8,128)(2,1)} %collective-permute-done), kind=kLoop, calls=%fused_computation.14 | loop fusion | bytes 3145728 | tf_op jit(solution)/shard_map/dynamic_update_slice | solution.py:22
  68.1 2.8 %bitcast_dynamic-update-slice_fusion.3 = bf16[3,8,128,2048]{3,2,0,1:T(8,128)(2,1)} fusion(bf16[3,8,128,2048]{3,2,0,1:T(8,128)(2,1)} %bitcast_dynamic-update-slice_fusion.4, bf16[3,128,2048]{2,1,0:T(8,128)(2,1)} %collective-permute-done.1), kind=kLoop, calls=%fused_computation.13 | loop fusion | bytes 3145728 | tf_op jit(solution)/shard_map/dynamic_update_slice | solution.py:22
  70.9 11.1 %collective-permute-done.5 = bf16[3,64,2048]{2,1,0:T(8,128)(2,1)} collective-permute-done((bf16[3,64,2048]{2,1,0:T(8,128)(2,1)S(1)}, bf16[3,64,2048]{2,1,0:T(8,128)(2,1)}, u32[]{:S(2)}, u32[]{:S(2)}) %collective-permute-start.5) | collective-permute-done | bytes 786464 | tf_op jit(solution)/shard_map/ppermute | solution.py:18
  85.8 2.8 %bitcast_dynamic-update-slice_fusion.2 = bf16[3,8,128,2048]{3,2,0,1:T(8,128)(2,1)} fusion(bf16[3,8,128,2048]{3,2,0,1:T(8,128)(2,1)} %bitcast_dynamic-update-slice_fusion.3, bf16[3,128,2048]{2,1,0:T(8,128)(2,1)} %collective-permute-done.2), kind=kLoop, calls=%fused_computation.12 | loop fusion | bytes 3145728 | tf_op jit(solution)/shard_map/dynamic_update_slice | solution.py:22
  88.6 2.7 %bitcast_dynamic-update-slice_fusion.1 = bf16[3,8,128,2048]{3,2,0,1:T(8,128)(2,1)} fusion(bf16[3,8,128,2048]{3,2,0,1:T(8,128)(2,1)} %bitcast_dynamic-update-slice_fusion.2, bf16[3,128,2048]{2,1,0:T(8,128)(2,1)} %collective-permute-done.3), kind=kLoop, calls=%fused_computation.11 | loop fusion | bytes 3145728 | tf_op jit(solution)/shard_map/dynamic_update_slice | solution.py:22
  91.3 2.7 %bitcast_dynamic-update-slice_fusion = bf16[3,8,128,2048]{3,2,0,1:T(8,128)(2,1)} fusion(bf16[3,8,128,2048]{3,2,0,1:T(8,128)(2,1)} %bitcast_dynamic-update-slice_fusion.1, bf16[3,128,2048]{2,1,0:T(8,128)(2,1)} %collective-permute-done.4), kind=kLoop, calls=%fused_computation.10 | loop fusion | bytes 3145728 | tf_op jit(solution)/shard_map/dynamic_update_slice | solution.py:22
  101.4 8.9 %fusion.4 = (bf16[1,8,128,2048]{3,2,0,1:T(8,128)(2,1)}, bf16[1,8,128,2048]{3,2,0,1:T(8,128)(2,1)}, bf16[1,8,128,2048]{3,2,0,1:T(8,128)(2,1)}) fusion(bf16[3,8,128,2048]{3,2,0,1:T(8,128)(2,1)} %bitcast_dynamic-update-slice_fusion.5), kind=kLoop, calls=%fused_computation.37 | loop fusion | bytes 25165824 | tf_op jit(solution)/shard_map/unstack | solution.py:36
  110.3 5.3 %fusion.7 = f32[1024,512]{1,0:T(8,128)S(1)} fusion(bf16[1024,2048]{1,0:T(8,128)(2,1)} %bitcast.47, bf16[2048,512]{1,0:T(8,128)(2,1)} %all-gather.2.cloned.1.call-done), kind=kOutput, calls=%fused_computation.40 | convolution fusion | flops 2147483648 | bytes 8388608 | tf_op jit(solution)/shard_map/dot_general | solution.py:69
  130.1 4.6 %all-to-all-start.3 = ((bf16[8,4,64,512]{3,2,0,1:T(8,128)(2,1)}), bf16[8,4,64,512]{3,2,0,1:T(8,128)(2,1)S(1)}, u32[]{:S(2)}, u32[]{:S(2)}) async-start(bf16[8,4,64,512]{3,2,0,1:T(8,128)(2,1)} %copy.14), calls=%async_computation.3 | async-start | bytes 4194304 | tf_op jit(solution)/shard_map/all_to_all | solution.py:64
  134.7 10.0 %convolution_convert_fusion.1 = bf16[1024,2048]{1,0:T(8,128)(2,1)} fusion(bf16[2048,512]{1,0:T(8,128)(2,1)} %bitcast.49, bf16[1024,2048]{1,0:T(8,128)(2,1)} %bitcast.46, bf16[2048,512]{1,0:T(8,128)(2,1)} %all-gather.2.cloned.1.call-done), kind=kOutput, calls=%fused_computation.3 | convolution fusion | flops 4298637312 | bytes 12582912 | tf_op jit(solution)/shard_map/dot_general | solution.py:73
  144.7 3.3 %split.17 = bf16[512,2048]{1,0:T(8,128)(2,1)} slice(bf16[1024,2048]{1,0:T(8,128)(2,1)} %convolution_convert_fusion.1), slice={[512:1024], [0:2048]} | slice | bytes 4194304 | tf_op jit(solution)/shard_map/split | solution.py:44
  148.2 5.4 %convolution_convert_fusion.2 = bf16[2048,512]{1,0:T(8,128)(2,1)} fusion(bf16[1024,2048]{1,0:T(8,128)(2,1)S(1)} %bitcast.45, f32[1024,512]{1,0:T(8,128)} %copy-done.13), kind=kOutput, calls=%fused_computation.4 | convolution fusion | flops 2150105088 | bytes 8388608 | tf_op jit(solution)/shard_map/dot_general | solution.py:77
  153.6 8.0 %all-to-all-done.3 = bf16[8,4,64,512]{3,2,0,1:T(8,128)(2,1)S(1)} async-done(((bf16[8,4,64,512]{3,2,0,1:T(8,128)(2,1)}), bf16[8,4,64,512]{3,2,0,1:T(8,128)(2,1)S(1)}, u32[]{:S(2)}, u32[]{:S(2)}) %all-to-all-start.3) | async-done | bytes 2097184 | tf_op jit(solution)/shard_map/all_to_all | solution.py:64
  163.0 3.5 %all-to-all-start.4 = ((bf16[8,64,512]{2,1,0:T(8,128)(2,1)}), bf16[8,64,512]{2,1,0:T(8,128)(2,1)S(1)}, u32[]{:S(2)}, u32[]{:S(2)}) async-start(bf16[8,64,512]{2,1,0:T(8,128)(2,1)} %reduce_sum.30), calls=%async_computation.4 | async-start | bytes 1048576 | tf_op jit(solution)/shard_map/all_to_all | solution.py:64
  166.5 3.2 %add_convert_fusion = bf16[512,2048]{1,0:T(8,128)(2,1)S(1)} fusion(bf16[512,2048]{1,0:T(8,128)(2,1)} %collective-permute-done.14, bf16[1024,2048]{1,0:T(8,128)(2,1)} %copy-done.2), kind=kLoop, calls=%fused_computation | loop fusion | flops 4194304 | bytes 6291456 | tf_op jit(solution)/shard_map/convert_element_type | solution.py:40
  190.3 5.4 %collective-permute-done.16 = bf16[128,2048]{1,0:T(8,128)(2,1)} collective-permute-done((bf16[128,2048]{1,0:T(8,128)(2,1)S(1)}, bf16[128,2048]{1,0:T(8,128)(2,1)}, u32[]{:S(2)}, u32[]{:S(2)}) %collective-permute-start.16) | collective-permute-done | bytes 524320 | tf_op jit(solution)/shard_map/ppermute | solution.py:18
  202.4 4.6 %all-to-all-start.5 = ((bf16[4,64,512]{2,1,0:T(8,128)(2,1)}), bf16[4,64,512]{2,1,0:T(8,128)(2,1)S(1)}, u32[]{:S(2)}, u32[]{:S(2)}) async-start(bf16[4,64,512]{2,1,0:T(8,128)(2,1)} %bitcast.56), calls=%async_computation.6 | async-start | bytes 524288 | tf_op jit(solution)/shard_map/all_to_all | solution.py:64
  209.2 4.4 %all-to-all-done.5 = bf16[4,64,512]{2,1,0:T(8,128)(2,1)S(1)} async-done(((bf16[4,64,512]{2,1,0:T(8,128)(2,1)}), bf16[4,64,512]{2,1,0:T(8,128)(2,1)S(1)}, u32[]{:S(2)}, u32[]{:S(2)}) %all-to-all-start.5) | async-done | bytes 262176 | tf_op jit(solution)/shard_map/all_to_all | solution.py:64
  (103 shorter events, 66.2 us)
Async XLA Ops:
  10.4 42.6 %collective-permute-start.1 = (bf16[3,128,2048]{2,1,0:T(8,128)(2,1)}, bf16[3,128,2048]{2,1,0:T(8,128)(2,1)}, u32[]{:S(2)}, u32[]{:S(2)}) collective-permute-start(bf16[3,128,2048]{2,1,0:T(8,128)(2,1)} %get-tuple-element.19), channel_id=1, source_target_pairs={{0,2},{2,4},{4,6},{6,0},{1,3},{3,5},{5,7},{7,1},{8,10},{10,12},{12... | collective-permute-start | bytes 4718600 | tf_op jit(solution)/shard_map/ppermute | solution.py:18
  12.7 11.0 %all-to-all-start = ((bf16[4,64,512]{2,1,0:T(8,128)(2,1)}), bf16[4,64,512]{2,1,0:T(8,128)(2,1)S(1)}, u32[]{:S(2)}, u32[]{:S(2)}) async-start(bf16[4,64,512]{2,1,0:T(8,128)(2,1)} %broadcast_in_dim.59), calls=%async_computation | async-start | bytes 524288 | tf_op jit(solution)/shard_map/all_to_all | solution.py:60
  17.0 46.3 %collective-permute-start.3 = (bf16[3,128,2048]{2,1,0:T(8,128)(2,1)}, bf16[3,128,2048]{2,1,0:T(8,128)(2,1)}, u32[]{:S(2)}, u32[]{:S(2)}) collective-permute-start(bf16[3,128,2048]{2,1,0:T(8,128)(2,1)} %get-tuple-element.19), channel_id=1, source_target_pairs={{0,6},{2,0},{4,2},{6,4},{1,7},{3,1},{5,3},{7,5},{8,14},{10,8},{12,... | collective-permute-start | bytes 4718600 | tf_op jit(solution)/shard_map/ppermute | solution.py:18
  17.5 47.8 %collective-permute-start = (bf16[3,128,2048]{2,1,0:T(8,128)(2,1)}, bf16[3,128,2048]{2,1,0:T(8,128)(2,1)}, u32[]{:S(2)}, u32[]{:S(2)}) collective-permute-start(bf16[3,128,2048]{2,1,0:T(8,128)(2,1)} %get-tuple-element.19), channel_id=1, source_target_pairs={{0,1},{1,0},{2,3},{3,2},{4,5},{5,4},{6,7},{7,6},{8,9},{9,8},{10,11... | collective-permute-start | bytes 4718600 | tf_op jit(solution)/shard_map/ppermute | solution.py:18
  49.4 34.9 %all-to-all-start.2 = ((bf16[4,8,64,512]{3,2,1,0:T(8,128)(2,1)}), bf16[4,8,64,512]{3,2,1,0:T(8,128)(2,1)S(1)}, u32[]{:S(2)}, u32[]{:S(2)}) async-start(bf16[4,8,64,512]{3,2,1,0:T(8,128)(2,1)} %broadcast_in_dim.61), calls=%async_computation.2 | async-start | bytes 4194304 | tf_op jit(solution)/shard_map/all_to_all | solution.py:60
  53.0 57.3 %all-gather.2.cloned.1.call-start = ((), (), s32[]{:S(2)}) async-start(), calls=%async_computation.7 | async-start | bytes 2359296 | tf_op jit(solution)/shard_map/all_gather | solution.py:86
  53.0 32.8 %collective-permute-start.2 = (bf16[3,128,2048]{2,1,0:T(8,128)(2,1)}, bf16[3,128,2048]{2,1,0:T(8,128)(2,1)}, u32[]{:S(2)}, u32[]{:S(2)}) collective-permute-start(bf16[3,128,2048]{2,1,0:T(8,128)(2,1)} %collective-permute-done.1), channel_id=1, source_target_pairs={{0,1},{1,0},{2,3},{3,2},{4,5},{5,4},{6,7},{7,6},{8,9},{9,8},{10,11... | collective-permute-start | bytes 4718600 | tf_op jit(solution)/shard_map/ppermute | solution.py:18
  61.9 20.1 %collective-permute-start.5 = (bf16[3,64,2048]{2,1,0:T(8,128)(2,1)S(1)}, bf16[3,64,2048]{2,1,0:T(8,128)(2,1)}, u32[]{:S(2)}, u32[]{:S(2)}) collective-permute-start(bf16[3,64,2048]{2,1,0:T(8,128)(2,1)S(1)} %slice.82), channel_id=1, source_target_pairs={{0,2},{2,4},{4,6},{6,0},{1,3},{3,5},{5,7},{7,1},{8,10},{10,12},{12... | collective-permute-start | bytes 2359304 | tf_op jit(solution)/shard_map/ppermute | solution.py:18
  64.5 19.7 %collective-permute-start.7 = (bf16[3,64,2048]{2,1,0:T(8,128)(2,1)S(1)}, bf16[3,64,2048]{2,1,0:T(8,128)(2,1)S(1)}, u32[]{:S(2)}, u32[]{:S(2)}) collective-permute-start(bf16[3,64,2048]{2,1,0:T(8,128)(2,1)S(1)} %slice.83), channel_id=1, source_target_pairs={{0,6},{2,0},{4,2},{6,4},{1,7},{3,1},{5,3},{7,5},{8,14},{10,8},{12,... | collective-permute-start | bytes 2359304 | tf_op jit(solution)/shard_map/ppermute | solution.py:18
  65.3 26.0 %collective-permute-start.4 = (bf16[3,128,2048]{2,1,0:T(8,128)(2,1)}, bf16[3,128,2048]{2,1,0:T(8,128)(2,1)}, u32[]{:S(2)}, u32[]{:S(2)}) collective-permute-start(bf16[3,128,2048]{2,1,0:T(8,128)(2,1)} %collective-permute-done.3), channel_id=1, source_target_pairs={{0,1},{1,0},{2,3},{3,2},{4,5},{5,4},{6,7},{7,6},{8,9},{9,8},{10,11... | collective-permute-start | bytes 4718600 | tf_op jit(solution)/shard_map/ppermute | solution.py:18
  82.1 14.1 %collective-permute-start.6 = (bf16[3,64,2048]{2,1,0:T(8,128)(2,1)}, bf16[3,64,2048]{2,1,0:T(8,128)(2,1)}, u32[]{:S(2)}, u32[]{:S(2)}) collective-permute-start(bf16[3,64,2048]{2,1,0:T(8,128)(2,1)} %collective-permute-done.5), channel_id=1, source_target_pairs={{0,1},{1,0},{2,3},{3,2},{4,5},{5,4},{6,7},{7,6},{8,9},{9,8},{10,11... | collective-permute-start | bytes 2359304 | tf_op jit(solution)/shard_map/ppermute | solution.py:18
  84.2 15.0 %collective-permute-start.8 = (bf16[3,64,2048]{2,1,0:T(8,128)(2,1)S(1)}, bf16[3,64,2048]{2,1,0:T(8,128)(2,1)}, u32[]{:S(2)}, u32[]{:S(2)}) collective-permute-start(bf16[3,64,2048]{2,1,0:T(8,128)(2,1)S(1)} %collective-permute-done.7), channel_id=1, source_target_pairs={{0,1},{1,0},{2,3},{3,2},{4,5},{5,4},{6,7},{7,6},{8,9},{9,8},{10,11... | collective-permute-start | bytes 2359304 | tf_op jit(solution)/shard_map/ppermute | solution.py:18
  124.9 41.6 %collective-permute-start.14 = (bf16[512,2048]{1,0:T(8,128)(2,1)}, bf16[512,2048]{1,0:T(8,128)(2,1)}, u32[]{:S(2)}, u32[]{:S(2)}) collective-permute-start(bf16[512,2048]{1,0:T(8,128)(2,1)} %split.19), channel_id=1, source_target_pairs={{0,1},{1,0},{2,3},{3,2},{4,5},{5,4},{6,7},{7,6},{8,9},{9,8},{10,11... | collective-permute-start | bytes 6291464 | tf_op jit(solution)/shard_map/ppermute | solution.py:18
  130.1 31.6 %all-to-all-start.3 = ((bf16[8,4,64,512]{3,2,0,1:T(8,128)(2,1)}), bf16[8,4,64,512]{3,2,0,1:T(8,128)(2,1)S(1)}, u32[]{:S(2)}, u32[]{:S(2)}) async-start(bf16[8,4,64,512]{3,2,0,1:T(8,128)(2,1)} %copy.14), calls=%async_computation.3 | async-start | bytes 4194304 | tf_op jit(solution)/shard_map/all_to_all | solution.py:64
  134.7 67.7 %reduce-scatter.2.cloned.1.call-start = ((), (), s32[]{:S(2)}) async-start(), calls=%async_computation.8 | async-start | bytes 2359296 | tf_op jit(solution)/shard_map/reduce_scatter | solution.py:95
  148.0 23.9 %collective-permute-start.9 = (bf16[512,2048]{1,0:T(8,128)(2,1)}, bf16[512,2048]{1,0:T(8,128)(2,1)}, u32[]{:S(2)}, u32[]{:S(2)}) collective-permute-start(bf16[512,2048]{1,0:T(8,128)(2,1)} %split.17), channel_id=1, source_target_pairs={{0,1},{1,0},{2,3},{3,2},{4,5},{5,4},{6,7},{7,6},{8,9},{9,8},{10,11... | collective-permute-start | bytes 6291464 | tf_op jit(solution)/shard_map/ppermute | solution.py:18
  163.0 26.6 %all-to-all-start.4 = ((bf16[8,64,512]{2,1,0:T(8,128)(2,1)}), bf16[8,64,512]{2,1,0:T(8,128)(2,1)S(1)}, u32[]{:S(2)}, u32[]{:S(2)}) async-start(bf16[8,64,512]{2,1,0:T(8,128)(2,1)} %reduce_sum.30), calls=%async_computation.4 | async-start | bytes 1048576 | tf_op jit(solution)/shard_map/all_to_all | solution.py:64
  174.4 10.0 %collective-permute-start.10 = (bf16[64,2048]{1,0:T(8,128)(2,1)S(1)}, bf16[64,2048]{1,0:T(8,128)(2,1)S(1)}, u32[]{:S(2)}, u32[]{:S(2)}) collective-permute-start(bf16[64,2048]{1,0:T(8,128)(2,1)S(1)} %get-tuple-element.15), channel_id=1, source_target_pairs={{0,2},{2,4},{4,6},{6,0},{1,3},{3,5},{5,7},{7,1},{8,10},{10,12},{12... | collective-permute-start | bytes 786440 | tf_op jit(solution)/shard_map/ppermute | solution.py:18
  175.5 10.2 %collective-permute-start.12 = (bf16[64,2048]{1,0:T(8,128)(2,1)S(1)}, bf16[64,2048]{1,0:T(8,128)(2,1)S(1)}, u32[]{:S(2)}, u32[]{:S(2)}) collective-permute-start(bf16[64,2048]{1,0:T(8,128)(2,1)S(1)} %get-tuple-element.16), channel_id=1, source_target_pairs={{0,6},{2,0},{4,2},{6,4},{1,7},{3,1},{5,3},{7,5},{8,14},{10,8},{12,... | collective-permute-start | bytes 786440 | tf_op jit(solution)/shard_map/ppermute | solution.py:18
  180.2 15.4 %collective-permute-start.16 = (bf16[128,2048]{1,0:T(8,128)(2,1)S(1)}, bf16[128,2048]{1,0:T(8,128)(2,1)}, u32[]{:S(2)}, u32[]{:S(2)}) collective-permute-start(bf16[128,2048]{1,0:T(8,128)(2,1)S(1)} %pad_maximum_fusion.3), channel_id=1, source_target_pairs={{0,2},{2,4},{4,6},{6,0},{1,3},{3,5},{5,7},{7,1},{8,10},{10,12},{12... | collective-permute-start | bytes 1572872 | tf_op jit(solution)/shard_map/ppermute | solution.py:18
  183.2 15.1 %collective-permute-start.18 = (bf16[128,2048]{1,0:T(8,128)(2,1)}, bf16[128,2048]{1,0:T(8,128)(2,1)}, u32[]{:S(2)}, u32[]{:S(2)}) collective-permute-start(bf16[128,2048]{1,0:T(8,128)(2,1)} %pad_maximum_fusion.4), channel_id=1, source_target_pairs={{0,6},{2,0},{4,2},{6,4},{1,7},{3,1},{5,3},{7,5},{8,14},{10,8},{12,... | collective-permute-start | bytes 1572872 | tf_op jit(solution)/shard_map/ppermute | solution.py:18
  186.7 20.3 %collective-permute-start.11 = (bf16[128,2048]{1,0:T(8,128)(2,1)}, bf16[128,2048]{1,0:T(8,128)(2,1)}, u32[]{:S(2)}, u32[]{:S(2)}) collective-permute-start(bf16[128,2048]{1,0:T(8,128)(2,1)} %pad_maximum_fusion.1), channel_id=1, source_target_pairs={{0,2},{2,4},{4,6},{6,0},{1,3},{3,5},{5,7},{7,1},{8,10},{10,12},{12... | collective-permute-start | bytes 1572872 | tf_op jit(solution)/shard_map/ppermute | solution.py:18
  189.3 17.7 %collective-permute-start.13 = (bf16[128,2048]{1,0:T(8,128)(2,1)}, bf16[128,2048]{1,0:T(8,128)(2,1)}, u32[]{:S(2)}, u32[]{:S(2)}) collective-permute-start(bf16[128,2048]{1,0:T(8,128)(2,1)} %pad_maximum_fusion.2), channel_id=1, source_target_pairs={{0,6},{2,0},{4,2},{6,4},{1,7},{3,1},{5,3},{7,5},{8,14},{10,8},{12,... | collective-permute-start | bytes 1572872 | tf_op jit(solution)/shard_map/ppermute | solution.py:18
  202.4 11.2 %all-to-all-start.5 = ((bf16[4,64,512]{2,1,0:T(8,128)(2,1)}), bf16[4,64,512]{2,1,0:T(8,128)(2,1)S(1)}, u32[]{:S(2)}, u32[]{:S(2)}) async-start(bf16[4,64,512]{2,1,0:T(8,128)(2,1)} %bitcast.56), calls=%async_computation.6 | async-start | bytes 524288 | tf_op jit(solution)/shard_map/all_to_all | solution.py:64
  (16 other events, 139.5 us)
Sparse Core Ops, SparseCore 0:
  60.9 37.6 all-gather.1
  153.8 48.5 reduce-scatter.1

commit v3 on v2

v3 whole, which is shorter than its diff:
```python
import math

import jax
import jax.numpy as jnp
from jax import lax
from jax.experimental import pallas as pl
from jax.experimental.pallas import tpu as pltpu
from jax.sharding import Mesh
from jax.sharding import PartitionSpec as P


FS = ("z", "x")
ALL = ("z", "x", "y", "c")
F32 = jnp.float32
BF16 = jnp.bfloat16
TILE = 512


def shift(x, axis, by):
    n = lax.axis_size(axis)
    return lax.ppermute(x, axis, [(i, (i + by) % n) for i in range(n)])


def gather_tokens(arrays):
    own = jnp.stack(arrays)
    half = own.shape[1] // 2
    behind, ahead = shift(own, "y", 1), shift(own, "y", -1)
    far_lo, far_hi = shift(behind[:, :half], "y", 1), shift(ahead[:, half:], "y", -1)
    pieces = (own, behind, ahead, far_lo, far_hi)
    partners = []
    for piece in pieces:
        partners.append(shift(piece, "c", 1))
    return (*pieces, *partners)


def plus(a, b):
    return (a.astype(F32) + b.astype(F32)).astype(BF16)


def scatter_tokens(mine, partners):
    partners = shift(partners, "c", 1)
    mine = plus(mine, partners)
    rows = mine.shape[0] // 4
    half = rows // 2
    own, behind, ahead, far = (mine[i * rows : (i + 1) * rows] for i in range(4))
    from_behind = shift(far[:half], "y", 1)
    from_ahead = shift(far[half:], "y", -1)
    ahead = jnp.concatenate([plus(ahead[:half], from_behind), ahead[half:]], axis=0)
    behind = jnp.concatenate([behind[:half], plus(behind[half:], from_ahead)], axis=0)
    a, b = shift(ahead, "y", 1), shift(behind, "y", -1)
    return (own.astype(F32) + a.astype(F32) + b.astype(F32)).astype(BF16)


def gather(x, axis):
    n = lax.axis_size(axis)
    return lax.all_to_all(jnp.broadcast_to(x[None], (n, *x.shape)), axis, 0, 0, tiled=True)


def exchange_sum(term, axis):
    tiles = lax.all_to_all(term, axis, 0, 0, tiled=True)
    return jnp.sum(tiles.astype(F32), axis=0)


def hop_sum(term, axis):
    n = lax.axis_size(axis)
    me = lax.axis_index(axis)

    def block(by):
        at = lax.rem(me + by, n)
        start = (at, *(0 for _ in term.shape[1:]))
        part = lax.dynamic_slice(term, start, (1, *term.shape[1:]), allow_negative_indices=False)
        return part[0]

    arrived = [shift(block(by), axis, by) for by in range(1, n)]
    return sum((a.astype(F32) for a in arrived), block(0).astype(F32))


def rows_times(left, right):
    return lax.dot_general(left, right, (((1,), (1,)), ((), ())), preferred_element_type=F32)


def over_tokens(left, right):
    return lax.dot_general(left, right, (((0,), (0,)), ((), ())), preferred_element_type=F32)


def copies(sources, target, sems, index):
    waits, row = [], 0
    for i, source in enumerate(sources):
        rows = source.shape[1]
        copy = pltpu.make_async_copy(source.at[index], target.at[pl.ds(row, rows)], sems.at[i])
        copy.start()
        waits.append((row, copy))
        row += rows
    return waits


def settle(waits, upto):
    while waits and waits[0][0] < upto:
        waits.pop(0)[1].wait()


def relu_times(rows, weight):
    return jnp.maximum(jnp.dot(rows, weight, preferred_element_type=F32), 0.0)


def back_kernel(*refs):
    pieces, (w, down_out, up_out, mine_out, theirs_out) = refs[:10], refs[10:15]
    saved, cot, up, down, relu, hid, pg, dt, ut, mine, theirs, in_sems, w_sems, out_sems = refs[15:]
    cols = up.shape[1]
    up_copy = pltpu.make_async_copy(w.at[:, pl.ds(0, cols)], up, w_sems.at[0])
    up_copy.start()
    saved_waits = copies(pieces, saved, in_sems.at[0], 0)
    down_copy = pltpu.make_async_copy(w.at[:, pl.ds(cols, cols)], down, w_sems.at[1])
    down_copy.start()
    cot_waits = copies(pieces, cot, in_sems.at[1], 1)
    up_copy.wait()
    for t in range(0, saved.shape[0], TILE):
        settle(saved_waits, t + TILE)
        at = pl.ds(t, TILE)
        r = relu_times(saved[at], up[...])
        relu[at] = r
        hid[at] = (r * r).astype(BF16)
    down_copy.wait()
    for t in range(0, saved.shape[0], TILE):
        settle(cot_waits, t + TILE)
        at = pl.ds(t, TILE)
        grad = jnp.dot(cot[at], down[...], preferred_element_type=F32)
        pg[at] = (2.0 * relu[at] * grad).astype(BF16)
    nx, nz, part = ut.shape[:3]

    @pl.loop(0, nz)
    def _(i):
        at = pl.ds(pl.multiple_of(i * nx * part, nx * part), nx * part)
        dt[at] = over_tokens(cot[:, at], hid[...]).astype(BF16)

    @pl.loop(0, nz)
    def _(i):
        at = pl.ds(pl.multiple_of(i * nx * part, nx * part), nx * part)
        term = over_tokens(saved[:, at], pg[...]).astype(BF16)
        for j in range(nx):
            ut[j, i] = term[j * part : (j + 1) * part]

    done = [
        pltpu.make_async_copy(a, b, out_sems.at[i])
        for i, (a, b) in enumerate(
            ((dt, down_out), (ut, up_out), (mine, mine_out), (theirs, theirs_out))
        )
    ]
    done[0].start()
    outputs(pg, 0, up, mine)
    done[1].start()
    outputs(pg, mine.shape[0], up, theirs)
    done[2].start()
    done[3].start()
    for copy in done:
        copy.wait()


def outputs(hidden, first, weight, out):
    @pl.loop(0, out.shape[0], step=TILE)
    def _(t):
        rows = hidden[pl.ds(pl.multiple_of(first + t, TILE), TILE)]
        for n in range(0, out.shape[1], 512):
            part = rows_times(rows, weight[n : n + 512])
            out[pl.ds(pl.multiple_of(t, TILE), TILE), n : n + 512] = part.astype(BF16)


def ahead_kernel(*refs):
    pieces, (w, mine_out, theirs_out) = refs[:10], refs[10:13]
    rows, up, down, hid, mine, theirs, in_sems, w_sems, out_sems = refs[13:]
    cols = up.shape[1]
    up_copy = pltpu.make_async_copy(w.at[:, pl.ds(0, cols)], up, w_sems.at[0])
    up_copy.start()
    waits = copies(pieces, rows, in_sems, 2)
    down_copy = pltpu.make_async_copy(w.at[:, pl.ds(cols, cols)], down, w_sems.at[1])
    down_copy.start()
    up_copy.wait()
    for t in range(0, rows.shape[0], TILE):
        settle(waits, t + TILE)
        at = pl.ds(t, TILE)
        r = relu_times(rows[at], up[...])
        hid[at] = (r * r).astype(BF16)
    down_copy.wait()
    first = pltpu.make_async_copy(mine, mine_out, out_sems.at[0])
    second = pltpu.make_async_copy(theirs, theirs_out, out_sems.at[1])
    outputs(hid, mine.shape[0], down, theirs)
    outputs(hid, 0, down, mine)
    second.start()
    first.start()
    first.wait()
    second.wait()


def call(kernel, pieces, weights, outs, scratch, dots):
    rows = sum(p.shape[1] for p in pieces)
    depth, cols = weights.shape[0], weights.shape[1] // 2
    hbm = pl.BlockSpec(memory_space=pltpu.HBM)
    return pl.pallas_call(
        kernel,
        out_shape=[jax.ShapeDtypeStruct(s, BF16) for s in outs],
        in_specs=[hbm] * (len(pieces) + 1),
        out_specs=[hbm] * len(outs),
        scratch_shapes=scratch,
        cost_estimate=pl.CostEstimate(
            flops=2 * dots * rows * depth * cols, bytes_accessed=20 << 20, transcendentals=0
        ),
        compiler_params=pltpu.CompilerParams(vmem_limit_bytes=60 * 1024 * 1024),
    )(*pieces, weights)


def back(pieces, weights, nz, nx):
    rows = sum(p.shape[1] for p in pieces)
    depth, cols = weights.shape[0], weights.shape[1] // 2
    n = len(pieces)
    up_shape = (nx, nz, depth // (nx * nz), cols)
    half = (rows // 2, depth)
    outs = ((depth, cols), up_shape, half, half)
    scratch = [
        pltpu.VMEM((rows, depth), BF16),
        pltpu.VMEM((rows, depth), BF16),
        pltpu.VMEM((depth, cols), BF16),
        pltpu.VMEM((depth, cols), BF16),
        pltpu.VMEM((rows, cols), F32),
        pltpu.VMEM((rows, cols), BF16),
        pltpu.VMEM((rows, cols), BF16),
        *(pltpu.VMEM(s, BF16) for s in outs),
        pltpu.SemaphoreType.DMA((2, n)),
        pltpu.SemaphoreType.DMA((2,)),
        pltpu.SemaphoreType.DMA((4,)),
    ]
    return call(back_kernel, pieces, weights, outs, scratch, 5)


def ahead_of(pieces, weights):
    rows = sum(p.shape[1] for p in pieces)
    depth, cols = weights.shape[0], weights.shape[1] // 2
    half = (rows // 2, depth)
    scratch = [
        pltpu.VMEM((rows, depth), BF16),
        pltpu.VMEM((depth, cols), BF16),
        pltpu.VMEM((depth, cols), BF16),
        pltpu.VMEM((rows, cols), BF16),
        pltpu.VMEM(half, BF16),
        pltpu.VMEM(half, BF16),
        pltpu.SemaphoreType.DMA((len(pieces),)),
        pltpu.SemaphoreType.DMA((2,)),
        pltpu.SemaphoreType.DMA((2,)),
    ]
    return call(ahead_kernel, pieces, weights, (half, half), scratch, 2)


def body(later_rows, earlier_rows, cotangent, up_weight, down_weight, up_total, down_total):
    n_dev = math.prod(lax.axis_size(a) for a in ALL)
    nz, nx = lax.axis_size("z"), lax.axis_size("x")
    factor = 1.0 / math.sqrt(later_rows.shape[0] * n_dev)
    weights = jnp.concatenate((up_weight, down_weight), axis=1)
    weights = gather(weights, "x").reshape(-1, weights.shape[1])
    weights = lax.all_gather(weights, "z", axis=0, tiled=True)
    pieces = gather_tokens((earlier_rows, cotangent, later_rows))
    down_term, up_term, mine, theirs = back(pieces, weights, nz, nx)
    down_term = lax.psum_scatter(down_term, "z", scatter_dimension=0, tiled=True)
    up_term = exchange_sum(up_term, "x").astype(BF16)
    up_term = exchange_sum(up_term, "z")
    earlier_grad = scatter_tokens(mine, theirs)
    mine, theirs = ahead_of(pieces, weights)
    later_out = scatter_tokens(mine, theirs)
    down_term = hop_sum(down_term.reshape(-1, *down_weight.shape), "x")
    up_updated = up_total + up_term * factor
    down_updated = down_total + down_term * factor
    return later_out, earlier_grad, up_updated, down_updated


def solution(mesh):
    n_tp = mesh.shape["tp"]
    finer = Mesh(mesh.devices.reshape(8, 4, n_tp // 2, 2), ALL)
    rows, weight = P(ALL, None), P(FS, ("y", "c"))
    return jax.shard_map(
        body,
        mesh=finer,
        in_specs=(rows, rows, rows, weight, weight, weight, weight),
        out_specs=(rows, rows, weight, weight),
        check_vma=False,
    )
```

time: 222 us -> 196 us (0.88)
  local copies, waits for them, and re-layouts: 54.2 us -> 3.32 us
  waiting for transfers between devices: 47.5 us -> 82.2 us
  Pallas kernels: 0 us -> 29.8 us
  matrix products: 27.9 us -> 0 us
  blocking collectives: 24 us -> 13.7 us
    ppermute x19 -> x22, waiting for transfers between devices: 27.1 us -> 64.5 us  [shift(): return lax.ppermute(x, axis, [(i, (i + by) % n) for i in range(n)])]
    pallas_call x0 -> x2, Pallas kernels: none -> 29.8 us  [call(): pl.pallas_call(kernel, out_shape=[jax.ShapeDtypeStruct(s, BF16) for s in...]
    dynamic_update_slice x10 -> x0, local copies, waits for them, and re-layouts: 28.8 us -> none  [place(): return lax.dynamic_update_slice(buffer, piece[:, None], (0, slot, row, 0))]
    dot_general x6 -> x0, matrix products: 27.9 us -> none  [the longest x2 12.3 us: rows_times(): lax.dot_general(left, right, (((1,), (1,)), ((), ())), preferred_element_...]
    all_to_all x1, blocking collectives: 24 us -> 13.7 us  [gather(): lax.all_to_all(jnp.broadcast_to(x[None], (n, *x.shape)), axis, 0, 0, tile...]
    another operation x1 -> x0, local copies, waits for them, and re-layouts: 8.93 us -> none  [gather_tokens(): return tuple((g.reshape(-1, g.shape[-1]) for g in group))]
    all_to_all x5 -> x2, starting transfers between devices: 20.5 us -> 12.1 us  [exchange_sum(): tiles = lax.all_to_all(term, axis, 0, 0, tiled=True)]
    ppermute x19 -> x22, starting transfers between devices: 13.6 us -> 20.7 us  [shift(): return lax.ppermute(x, axis, [(i, (i + by) % n) for i in range(n)])]
  transfers between devices with their start and end apart: 26 -> 26, of which waited for: 12 -> 15; matrix products, arithmetic and copies ran while one was open for 37% -> 8% of each run, Pallas kernels for 0% -> 5%
where the time goes in v3:
time: 196 us; the launch traced here: 194 us
  waiting for transfers between devices  82.2 us (42%)
  starting transfers between devices  32.9 us (17%)
  Pallas kernels  29.8 us (15%)
  other arithmetic  17.5 us (9%)
  between operations  14.3 us (7%)
  blocking collectives  13.7 us (7%)
  local copies, waits for them, and re-layouts  3.32 us (2%)
    ppermute x22, waiting for transfers between devices, shift(): return lax.ppermute(x, axis, [(i, (i + by) % n) for i in range(n)])  64.5 us
    pallas_call x2, Pallas kernels, call(): pl.pallas_call(kernel, out_shape=[jax.ShapeDtypeStruct(s, BF16) for s in...  29.8 us
    ppermute x22, starting transfers between devices, shift(): return lax.ppermute(x, axis, [(i, (i + by) % n) for i in range(n)])  20.7 us
    all_to_all x2, waiting for transfers between devices, exchange_sum(): tiles = lax.all_to_all(term, axis, 0, 0, tiled=True)  17.7 us
    all_to_all x1, blocking collectives, gather(): lax.all_to_all(jnp.broadcast_to(x[None], (n, *x.shape)), axis, 0, 0, tile...  13.7 us
    all_to_all x2, starting transfers between devices, exchange_sum(): tiles = lax.all_to_all(term, axis, 0, 0, tiled=True)  12.1 us
    convert_element_type x4, other arithmetic, plus(): return (a.astype(F32) + b.astype(F32)).astype(BF16)  5.63 us
    convert_element_type x2, other arithmetic, scatter_tokens(): return (own.astype(F32) + a.astype(F32) + b.astype(F32)).astype(BF16)  4.63 us
  transfers between devices with their start and end apart: 26, of which 15 were waited for; matrix products, arithmetic and copies ran while one was open for 8% of the time, Pallas kernels for 5%

profile of v3, /device:TPU:8, one launch (start us, length us, event | category | flops | bytes accessed | tf_op | source)
XLA Modules:
  0.0 193.7 jit_solution(3698675726971477071)
XLA Ops:
  8.3 13.7 %all_to_all.15 = bf16[4,64,1024]{2,1,0:T(8,128)(2,1)} all-to-all(bf16[4,64,1024]{2,1,0:T(8,128)(2,1)S(1)} %broadcast_in_dim.2), channel_id=1, replica_groups=mesh['z'=8,'x'=4,'y'=4,'c'=2] {'x'}, dimensions={0} | all-to-all | bytes 1048576 | tf_op jit(solution)/shard_map/all_to_all | solution.py:56
  22.2 1.7 collective-permute-start
  24.3 33.0 %collective-permute-done.refs_1_ = bf16[3,128,2048]{2,1,0:T(8,128)(2,1)S(1)} collective-permute-done((bf16[3,128,2048]{2,1,0:T(8,128)(2,1)S(1)}, bf16[3,128,2048]{2,1,0:T(8,128)(2,1)S(1)}, u32[]{:S(2)}, u32[]{:S(2)}) %collective-permute-start) | collective-permute-done | bytes 1572896 | tf_op jit(solution)/shard_map/ppermute | solution.py:21
  57.3 1.7 collective-permute-start.2
  60.1 14.7 %collective-permute-done.2.refs_3_ = bf16[3,64,2048]{2,1,0:T(8,128)(2,1)S(1)} collective-permute-done((bf16[3,64,2048]{2,1,0:T(8,128)(2,1)S(1)}, bf16[3,64,2048]{2,1,0:T(8,128)(2,1)S(1)}, u32[]{:S(2)}, u32[]{:S(2)}) %collective-permute-start.2) | collective-permute-done | bytes 786464 | tf_op jit(solution)/shard_map/ppermute | solution.py:21
  80.6 20.7 %shard_map.103 = (bf16[2048,512]{1,0:T(8,128)(2,1)}, bf16[4,8,64,512]{3,2,1,0:T(8,128)(2,1)}, bf16[512,2048]{1,0:T(8,128)(2,1)}, bf16[512,2048]{1,0:T(8,128)(2,1)}) custom-call(bf16[3,128,2048]{2,1,0:T(8,128)(2,1)} %copy-done.1, bf16[3,128,2048]{2,1,0:T(8,128)(2,1)} %copy-done.2, bf16[3,128,2048]{2,1,0:T(8,128)(2,1)} %copy-done.3, ...), custom_call_target="tpu_custom_call" | custom-call | flops 10737418240 | bytes 20971520 | tf_op jit(solution)/shard_map/pallas_call | solution.py:198
  101.7 3.6 %all-to-all-start.1 = ((bf16[4,8,64,512]{3,2,1,0:T(8,128)(2,1)}), bf16[4,8,64,512]{3,2,1,0:T(8,128)(2,1)S(1)}, u32[]{:S(2)}, u32[]{:S(2)}) async-start(bf16[4,8,64,512]{3,2,1,0:T(8,128)(2,1)} %get-tuple-element.14), calls=%async_computation.1 | async-start | bytes 4194304 | tf_op jit(solution)/shard_map/all_to_all | solution.py:60
  105.4 9.1 %shard_map.102 = (bf16[512,2048]{1,0:T(8,128)(2,1)}, bf16[512,2048]{1,0:T(8,128)(2,1)}) custom-call(bf16[3,128,2048]{2,1,0:T(8,128)(2,1)} %copy-done.1, bf16[3,128,2048]{2,1,0:T(8,128)(2,1)} %copy-done.2, bf16[3,128,2048]{2,1,0:T(8,128)(2,1)} %copy-done.3, bf16[3,64,2048]{2,1,0:T(8,128)(2,1)} %copy-done.7, bf16[3,64,2048]{2,1,0:T(8,128)(2,1)} %copy-done.8, ...), custom_call_target="tpu_custom_call" | custom-call | flops 4294967296 | bytes 20971520 | tf_op jit(solution)/shard_map/pallas_call | solution.py:198
  115.0 17.4 %all-to-all-done.1 = bf16[4,8,64,512]{3,2,1,0:T(8,128)(2,1)S(1)} async-done(((bf16[4,8,64,512]{3,2,1,0:T(8,128)(2,1)}), bf16[4,8,64,512]{3,2,1,0:T(8,128)(2,1)S(1)}, u32[]{:S(2)}, u32[]{:S(2)}) %all-to-all-start.1) | async-done | bytes 2097184 | tf_op jit(solution)/shard_map/all_to_all | solution.py:60
  133.7 8.5 %all-to-all-start.2 = ((bf16[8,64,512]{2,1,0:T(8,128)(2,1)}), bf16[8,64,512]{2,1,0:T(8,128)(2,1)S(1)}, u32[]{:S(2)}, u32[]{:S(2)}) async-start(bf16[8,64,512]{2,1,0:T(8,128)(2,1)} %reduce_sum.21), calls=%async_computation.2 | async-start | bytes 1048576 | tf_op jit(solution)/shard_map/all_to_all | solution.py:60
  142.2 3.0 %add_convert_fusion = bf16[512,2048]{1,0:T(8,128)(2,1)S(1)} fusion(bf16[512,2048]{1,0:T(8,128)(2,1)} %collective-permute-done.14, bf16[512,2048]{1,0:T(8,128)(2,1)} %get-tuple-element.12), kind=kLoop, calls=%fused_computation | loop fusion | flops 4194304 | bytes 6291456 | tf_op jit(solution)/shard_map/convert_element_type | solution.py:37
  146.7 1.5 collective-permute-start.17
  148.2 2.4 %add_convert_fusion.1 = bf16[512,2048]{1,0:T(8,128)(2,1)S(1)} fusion(bf16[512,2048]{1,0:T(8,128)(2,1)} %collective-permute-done.9, bf16[512,2048]{1,0:T(8,128)(2,1)S(1)} %copy-done.4), kind=kLoop, calls=%fused_computation.1 | loop fusion | flops 4194304 | bytes 6291456 | tf_op jit(solution)/shard_map/convert_element_type | solution.py:37
  152.1 1.9 %collective-permute-start.12 = (bf16[64,2048]{1,0:T(8,128)(2,1)S(1)}, bf16[64,2048]{1,0:T(8,128)(2,1)S(1)}, u32[]{:S(2)}, u32[]{:S(2)}) collective-permute-start(bf16[64,2048]{1,0:T(8,128)(2,1)S(1)} %get-tuple-element.25), channel_id=1, source_target_pairs={{0,6},{2,0},{4,2},{6,4},{1,7},{3,1},{5,3},{7,5},{8,14},{10,8},{12,... | collective-permute-start | bytes 786440 | tf_op jit(solution)/shard_map/ppermute | solution.py:21
  154.2 1.6 collective-permute-done.17
  156.8 1.7 collective-permute-start.16
  161.3 1.8 collective-permute-start.11
  164.0 1.4 collective-permute-start.13
  166.5 5.9 %collective-permute-done.16 = bf16[128,2048]{1,0:T(8,128)(2,1)} collective-permute-done((bf16[128,2048]{1,0:T(8,128)(2,1)}, bf16[128,2048]{1,0:T(8,128)(2,1)}, u32[]{:S(2)}, u32[]{:S(2)}) %collective-permute-start.16) | collective-permute-done | bytes 524320 | tf_op jit(solution)/shard_map/ppermute | solution.py:21
  172.4 2.0 %collective-permute-done.18 = bf16[128,2048]{1,0:T(8,128)(2,1)} collective-permute-done((bf16[128,2048]{1,0:T(8,128)(2,1)}, bf16[128,2048]{1,0:T(8,128)(2,1)}, u32[]{:S(2)}, u32[]{:S(2)}) %collective-permute-start.18) | collective-permute-done | bytes 524320 | tf_op jit(solution)/shard_map/ppermute | solution.py:21
  174.4 2.4 %add_convert_fusion.2 = bf16[128,2048]{1,0:T(8,128)(2,1)} fusion(bf16[128,2048]{1,0:T(8,128)(2,1)} %collective-permute-done.18, bf16[128,2048]{1,0:T(8,128)(2,1)} %collective-permute-done.16, bf16[512,2048]{1,0:T(8,128)(2,1)} %copy-done), kind=kLoop, calls=%fused_computation.4 | loop fusion | flops 1572864 | bytes 2097152 | tf_op jit(solution)/shard_map/convert_element_type | solution.py:51
  178.5 1.9 %collective-permute-start.20 = (bf16[64,512]{1,0:T(8,128)(2,1)S(1)}, bf16[64,512]{1,0:T(8,128)(2,1)S(1)}, u32[]{:S(2)}, u32[]{:S(2)}) collective-permute-start(bf16[64,512]{1,0:T(8,128)(2,1)S(1)} %get-tuple-element.30), channel_id=1, source_target_pairs={{0,16},{8,24},{16,0},{24,8},{1,17},{9,25},{17,1},{25,9},{2,18},{10... | collective-permute-start | bytes 196616 | tf_op jit(solution)/shard_map/ppermute | solution.py:21
  183.1 2.2 %add_convert_fusion.3 = bf16[128,2048]{1,0:T(8,128)(2,1)} fusion(bf16[128,2048]{1,0:T(8,128)(2,1)} %collective-permute-done.13, bf16[128,2048]{1,0:T(8,128)(2,1)} %collective-permute-done.11, bf16[512,2048]{1,0:T(8,128)(2,1)S(1)} %add_convert_fusion.1), kind=kLoop, calls=%fused_computation.5 | loop fusion | flops 1572864 | bytes 2097152 | tf_op jit(solution)/shard_map/convert_element_type | solution.py:51
  185.4 1.5 fusion.3
  (87 shorter events, 24.0 us)
Async XLA Ops:
  7.2 73.4 %all-gather.2.cloned.1.call-start = ((), (), s32[]{:S(2)}) async-start(), calls=%async_computation.4 | async-start | bytes 4718592 | tf_op jit(solution)/shard_map/all_gather | solution.py:258
  22.2 35.1 %collective-permute-start = (bf16[3,128,2048]{2,1,0:T(8,128)(2,1)S(1)}, bf16[3,128,2048]{2,1,0:T(8,128)(2,1)S(1)}, u32[]{:S(2)}, u32[]{:S(2)}) collective-permute-start(bf16[3,128,2048]{2,1,0:T(8,128)(2,1)S(1)} %pad_maximum_fusion.refs_0_), channel_id=1, source_target_pairs={{0,2},{2,4},{4,6},{6,0},{1,3},{3,5},{5,7},{7,1},{8,10},{10,12},{12... | collective-permute-start | bytes 4718600 | tf_op jit(solution)/shard_map/ppermute | solution.py:21
  23.9 35.1 %collective-permute-start.1 = (bf16[3,128,2048]{2,1,0:T(8,128)(2,1)S(1)}, bf16[3,128,2048]{2,1,0:T(8,128)(2,1)S(1)}, u32[]{:S(2)}, u32[]{:S(2)}) collective-permute-start(bf16[3,128,2048]{2,1,0:T(8,128)(2,1)S(1)} %pad_maximum_fusion.refs_0_), channel_id=1, source_target_pairs={{0,6},{2,0},{4,2},{6,4},{1,7},{3,1},{5,3},{7,5},{8,14},{10,8},{12,... | collective-permute-start | bytes 4718600 | tf_op jit(solution)/shard_map/ppermute | solution.py:21
  24.3 52.0 %collective-permute-start.4 = (bf16[3,128,2048]{2,1,0:T(8,128)(2,1)S(1)}, bf16[3,128,2048]{2,1,0:T(8,128)(2,1)S(1)}, u32[]{:S(2)}, u32[]{:S(2)}) collective-permute-start(bf16[3,128,2048]{2,1,0:T(8,128)(2,1)S(1)} %pad_maximum_fusion.refs_0_), channel_id=1, source_target_pairs={{0,1},{1,0},{2,3},{3,2},{4,5},{5,4},{6,7},{7,6},{8,9},{9,8},{10,11... | collective-permute-start | bytes 4718600 | tf_op jit(solution)/shard_map/ppermute | solution.py:21
  57.3 17.5 %collective-permute-start.2 = (bf16[3,64,2048]{2,1,0:T(8,128)(2,1)S(1)}, bf16[3,64,2048]{2,1,0:T(8,128)(2,1)S(1)}, u32[]{:S(2)}, u32[]{:S(2)}) collective-permute-start(bf16[3,64,2048]{2,1,0:T(8,128)(2,1)S(1)} %slice.82), channel_id=1, source_target_pairs={{0,2},{2,4},{4,6},{6,0},{1,3},{3,5},{5,7},{7,1},{8,10},{10,12},{12... | collective-permute-start | bytes 2359304 | tf_op jit(solution)/shard_map/ppermute | solution.py:21
  59.1 17.2 %collective-permute-start.3 = (bf16[3,64,2048]{2,1,0:T(8,128)(2,1)S(1)}, bf16[3,64,2048]{2,1,0:T(8,128)(2,1)S(1)}, u32[]{:S(2)}, u32[]{:S(2)}) collective-permute-start(bf16[3,64,2048]{2,1,0:T(8,128)(2,1)S(1)} %slice.83), channel_id=1, source_target_pairs={{0,6},{2,0},{4,2},{6,4},{1,7},{3,1},{5,3},{7,5},{8,14},{10,8},{12,... | collective-permute-start | bytes 2359304 | tf_op jit(solution)/shard_map/ppermute | solution.py:21
  59.6 19.0 %collective-permute-start.5 = (bf16[3,128,2048]{2,1,0:T(8,128)(2,1)S(1)}, bf16[3,128,2048]{2,1,0:T(8,128)(2,1)S(1)}, u32[]{:S(2)}, u32[]{:S(2)}) collective-permute-start(bf16[3,128,2048]{2,1,0:T(8,128)(2,1)S(1)} %collective-permute-done.refs_1_), channel_id=1, source_target_pairs={{0,1},{1,0},{2,3},{3,2},{4,5},{5,4},{6,7},{7,6},{8,9},{9,8},{10,11... | collective-permute-start | bytes 4718600 | tf_op jit(solution)/shard_map/ppermute | solution.py:21
  59.6 21.0 %collective-permute-start.6 = (bf16[3,128,2048]{2,1,0:T(8,128)(2,1)S(1)}, bf16[3,128,2048]{2,1,0:T(8,128)(2,1)}, u32[]{:S(2)}, u32[]{:S(2)}) collective-permute-start(bf16[3,128,2048]{2,1,0:T(8,128)(2,1)S(1)} %collective-permute-done.1.refs_2_), channel_id=1, source_target_pairs={{0,1},{1,0},{2,3},{3,2},{4,5},{5,4},{6,7},{7,6},{8,9},{9,8},{10,11... | collective-permute-start | bytes 4718600 | tf_op jit(solution)/shard_map/ppermute | solution.py:21
  101.3 40.9 %collective-permute-start.14 = (bf16[512,2048]{1,0:T(8,128)(2,1)}, bf16[512,2048]{1,0:T(8,128)(2,1)}, u32[]{:S(2)}, u32[]{:S(2)}) collective-permute-start(bf16[512,2048]{1,0:T(8,128)(2,1)} %get-tuple-element.13), channel_id=1, source_target_pairs={{0,1},{1,0},{2,3},{3,2},{4,5},{5,4},{6,7},{7,6},{8,9},{9,8},{10,11... | collective-permute-start | bytes 6291464 | tf_op jit(solution)/shard_map/ppermute | solution.py:21
  101.7 30.7 %all-to-all-start.1 = ((bf16[4,8,64,512]{3,2,1,0:T(8,128)(2,1)}), bf16[4,8,64,512]{3,2,1,0:T(8,128)(2,1)S(1)}, u32[]{:S(2)}, u32[]{:S(2)}) async-start(bf16[4,8,64,512]{3,2,1,0:T(8,128)(2,1)} %get-tuple-element.14), calls=%async_computation.1 | async-start | bytes 4194304 | tf_op jit(solution)/shard_map/all_to_all | solution.py:60
  105.3 71.5 %reduce-scatter.2.cloned.1.call-start = ((), (), s32[]{:S(2)}) async-start(), calls=%async_computation.5 | async-start | bytes 2359296 | tf_op jit(solution)/shard_map/reduce_scatter | solution.py:261
  114.5 33.7 %collective-permute-start.9 = (bf16[512,2048]{1,0:T(8,128)(2,1)}, bf16[512,2048]{1,0:T(8,128)(2,1)}, u32[]{:S(2)}, u32[]{:S(2)}) collective-permute-start(bf16[512,2048]{1,0:T(8,128)(2,1)} %get-tuple-element.11), channel_id=1, source_target_pairs={{0,1},{1,0},{2,3},{3,2},{4,5},{5,4},{6,7},{7,6},{8,9},{9,8},{10,11... | collective-permute-start | bytes 6291464 | tf_op jit(solution)/shard_map/ppermute | solution.py:21
  133.7 32.0 %all-to-all-start.2 = ((bf16[8,64,512]{2,1,0:T(8,128)(2,1)}), bf16[8,64,512]{2,1,0:T(8,128)(2,1)S(1)}, u32[]{:S(2)}, u32[]{:S(2)}) async-start(bf16[8,64,512]{2,1,0:T(8,128)(2,1)} %reduce_sum.21), calls=%async_computation.2 | async-start | bytes 1048576 | tf_op jit(solution)/shard_map/all_to_all | solution.py:60
  145.3 8.9 %collective-permute-start.15 = (bf16[64,2048]{1,0:T(8,128)(2,1)S(1)}, bf16[64,2048]{1,0:T(8,128)(2,1)S(1)}, u32[]{:S(2)}, u32[]{:S(2)}) collective-permute-start(bf16[64,2048]{1,0:T(8,128)(2,1)S(1)} %get-tuple-element.18), channel_id=1, source_target_pairs={{0,2},{2,4},{4,6},{6,0},{1,3},{3,5},{5,7},{7,1},{8,10},{10,12},{12... | collective-permute-start | bytes 786440 | tf_op jit(solution)/shard_map/ppermute | solution.py:21
  146.7 9.1 %collective-permute-start.17 = (bf16[64,2048]{1,0:T(8,128)(2,1)S(1)}, bf16[64,2048]{1,0:T(8,128)(2,1)S(1)}, u32[]{:S(2)}, u32[]{:S(2)}) collective-permute-start(bf16[64,2048]{1,0:T(8,128)(2,1)S(1)} %get-tuple-element.19), channel_id=1, source_target_pairs={{0,6},{2,0},{4,2},{6,4},{1,7},{3,1},{5,3},{7,5},{8,14},{10,8},{12,... | collective-permute-start | bytes 786440 | tf_op jit(solution)/shard_map/ppermute | solution.py:21
  150.7 10.4 %collective-permute-start.10 = (bf16[64,2048]{1,0:T(8,128)(2,1)S(1)}, bf16[64,2048]{1,0:T(8,128)(2,1)S(1)}, u32[]{:S(2)}, u32[]{:S(2)}) collective-permute-start(bf16[64,2048]{1,0:T(8,128)(2,1)S(1)} %get-tuple-element.24), channel_id=1, source_target_pairs={{0,2},{2,4},{4,6},{6,0},{1,3},{3,5},{5,7},{7,1},{8,10},{10,12},{12... | collective-permute-start | bytes 786440 | tf_op jit(solution)/shard_map/ppermute | solution.py:21
  152.1 9.1 %collective-permute-start.12 = (bf16[64,2048]{1,0:T(8,128)(2,1)S(1)}, bf16[64,2048]{1,0:T(8,128)(2,1)S(1)}, u32[]{:S(2)}, u32[]{:S(2)}) collective-permute-start(bf16[64,2048]{1,0:T(8,128)(2,1)S(1)} %get-tuple-element.25), channel_id=1, source_target_pairs={{0,6},{2,0},{4,2},{6,4},{1,7},{3,1},{5,3},{7,5},{8,14},{10,8},{12,... | collective-permute-start | bytes 786440 | tf_op jit(solution)/shard_map/ppermute | solution.py:21
  156.8 15.6 %collective-permute-start.16 = (bf16[128,2048]{1,0:T(8,128)(2,1)}, bf16[128,2048]{1,0:T(8,128)(2,1)}, u32[]{:S(2)}, u32[]{:S(2)}) collective-permute-start(bf16[128,2048]{1,0:T(8,128)(2,1)} %pad_maximum_fusion.3), channel_id=1, source_target_pairs={{0,2},{2,4},{4,6},{6,0},{1,3},{3,5},{5,7},{7,1},{8,10},{10,12},{12... | collective-permute-start | bytes 1572872 | tf_op jit(solution)/shard_map/ppermute | solution.py:21
  159.3 15.1 %collective-permute-start.18 = (bf16[128,2048]{1,0:T(8,128)(2,1)}, bf16[128,2048]{1,0:T(8,128)(2,1)}, u32[]{:S(2)}, u32[]{:S(2)}) collective-permute-start(bf16[128,2048]{1,0:T(8,128)(2,1)} %pad_maximum_fusion.4), channel_id=1, source_target_pairs={{0,6},{2,0},{4,2},{6,4},{1,7},{3,1},{5,3},{7,5},{8,14},{10,8},{12,... | collective-permute-start | bytes 1572872 | tf_op jit(solution)/shard_map/ppermute | solution.py:21
  161.3 20.7 %collective-permute-start.11 = (bf16[128,2048]{1,0:T(8,128)(2,1)S(1)}, bf16[128,2048]{1,0:T(8,128)(2,1)}, u32[]{:S(2)}, u32[]{:S(2)}) collective-permute-start(bf16[128,2048]{1,0:T(8,128)(2,1)S(1)} %pad_maximum_fusion.1), channel_id=1, source_target_pairs={{0,2},{2,4},{4,6},{6,0},{1,3},{3,5},{5,7},{7,1},{8,10},{10,12},{12... | collective-permute-start | bytes 1572872 | tf_op jit(solution)/shard_map/ppermute | solution.py:21
  164.0 19.1 %collective-permute-start.13 = (bf16[128,2048]{1,0:T(8,128)(2,1)}, bf16[128,2048]{1,0:T(8,128)(2,1)}, u32[]{:S(2)}, u32[]{:S(2)}) collective-permute-start(bf16[128,2048]{1,0:T(8,128)(2,1)} %pad_maximum_fusion.2), channel_id=1, source_target_pairs={{0,6},{2,0},{4,2},{6,4},{1,7},{3,1},{5,3},{7,5},{8,14},{10,8},{12,... | collective-permute-start | bytes 1572872 | tf_op jit(solution)/shard_map/ppermute | solution.py:21
  177.7 7.6 %collective-permute-start.19 = (bf16[64,512]{1,0:T(8,128)(2,1)S(1)}, bf16[64,512]{1,0:T(8,128)(2,1)S(1)}, u32[]{:S(2)}, u32[]{:S(2)}) collective-permute-start(bf16[64,512]{1,0:T(8,128)(2,1)S(1)} %get-tuple-element.28), channel_id=1, source_target_pairs={{0,8},{8,16},{16,24},{24,0},{1,9},{9,17},{17,25},{25,1},{2,10},{10... | collective-permute-start | bytes 196616 | tf_op jit(solution)/shard_map/ppermute | solution.py:21
  178.5 6.8 %collective-permute-start.20 = (bf16[64,512]{1,0:T(8,128)(2,1)S(1)}, bf16[64,512]{1,0:T(8,128)(2,1)S(1)}, u32[]{:S(2)}, u32[]{:S(2)}) collective-permute-start(bf16[64,512]{1,0:T(8,128)(2,1)S(1)} %get-tuple-element.30), channel_id=1, source_target_pairs={{0,16},{8,24},{16,0},{24,8},{1,17},{9,25},{17,1},{25,9},{2,18},{10... | collective-permute-start | bytes 196616 | tf_op jit(solution)/shard_map/ppermute | solution.py:21
  180.5 4.9 %collective-permute-start.21 = (bf16[64,512]{1,0:T(8,128)(2,1)S(1)}, bf16[64,512]{1,0:T(8,128)(2,1)S(1)}, u32[]{:S(2)}, u32[]{:S(2)}) collective-permute-start(bf16[64,512]{1,0:T(8,128)(2,1)S(1)} %get-tuple-element.29), channel_id=1, source_target_pairs={{0,24},{8,0},{16,8},{24,16},{1,25},{9,1},{17,9},{25,17},{2,26},{10... | collective-permute-start | bytes 196616 | tf_op jit(solution)/shard_map/ppermute | solution.py:21
  (18 other events, 201.2 us)
Sparse Core Ops, SparseCore 0:
  22.1 55.7 all-gather.1
  115.1 54.9 reduce-scatter.1

commit v4 on v3

--- a/solution.py
+++ b/solution.py
@@ -66,7 +66,7 @@
     me = lax.axis_index(axis)
 
     def block(by):
-        at = lax.rem(me + by, n)
+        at = (me + by) & (n - 1)
         start = (at, *(0 for _ in term.shape[1:]))
         part = lax.dynamic_slice(term, start, (1, *term.shape[1:]), allow_negative_indices=False)
         return part[0]
@@ -103,9 +103,9 @@
     return jnp.maximum(jnp.dot(rows, weight, preferred_element_type=F32), 0.0)
 
 
-def back_kernel(*refs):
-    pieces, (w, down_out, up_out, mine_out, theirs_out) = refs[:10], refs[10:15]
-    saved, cot, up, down, relu, hid, pg, dt, ut, mine, theirs, in_sems, w_sems, out_sems = refs[15:]
+def up_kernel(*refs):
+    pieces, (w, up_out, hid_out, pg_out) = refs[:10], refs[10:14]
+    saved, cot, up, down, relu, hid, pg, ut, in_sems, w_sems, out_sems = refs[14:]
     cols = up.shape[1]
     up_copy = pltpu.make_async_copy(w.at[:, pl.ds(0, cols)], up, w_sems.at[0])
     up_copy.start()
@@ -126,12 +126,9 @@
         at = pl.ds(t, TILE)
         grad = jnp.dot(cot[at], down[...], preferred_element_type=F32)
         pg[at] = (2.0 * relu[at] * grad).astype(BF16)
+    hid_copy = pltpu.make_async_copy(hid, hid_out, out_sems.at[0])
+    hid_copy.start()
     nx, nz, part = ut.shape[:3]
-
-    @pl.loop(0, nz)
-    def _(i):
-        at = pl.ds(pl.multiple_of(i * nx * part, nx * part), nx * part)
-        dt[at] = over_tokens(cot[:, at], hid[...]).astype(BF16)
 
     @pl.loop(0, nz)
     def _(i):
@@ -140,20 +137,49 @@
         for j in range(nx):
             ut[j, i] = term[j * part : (j + 1) * part]
 
-    done = [
-        pltpu.make_async_copy(a, b, out_sems.at[i])
-        for i, (a, b) in enumerate(
-            ((dt, down_out), (ut, up_out), (mine, mine_out), (theirs, theirs_out))
-        )
-    ]
-    done[0].start()
+    pg_copy = pltpu.make_async_copy(pg, pg_out, out_sems.at[1])
+    pg_copy.start()
+    ut_copy = pltpu.make_async_copy(ut, up_out, out_sems.at[2])
+    ut_copy.start()
+    hid_copy.wait()
+    pg_copy.wait()
+    ut_copy.wait()
+
+
+def down_kernel(*refs):
+    pieces, (hid_in, down_out) = refs[:10], refs[10:12]
+    cot, hid, dt, in_sems, sems = refs[12:]
+    hid_copy = pltpu.make_async_copy(hid_in, hid, sems.at[0])
+    hid_copy.start()
+    settle(copies(pieces, cot, in_sems, 1), cot.shape[0])
+    hid_copy.wait()
+    block = dt.shape[0] // 8
+
+    @pl.loop(0, 8)
+    def _(i):
+        at = pl.ds(pl.multiple_of(i * block, block), block)
+        dt[at] = over_tokens(cot[:, at], hid[...]).astype(BF16)
+
+    out_copy = pltpu.make_async_copy(dt, down_out, sems.at[1])
+    out_copy.start()
+    out_copy.wait()
+
+
+def rows_kernel(pg_in, w, mine_out, theirs_out, pg, up, mine, theirs, sems):
+    pg_copy = pltpu.make_async_copy(pg_in, pg, sems.at[0])
+    up_copy = pltpu.make_async_copy(w.at[:, pl.ds(0, up.shape[1])], up, sems.at[1])
+    pg_copy.start()
+    up_copy.start()
+    pg_copy.wait()
+    up_copy.wait()
+    first = pltpu.make_async_copy(mine, mine_out, sems.at[2])
+    second = pltpu.make_async_copy(theirs, theirs_out, sems.at[3])
+    outputs(pg, mine.shape[0], up, theirs)
     outputs(pg, 0, up, mine)
-    done[1].start()
-    outputs(pg, mine.shape[0], up, theirs)
-    done[2].start()
-    done[3].start()
-    for copy in done:
-        copy.wait()
+    second.start()
+    first.start()
+    first.wait()
+    second.wait()
 
 
 def outputs(hidden, first, weight, out):
@@ -191,62 +217,49 @@
     second.wait()
 
 
-def call(kernel, pieces, weights, outs, scratch, dots):
-    rows = sum(p.shape[1] for p in pieces)
-    depth, cols = weights.shape[0], weights.shape[1] // 2
+def call(kernel, operands, outs, scratch, flops):
     hbm = pl.BlockSpec(memory_space=pltpu.HBM)
     return pl.pallas_call(
         kernel,
         out_shape=[jax.ShapeDtypeStruct(s, BF16) for s in outs],
-        in_specs=[hbm] * (len(pieces) + 1),
+        in_specs=[hbm] * len(operands),
         out_specs=[hbm] * len(outs),
-        scratch_shapes=scratch,
-        cost_estimate=pl.CostEstimate(
-            flops=2 * dots * rows * depth * cols, bytes_accessed=20 << 20, transcendentals=0
-        ),
+        scratch_shapes=[pltpu.VMEM(*s) for s in scratch[0]]
+        + [pltpu.SemaphoreType.DMA(s) for s in scratch[1]],
+        cost_estimate=pl.CostEstimate(flops=flops, bytes_accessed=12 << 20, transcendentals=0),
         compiler_params=pltpu.CompilerParams(vmem_limit_bytes=60 * 1024 * 1024),
-    )(*pieces, weights)
-
-
-def back(pieces, weights, nz, nx):
+    )(*operands)
+
+
+def products(pieces, weights, nz, nx):
     rows = sum(p.shape[1] for p in pieces)
     depth, cols = weights.shape[0], weights.shape[1] // 2
     n = len(pieces)
+    flops = 2 * rows * depth * cols
+    group, weight, wide = ((rows, depth), BF16), ((depth, cols), BF16), ((rows, cols), BF16)
     up_shape = (nx, nz, depth // (nx * nz), cols)
     half = (rows // 2, depth)
-    outs = ((depth, cols), up_shape, half, half)
-    scratch = [
-        pltpu.VMEM((rows, depth), BF16),
-        pltpu.VMEM((rows, depth), BF16),
-        pltpu.VMEM((depth, cols), BF16),
-        pltpu.VMEM((depth, cols), BF16),
-        pltpu.VMEM((rows, cols), F32),
-        pltpu.VMEM((rows, cols), BF16),
-        pltpu.VMEM((rows, cols), BF16),
-        *(pltpu.VMEM(s, BF16) for s in outs),
-        pltpu.SemaphoreType.DMA((2, n)),
-        pltpu.SemaphoreType.DMA((2,)),
-        pltpu.SemaphoreType.DMA((4,)),
-    ]
-    return call(back_kernel, pieces, weights, outs, scratch, 5)
-
-
-def ahead_of(pieces, weights):
-    rows = sum(p.shape[1] for p in pieces)
-    depth, cols = weights.shape[0], weights.shape[1] // 2
-    half = (rows // 2, depth)
-    scratch = [
-        pltpu.VMEM((rows, depth), BF16),
-        pltpu.VMEM((depth, cols), BF16),
-        pltpu.VMEM((depth, cols), BF16),
-        pltpu.VMEM((rows, cols), BF16),
-        pltpu.VMEM(half, BF16),
-        pltpu.VMEM(half, BF16),
-        pltpu.SemaphoreType.DMA((len(pieces),)),
-        pltpu.SemaphoreType.DMA((2,)),
-        pltpu.SemaphoreType.DMA((2,)),
-    ]
-    return call(ahead_kernel, pieces, weights, (half, half), scratch, 2)
+
+    def up_term():
+        vmem = (group, group, weight, weight, (wide[0], F32), wide, wide, (up_shape, BF16))
+        outs = (up_shape, wide[0], wide[0])
+        return call(up_kernel, (*pieces, weights), outs, (vmem, ((2, n), (2,), (3,))), 3 * flops)
+
+    def down_term(hidden):
+        vmem = (group, wide, weight)
+        return call(down_kernel, (*pieces, hidden), (weight[0],), (vmem, ((n,), (2,))), flops)[0]
+
+    def row_grad(pre_grad):
+        vmem = (wide, weight, (half, BF16), (half, BF16))
+        return call(rows_kernel, (pre_grad, weights), (half, half), (vmem, ((4,),)), flops)
+
+    def later():
+        vmem = (group, weight, weight, wide, (half, BF16), (half, BF16))
+        return call(
+            ahead_kernel, (*pieces, weights), (half, half), (vmem, ((n,), (2,), (2,))), 2 * flops
+        )
+
+    return up_term, down_term, row_grad, later
 
 
 def body(later_rows, earlier_rows, cotangent, up_weight, down_weight, up_total, down_total):
@@ -257,12 +270,15 @@
     weights = gather(weights, "x").reshape(-1, weights.shape[1])
     weights = lax.all_gather(weights, "z", axis=0, tiled=True)
     pieces = gather_tokens((earlier_rows, cotangent, later_rows))
-    down_term, up_term, mine, theirs = back(pieces, weights, nz, nx)
+    grad_up, grad_down, grad_rows, ahead = products(pieces, weights, nz, nx)
+    up_term, hidden, pre_grad = grad_up()
+    up_term = exchange_sum(up_term, "x").astype(BF16)
+    down_term = grad_down(hidden)
     down_term = lax.psum_scatter(down_term, "z", scatter_dimension=0, tiled=True)
-    up_term = exchange_sum(up_term, "x").astype(BF16)
     up_term = exchange_sum(up_term, "z")
+    mine, theirs = grad_rows(pre_grad)
     earlier_grad = scatter_tokens(mine, theirs)
-    mine, theirs = ahead_of(pieces, weights)
+    mine, theirs = ahead()
     later_out = scatter_tokens(mine, theirs)
     down_term = hop_sum(down_term.reshape(-1, *down_weight.shape), "x")
     up_updated = up_total + up_term * factor

time: 196 us -> 202 us (1.031)
  Pallas kernels: 29.8 us -> 37 us
    pallas_call x2 -> x4, Pallas kernels: 29.8 us -> 37 us  [call(): pl.pallas_call(kernel, out_shape=[jax.ShapeDtypeStruct(s, BF16) for s in...]
    all_to_all x2, waiting for transfers between devices: 17.7 us -> 13.1 us  [exchange_sum(): tiles = lax.all_to_all(term, axis, 0, 0, tiled=True)]
    ppermute x22, waiting for transfers between devices: 64.5 us -> 69 us  [shift(): return lax.ppermute(x, axis, [(i, (i + by) % n) for i in range(n)])]
  transfers between devices with their start and end apart: 26 -> 26, of which waited for: 15 -> 16; matrix products, arithmetic and copies ran while one was open for 8% -> 8% of each run, Pallas kernels for 5% -> 14%
where the time goes in v4:
time: 202 us; the launch traced here: 199 us
  waiting for transfers between devices  82.1 us (41%)
  Pallas kernels  37 us (18%)
  starting transfers between devices  32.3 us (16%)
  other arithmetic  17.5 us (9%)
  between operations  14.4 us (7%)
  blocking collectives  13.7 us (7%)
  local copies, waits for them, and re-layouts  2.2 us (1%)
    ppermute x22, waiting for transfers between devices, shift(): return lax.ppermute(x, axis, [(i, (i + by) % n) for i in range(n)])  69 us
    pallas_call x4, Pallas kernels, call(): pl.pallas_call(kernel, out_shape=[jax.ShapeDtypeStruct(s, BF16) for s in...  37 us
    ppermute x22, starting transfers between devices, shift(): return lax.ppermute(x, axis, [(i, (i + by) % n) for i in range(n)])  20.1 us
    all_to_all x1, blocking collectives, gather(): lax.all_to_all(jnp.broadcast_to(x[None], (n, *x.shape)), axis, 0, 0, tile...  13.7 us
    all_to_all x2, waiting for transfers between devices, exchange_sum(): tiles = lax.all_to_all(term, axis, 0, 0, tiled=True)  13.1 us
    all_to_all x2, starting transfers between devices, exchange_sum(): tiles = lax.all_to_all(term, axis, 0, 0, tiled=True)  12.1 us
    convert_element_type x4, other arithmetic, plus(): return (a.astype(F32) + b.astype(F32)).astype(BF16)  5.64 us
    convert_element_type x2, other arithmetic, scatter_tokens(): return (own.astype(F32) + a.astype(F32) + b.astype(F32)).astype(BF16)  4.63 us
  transfers between devices with their start and end apart: 26, of which 16 were waited for; matrix products, arithmetic and copies ran while one was open for 8% of the time, Pallas kernels for 14%

profile of v4, /device:TPU:8, one launch (start us, length us, event | category | flops | bytes accessed | tf_op | source)
XLA Modules:
  0.0 199.2 jit_solution(14563788257565166261)
XLA Ops:
  8.3 13.7 %all_to_all.15 = bf16[4,64,1024]{2,1,0:T(8,128)(2,1)} all-to-all(bf16[4,64,1024]{2,1,0:T(8,128)(2,1)S(1)} %broadcast_in_dim.2), channel_id=1, replica_groups=mesh['z'=8,'x'=4,'y'=4,'c'=2] {'x'}, dimensions={0} | all-to-all | bytes 1048576 | tf_op jit(solution)/shard_map/all_to_all | solution.py:56
  24.3 33.0 %collective-permute-done.1.refs_2_ = bf16[3,128,2048]{2,1,0:T(8,128)(2,1)S(1)} collective-permute-done((bf16[3,128,2048]{2,1,0:T(8,128)(2,1)S(1)}, bf16[3,128,2048]{2,1,0:T(8,128)(2,1)S(1)}, u32[]{:S(2)}, u32[]{:S(2)}) %collective-permute-start.1) | collective-permute-done | bytes 1572896 | tf_op jit(solution)/shard_map/ppermute | solution.py:21
  60.1 14.7 %collective-permute-done.3.refs_4_ = bf16[3,64,2048]{2,1,0:T(8,128)(2,1)S(1)} collective-permute-done((bf16[3,64,2048]{2,1,0:T(8,128)(2,1)S(1)}, bf16[3,64,2048]{2,1,0:T(8,128)(2,1)S(1)}, u32[]{:S(2)}, u32[]{:S(2)}) %collective-permute-start.3) | collective-permute-done | bytes 786464 | tf_op jit(solution)/shard_map/ppermute | solution.py:21
  74.8 2.8 %collective-permute-done.2.refs_3_ = bf16[3,64,2048]{2,1,0:T(8,128)(2,1)S(1)} collective-permute-done((bf16[3,64,2048]{2,1,0:T(8,128)(2,1)S(1)}, bf16[3,64,2048]{2,1,0:T(8,128)(2,1)S(1)}, u32[]{:S(2)}, u32[]{:S(2)}) %collective-permute-start.2) | collective-permute-done | bytes 786464 | tf_op jit(solution)/shard_map/ppermute | solution.py:21
  77.7 2.2 %collective-permute-done.7.refs_8_ = bf16[3,64,2048]{2,1,0:T(8,128)(2,1)S(1)} collective-permute-done((bf16[3,64,2048]{2,1,0:T(8,128)(2,1)S(1)}, bf16[3,64,2048]{2,1,0:T(8,128)(2,1)S(1)}, u32[]{:S(2)}, u32[]{:S(2)}) %collective-permute-start.7) | collective-permute-done | bytes 786464 | tf_op jit(solution)/shard_map/ppermute | solution.py:21
  80.9 9.1 %shard_map.102 = (bf16[512,2048]{1,0:T(8,128)(2,1)}, bf16[512,2048]{1,0:T(8,128)(2,1)}) custom-call(bf16[3,128,2048]{2,1,0:T(8,128)(2,1)} %copy-done, bf16[3,128,2048]{2,1,0:T(8,128)(2,1)} %copy-done.2, bf16[3,128,2048]{2,1,0:T(8,128)(2,1)} %copy-done.1, bf16[3,64,2048]{2,1,0:T(8,128)(2,1)} %copy-done.7, bf16[3,64,2048]{2,1,0:T(8,128)(2,1)} %copy-done.6, ...), custom_call_target="tpu_custom_call" | custom-call | flops 4294967296 | bytes 12582912 | tf_op jit(solution)/shard_map/pallas_call | solution.py:222
  90.4 14.4 %shard_map.103 = (bf16[4,8,64,512]{3,2,1,0:T(8,128)(2,1)}, bf16[1024,512]{1,0:T(8,128)(2,1)}, bf16[1024,512]{1,0:T(8,128)(2,1)}) custom-call(bf16[3,128,2048]{2,1,0:T(8,128)(2,1)} %copy-done, bf16[3,128,2048]{2,1,0:T(8,128)(2,1)} %copy-done.2, bf16[3,128,2048]{2,1,0:T(8,128)(2,1)} %copy-done.1, bf16[3,64,2048]{2,1,0:T(8,128)(2,1)} %copy-done.7, ...), custom_call_target="tpu_custom_call" | custom-call | flops 6442450944 | bytes 12582912 | tf_op jit(solution)/shard_map/pallas_call | solution.py:222
  104.8 3.6 %all-to-all-start.1 = ((bf16[4,8,64,512]{3,2,1,0:T(8,128)(2,1)}), bf16[4,8,64,512]{3,2,1,0:T(8,128)(2,1)S(1)}, u32[]{:S(2)}, u32[]{:S(2)}) async-start(bf16[4,8,64,512]{3,2,1,0:T(8,128)(2,1)} %get-tuple-element.16), calls=%async_computation.1 | async-start | bytes 4194304 | tf_op jit(solution)/shard_map/all_to_all | solution.py:60
  108.4 5.7 %shard_map.104 = (bf16[512,2048]{1,0:T(8,128)(2,1)}, bf16[512,2048]{1,0:T(8,128)(2,1)}) custom-call(bf16[1024,512]{1,0:T(8,128)(2,1)} %get-tuple-element.13.pg_in, bf16[2048,1024]{1,0:T(8,128)(2,1)} %all-gather.2.cloned.1.call-done.refs_10_.w), custom_call_target="tpu_custom_call" | custom-call | flops 2147483648 | bytes 12582912 | tf_op jit(solution)/shard_map/pallas_call | solution.py:222
  114.6 7.8 %shard_map.105 = bf16[2048,512]{1,0:T(8,128)(2,1)} custom-call(bf16[3,128,2048]{2,1,0:T(8,128)(2,1)} %copy-done, bf16[3,128,2048]{2,1,0:T(8,128)(2,1)} %copy-done.2, bf16[3,128,2048]{2,1,0:T(8,128)(2,1)} %copy-done.1, bf16[3,64,2048]{2,1,0:T(8,128)(2,1)} %copy-done.7, bf16[3,64,2048]{2,1,0:T(8,128)(2,1)} %copy-done.6, bf16[3,128,2048]{2,1,0:T(8,128)(2,1)} %copy-done.4, ...), custom_call_target="tpu_custom_call" | custom-call | flops 2147483648 | bytes 12582912 | tf_op jit(solution)/shard_map/pallas_call | solution.py:222
  122.5 13.0 %all-to-all-done.1 = bf16[4,8,64,512]{3,2,1,0:T(8,128)(2,1)S(1)} async-done(((bf16[4,8,64,512]{3,2,1,0:T(8,128)(2,1)}), bf16[4,8,64,512]{3,2,1,0:T(8,128)(2,1)S(1)}, u32[]{:S(2)}, u32[]{:S(2)}) %all-to-all-start.1) | async-done | bytes 2097184 | tf_op jit(solution)/shard_map/all_to_all | solution.py:60
  136.8 8.5 %all-to-all-start.2 = ((bf16[8,64,512]{2,1,0:T(8,128)(2,1)}), bf16[8,64,512]{2,1,0:T(8,128)(2,1)S(1)}, u32[]{:S(2)}, u32[]{:S(2)}) async-start(bf16[8,64,512]{2,1,0:T(8,128)(2,1)} %reduce_sum.21), calls=%async_computation.2 | async-start | bytes 1048576 | tf_op jit(solution)/shard_map/all_to_all | solution.py:60
  145.3 3.0 %add_convert_fusion.1 = bf16[512,2048]{1,0:T(8,128)(2,1)S(1)} fusion(bf16[512,2048]{1,0:T(8,128)(2,1)} %collective-permute-done.9, bf16[512,2048]{1,0:T(8,128)(2,1)} %get-tuple-element.11), kind=kLoop, calls=%fused_computation.1 | loop fusion | flops 4194304 | bytes 6291456 | tf_op jit(solution)/shard_map/convert_element_type | solution.py:37
  149.5 2.1 %collective-permute-start.12 = (bf16[64,2048]{1,0:T(8,128)(2,1)S(1)}, bf16[64,2048]{1,0:T(8,128)(2,1)S(1)}, u32[]{:S(2)}, u32[]{:S(2)}) collective-permute-start(bf16[64,2048]{1,0:T(8,128)(2,1)S(1)} %get-tuple-element.27), channel_id=1, source_target_pairs={{0,6},{2,0},{4,2},{6,4},{1,7},{3,1},{5,3},{7,5},{8,14},{10,8},{12,... | collective-permute-start | bytes 786440 | tf_op jit(solution)/shard_map/ppermute | solution.py:21
  151.6 2.4 %add_convert_fusion = bf16[512,2048]{1,0:T(8,128)(2,1)S(1)} fusion(bf16[512,2048]{1,0:T(8,128)(2,1)} %collective-permute-done.14, bf16[512,2048]{1,0:T(8,128)(2,1)S(1)} %copy-done.10), kind=kLoop, calls=%fused_computation | loop fusion | flops 4194304 | bytes 6291456 | tf_op jit(solution)/shard_map/convert_element_type | solution.py:37
  155.0 2.4 %collective-permute-start.17 = (bf16[64,2048]{1,0:T(8,128)(2,1)S(1)}, bf16[64,2048]{1,0:T(8,128)(2,1)S(1)}, u32[]{:S(2)}, u32[]{:S(2)}) collective-permute-start(bf16[64,2048]{1,0:T(8,128)(2,1)S(1)} %get-tuple-element.21), channel_id=1, source_target_pairs={{0,6},{2,0},{4,2},{6,4},{1,7},{3,1},{5,3},{7,5},{8,14},{10,8},{12,... | collective-permute-start | bytes 786440 | tf_op jit(solution)/shard_map/ppermute | solution.py:21
  159.7 1.8 collective-permute-start.13
  164.5 2.9 %collective-permute-start.18 = (bf16[128,2048]{1,0:T(8,128)(2,1)S(1)}, bf16[128,2048]{1,0:T(8,128)(2,1)}, u32[]{:S(2)}, u32[]{:S(2)}) collective-permute-start(bf16[128,2048]{1,0:T(8,128)(2,1)S(1)} %pad_maximum_fusion.4), channel_id=1, source_target_pairs={{0,6},{2,0},{4,2},{6,4},{1,7},{3,1},{5,3},{7,5},{8,14},{10,8},{12,... | collective-permute-start | bytes 1572872 | tf_op jit(solution)/shard_map/ppermute | solution.py:21
  169.1 6.6 %collective-permute-done.13 = bf16[128,2048]{1,0:T(8,128)(2,1)} collective-permute-done((bf16[128,2048]{1,0:T(8,128)(2,1)}, bf16[128,2048]{1,0:T(8,128)(2,1)}, u32[]{:S(2)}, u32[]{:S(2)}) %collective-permute-start.13) | collective-permute-done | bytes 524320 | tf_op jit(solution)/shard_map/ppermute | solution.py:21
  175.7 2.7 %collective-permute-done.11 = bf16[128,2048]{1,0:T(8,128)(2,1)} collective-permute-done((bf16[128,2048]{1,0:T(8,128)(2,1)}, bf16[128,2048]{1,0:T(8,128)(2,1)}, u32[]{:S(2)}, u32[]{:S(2)}) %collective-permute-start.11) | collective-permute-done | bytes 524320 | tf_op jit(solution)/shard_map/ppermute | solution.py:21
  178.4 2.4 %add_convert_fusion.3 = bf16[128,2048]{1,0:T(8,128)(2,1)} fusion(bf16[128,2048]{1,0:T(8,128)(2,1)} %collective-permute-done.13, bf16[128,2048]{1,0:T(8,128)(2,1)} %collective-permute-done.11, bf16[512,2048]{1,0:T(8,128)(2,1)} %copy-done.3), kind=kLoop, calls=%fused_computation.5 | loop fusion | flops 1572864 | bytes 2097152 | tf_op jit(solution)/shard_map/convert_element_type | solution.py:51
  182.3 2.7 %collective-permute-start.21 = (bf16[64,512]{1,0:T(8,128)(2,1)S(1)}, bf16[64,512]{1,0:T(8,128)(2,1)S(1)}, u32[]{:S(2)}, u32[]{:S(2)}) collective-permute-start(bf16[64,512]{1,0:T(8,128)(2,1)S(1)} %get-tuple-element.31), channel_id=1, source_target_pairs={{0,24},{8,0},{16,8},{24,16},{1,25},{9,1},{17,9},{25,17},{2,26},{10... | collective-permute-start | bytes 196616 | tf_op jit(solution)/shard_map/ppermute | solution.py:21
  186.5 2.2 %add_convert_fusion.2 = bf16[128,2048]{1,0:T(8,128)(2,1)} fusion(bf16[128,2048]{1,0:T(8,128)(2,1)} %collective-permute-done.18, bf16[128,2048]{1,0:T(8,128)(2,1)} %collective-permute-done.16, bf16[512,2048]{1,0:T(8,128)(2,1)S(1)} %add_convert_fusion), kind=kLoop, calls=%fused_computation.4 | loop fusion | flops 1572864 | bytes 2097152 | tf_op jit(solution)/shard_map/convert_element_type | solution.py:51
  188.7 2.1 %collective-permute-done.20 = bf16[64,512]{1,0:T(8,128)(2,1)S(1)} collective-permute-done((bf16[64,512]{1,0:T(8,128)(2,1)S(1)}, bf16[64,512]{1,0:T(8,128)(2,1)S(1)}, u32[]{:S(2)}, u32[]{:S(2)}) %collective-permute-start.20) | collective-permute-done | bytes 65568 | tf_op jit(solution)/shard_map/ppermute | solution.py:21
  (89 shorter events, 22.9 us)
Async XLA Ops:
  7.2 73.7 %all-gather.2.cloned.1.call-start = ((), (), s32[]{:S(2)}) async-start(), calls=%async_computation.4 | async-start | bytes 4718592 | tf_op jit(solution)/shard_map/all_gather | solution.py:271
  22.2 35.1 %collective-permute-start.1 = (bf16[3,128,2048]{2,1,0:T(8,128)(2,1)S(1)}, bf16[3,128,2048]{2,1,0:T(8,128)(2,1)S(1)}, u32[]{:S(2)}, u32[]{:S(2)}) collective-permute-start(bf16[3,128,2048]{2,1,0:T(8,128)(2,1)S(1)} %pad_maximum_fusion.refs_0_), channel_id=1, source_target_pairs={{0,6},{2,0},{4,2},{6,4},{1,7},{3,1},{5,3},{7,5},{8,14},{10,8},{12,... | collective-permute-start | bytes 4718600 | tf_op jit(solution)/shard_map/ppermute | solution.py:21
  22.7 36.0 %collective-permute-start = (bf16[3,128,2048]{2,1,0:T(8,128)(2,1)S(1)}, bf16[3,128,2048]{2,1,0:T(8,128)(2,1)S(1)}, u32[]{:S(2)}, u32[]{:S(2)}) collective-permute-start(bf16[3,128,2048]{2,1,0:T(8,128)(2,1)S(1)} %pad_maximum_fusion.refs_0_), channel_id=1, source_target_pairs={{0,2},{2,4},{4,6},{6,0},{1,3},{3,5},{5,7},{7,1},{8,10},{10,12},{12... | collective-permute-start | bytes 4718600 | tf_op jit(solution)/shard_map/ppermute | solution.py:21
  24.3 53.3 %collective-permute-start.4 = (bf16[3,128,2048]{2,1,0:T(8,128)(2,1)S(1)}, bf16[3,128,2048]{2,1,0:T(8,128)(2,1)S(1)}, u32[]{:S(2)}, u32[]{:S(2)}) collective-permute-start(bf16[3,128,2048]{2,1,0:T(8,128)(2,1)S(1)} %pad_maximum_fusion.refs_0_), channel_id=1, source_target_pairs={{0,1},{1,0},{2,3},{3,2},{4,5},{5,4},{6,7},{7,6},{8,9},{9,8},{10,11... | collective-permute-start | bytes 4718600 | tf_op jit(solution)/shard_map/ppermute | solution.py:21
  57.3 17.5 %collective-permute-start.3 = (bf16[3,64,2048]{2,1,0:T(8,128)(2,1)S(1)}, bf16[3,64,2048]{2,1,0:T(8,128)(2,1)S(1)}, u32[]{:S(2)}, u32[]{:S(2)}) collective-permute-start(bf16[3,64,2048]{2,1,0:T(8,128)(2,1)S(1)} %slice.83), channel_id=1, source_target_pairs={{0,6},{2,0},{4,2},{6,4},{1,7},{3,1},{5,3},{7,5},{8,14},{10,8},{12,... | collective-permute-start | bytes 2359304 | tf_op jit(solution)/shard_map/ppermute | solution.py:21
  58.8 18.8 %collective-permute-start.2 = (bf16[3,64,2048]{2,1,0:T(8,128)(2,1)S(1)}, bf16[3,64,2048]{2,1,0:T(8,128)(2,1)S(1)}, u32[]{:S(2)}, u32[]{:S(2)}) collective-permute-start(bf16[3,64,2048]{2,1,0:T(8,128)(2,1)S(1)} %slice.82), channel_id=1, source_target_pairs={{0,2},{2,4},{4,6},{6,0},{1,3},{3,5},{5,7},{7,1},{8,10},{10,12},{12... | collective-permute-start | bytes 2359304 | tf_op jit(solution)/shard_map/ppermute | solution.py:21
  59.6 18.1 %collective-permute-start.6 = (bf16[3,128,2048]{2,1,0:T(8,128)(2,1)S(1)}, bf16[3,128,2048]{2,1,0:T(8,128)(2,1)S(1)}, u32[]{:S(2)}, u32[]{:S(2)}) collective-permute-start(bf16[3,128,2048]{2,1,0:T(8,128)(2,1)S(1)} %collective-permute-done.1.refs_2_), channel_id=1, source_target_pairs={{0,1},{1,0},{2,3},{3,2},{4,5},{5,4},{6,7},{7,6},{8,9},{9,8},{10,11... | collective-permute-start | bytes 4718600 | tf_op jit(solution)/shard_map/ppermute | solution.py:21
  59.6 21.2 %collective-permute-start.5 = (bf16[3,128,2048]{2,1,0:T(8,128)(2,1)S(1)}, bf16[3,128,2048]{2,1,0:T(8,128)(2,1)}, u32[]{:S(2)}, u32[]{:S(2)}) collective-permute-start(bf16[3,128,2048]{2,1,0:T(8,128)(2,1)S(1)} %collective-permute-done.refs_1_), channel_id=1, source_target_pairs={{0,1},{1,0},{2,3},{3,2},{4,5},{5,4},{6,7},{7,6},{8,9},{9,8},{10,11... | collective-permute-start | bytes 4718600 | tf_op jit(solution)/shard_map/ppermute | solution.py:21
  90.0 55.3 %collective-permute-start.9 = (bf16[512,2048]{1,0:T(8,128)(2,1)}, bf16[512,2048]{1,0:T(8,128)(2,1)}, u32[]{:S(2)}, u32[]{:S(2)}) collective-permute-start(bf16[512,2048]{1,0:T(8,128)(2,1)} %get-tuple-element.12), channel_id=1, source_target_pairs={{0,1},{1,0},{2,3},{3,2},{4,5},{5,4},{6,7},{7,6},{8,9},{9,8},{10,11... | collective-permute-start | bytes 6291464 | tf_op jit(solution)/shard_map/ppermute | solution.py:21
  104.8 30.7 %all-to-all-start.1 = ((bf16[4,8,64,512]{3,2,1,0:T(8,128)(2,1)}), bf16[4,8,64,512]{3,2,1,0:T(8,128)(2,1)S(1)}, u32[]{:S(2)}, u32[]{:S(2)}) async-start(bf16[4,8,64,512]{3,2,1,0:T(8,128)(2,1)} %get-tuple-element.16), calls=%async_computation.1 | async-start | bytes 4194304 | tf_op jit(solution)/shard_map/all_to_all | solution.py:60
  108.4 72.4 %reduce-scatter.2.cloned.1.call-start = ((), (), s32[]{:S(2)}) async-start(), calls=%async_computation.5 | async-start | bytes 2359296 | tf_op jit(solution)/shard_map/reduce_scatter | solution.py:277
  114.2 37.4 %collective-permute-start.14 = (bf16[512,2048]{1,0:T(8,128)(2,1)}, bf16[512,2048]{1,0:T(8,128)(2,1)}, u32[]{:S(2)}, u32[]{:S(2)}) collective-permute-start(bf16[512,2048]{1,0:T(8,128)(2,1)} %get-tuple-element.15), channel_id=1, source_target_pairs={{0,1},{1,0},{2,3},{3,2},{4,5},{5,4},{6,7},{7,6},{8,9},{9,8},{10,11... | collective-permute-start | bytes 6291464 | tf_op jit(solution)/shard_map/ppermute | solution.py:21
  136.8 31.6 %all-to-all-start.2 = ((bf16[8,64,512]{2,1,0:T(8,128)(2,1)}), bf16[8,64,512]{2,1,0:T(8,128)(2,1)S(1)}, u32[]{:S(2)}, u32[]{:S(2)}) async-start(bf16[8,64,512]{2,1,0:T(8,128)(2,1)} %reduce_sum.21), calls=%async_computation.2 | async-start | bytes 1048576 | tf_op jit(solution)/shard_map/all_to_all | solution.py:60
  148.4 9.2 %collective-permute-start.10 = (bf16[64,2048]{1,0:T(8,128)(2,1)S(1)}, bf16[64,2048]{1,0:T(8,128)(2,1)S(1)}, u32[]{:S(2)}, u32[]{:S(2)}) collective-permute-start(bf16[64,2048]{1,0:T(8,128)(2,1)S(1)} %get-tuple-element.26), channel_id=1, source_target_pairs={{0,2},{2,4},{4,6},{6,0},{1,3},{3,5},{5,7},{7,1},{8,10},{10,12},{12... | collective-permute-start | bytes 786440 | tf_op jit(solution)/shard_map/ppermute | solution.py:21
  149.5 9.3 %collective-permute-start.12 = (bf16[64,2048]{1,0:T(8,128)(2,1)S(1)}, bf16[64,2048]{1,0:T(8,128)(2,1)S(1)}, u32[]{:S(2)}, u32[]{:S(2)}) collective-permute-start(bf16[64,2048]{1,0:T(8,128)(2,1)S(1)} %get-tuple-element.27), channel_id=1, source_target_pairs={{0,6},{2,0},{4,2},{6,4},{1,7},{3,1},{5,3},{7,5},{8,14},{10,8},{12,... | collective-permute-start | bytes 786440 | tf_op jit(solution)/shard_map/ppermute | solution.py:21
  154.1 8.8 %collective-permute-start.15 = (bf16[64,2048]{1,0:T(8,128)(2,1)S(1)}, bf16[64,2048]{1,0:T(8,128)(2,1)S(1)}, u32[]{:S(2)}, u32[]{:S(2)}) collective-permute-start(bf16[64,2048]{1,0:T(8,128)(2,1)S(1)} %get-tuple-element.20), channel_id=1, source_target_pairs={{0,2},{2,4},{4,6},{6,0},{1,3},{3,5},{5,7},{7,1},{8,10},{10,12},{12... | collective-permute-start | bytes 786440 | tf_op jit(solution)/shard_map/ppermute | solution.py:21
  155.0 9.4 %collective-permute-start.17 = (bf16[64,2048]{1,0:T(8,128)(2,1)S(1)}, bf16[64,2048]{1,0:T(8,128)(2,1)S(1)}, u32[]{:S(2)}, u32[]{:S(2)}) collective-permute-start(bf16[64,2048]{1,0:T(8,128)(2,1)S(1)} %get-tuple-element.21), channel_id=1, source_target_pairs={{0,6},{2,0},{4,2},{6,4},{1,7},{3,1},{5,3},{7,5},{8,14},{10,8},{12,... | collective-permute-start | bytes 786440 | tf_op jit(solution)/shard_map/ppermute | solution.py:21
  159.7 16.0 %collective-permute-start.13 = (bf16[128,2048]{1,0:T(8,128)(2,1)}, bf16[128,2048]{1,0:T(8,128)(2,1)}, u32[]{:S(2)}, u32[]{:S(2)}) collective-permute-start(bf16[128,2048]{1,0:T(8,128)(2,1)} %pad_maximum_fusion.2), channel_id=1, source_target_pairs={{0,6},{2,0},{4,2},{6,4},{1,7},{3,1},{5,3},{7,5},{8,14},{10,8},{12,... | collective-permute-start | bytes 1572872 | tf_op jit(solution)/shard_map/ppermute | solution.py:21
  162.4 16.0 %collective-permute-start.11 = (bf16[128,2048]{1,0:T(8,128)(2,1)}, bf16[128,2048]{1,0:T(8,128)(2,1)}, u32[]{:S(2)}, u32[]{:S(2)}) collective-permute-start(bf16[128,2048]{1,0:T(8,128)(2,1)} %pad_maximum_fusion.1), channel_id=1, source_target_pairs={{0,2},{2,4},{4,6},{6,0},{1,3},{3,5},{5,7},{7,1},{8,10},{10,12},{12... | collective-permute-start | bytes 1572872 | tf_op jit(solution)/shard_map/ppermute | solution.py:21
  164.5 21.5 %collective-permute-start.18 = (bf16[128,2048]{1,0:T(8,128)(2,1)S(1)}, bf16[128,2048]{1,0:T(8,128)(2,1)}, u32[]{:S(2)}, u32[]{:S(2)}) collective-permute-start(bf16[128,2048]{1,0:T(8,128)(2,1)S(1)} %pad_maximum_fusion.4), channel_id=1, source_target_pairs={{0,6},{2,0},{4,2},{6,4},{1,7},{3,1},{5,3},{7,5},{8,14},{10,8},{12,... | collective-permute-start | bytes 1572872 | tf_op jit(solution)/shard_map/ppermute | solution.py:21
  168.3 18.2 %collective-permute-start.16 = (bf16[128,2048]{1,0:T(8,128)(2,1)}, bf16[128,2048]{1,0:T(8,128)(2,1)}, u32[]{:S(2)}, u32[]{:S(2)}) collective-permute-start(bf16[128,2048]{1,0:T(8,128)(2,1)} %pad_maximum_fusion.3), channel_id=1, source_target_pairs={{0,2},{2,4},{4,6},{6,0},{1,3},{3,5},{5,7},{7,1},{8,10},{10,12},{12... | collective-permute-start | bytes 1572872 | tf_op jit(solution)/shard_map/ppermute | solution.py:21
  181.7 7.0 %collective-permute-start.19 = (bf16[64,512]{1,0:T(8,128)(2,1)S(1)}, bf16[64,512]{1,0:T(8,128)(2,1)S(1)}, u32[]{:S(2)}, u32[]{:S(2)}) collective-permute-start(bf16[64,512]{1,0:T(8,128)(2,1)S(1)} %get-tuple-element.30), channel_id=1, source_target_pairs={{0,8},{8,16},{16,24},{24,0},{1,9},{9,17},{17,25},{25,1},{2,10},{10... | collective-permute-start | bytes 196616 | tf_op jit(solution)/shard_map/ppermute | solution.py:21
  182.3 6.4 %collective-permute-start.21 = (bf16[64,512]{1,0:T(8,128)(2,1)S(1)}, bf16[64,512]{1,0:T(8,128)(2,1)S(1)}, u32[]{:S(2)}, u32[]{:S(2)}) collective-permute-start(bf16[64,512]{1,0:T(8,128)(2,1)S(1)} %get-tuple-element.31), channel_id=1, source_target_pairs={{0,24},{8,0},{16,8},{24,16},{1,25},{9,1},{17,9},{25,17},{2,26},{10... | collective-permute-start | bytes 196616 | tf_op jit(solution)/shard_map/ppermute | solution.py:21
  185.0 5.8 %collective-permute-start.20 = (bf16[64,512]{1,0:T(8,128)(2,1)S(1)}, bf16[64,512]{1,0:T(8,128)(2,1)S(1)}, u32[]{:S(2)}, u32[]{:S(2)}) collective-permute-start(bf16[64,512]{1,0:T(8,128)(2,1)S(1)} %get-tuple-element.32), channel_id=1, source_target_pairs={{0,16},{8,24},{16,0},{24,8},{1,17},{9,25},{17,1},{25,9},{2,18},{10... | collective-permute-start | bytes 196616 | tf_op jit(solution)/shard_map/ppermute | solution.py:21
  (18 other events, 207.4 us)
Sparse Core Ops, SparseCore 0:
  22.1 55.7 all-gather.1
  122.6 55.1 reduce-scatter.1

commit v5 on v4

v5 whole, which is shorter than its diff:
```python
import math

import jax
import jax.numpy as jnp
from jax import lax
from jax.experimental import pallas as pl
from jax.experimental.pallas import tpu as pltpu
from jax.sharding import Mesh
from jax.sharding import PartitionSpec as P


FS = ("z", "x")
ALL = ("z", "x", "y", "c")
F32 = jnp.float32
BF16 = jnp.bfloat16
TILE = 512


def shift(x, axis, by):
    n = lax.axis_size(axis)
    return lax.ppermute(x, axis, [(i, (i + by) % n) for i in range(n)])


def gather_tokens(arrays):
    own = jnp.stack(arrays)
    half = own.shape[1] // 2
    behind, ahead = shift(own, "y", 1), shift(own, "y", -1)
    far_lo, far_hi = shift(behind[:, :half], "y", 1), shift(ahead[:, half:], "y", -1)
    pieces = (own, behind, ahead, far_lo, far_hi)
    partners = []
    for piece in pieces:
        partners.append(shift(piece, "c", 1))
    return (*pieces, *partners)


def gather_later(own):
    behind, ahead, far = (shift(own, "y", by) for by in (1, -1, 2))
    mine = jnp.concatenate((own, behind, ahead, far), axis=0)[None]
    return mine, shift(mine, "c", 1)


def plus(a, b):
    return (a.astype(F32) + b.astype(F32)).astype(BF16)


def scatter_tokens(mine, partners):
    partners = shift(partners, "c", 1)
    rows = mine.shape[0] // 4
    at = [slice(i * rows, (i + 1) * rows) for i in range(4)]
    behind, ahead, far = (plus(mine[i], partners[i]) for i in at[1:])
    arrived = (shift(ahead, "y", 1), shift(behind, "y", -1), shift(far, "y", 2))
    total = mine[at[0]].astype(F32) + partners[at[0]].astype(F32)
    return sum((a.astype(F32) for a in arrived), total).astype(BF16)


def gather(x, axis):
    n = lax.axis_size(axis)
    return lax.all_to_all(jnp.broadcast_to(x[None], (n, *x.shape)), axis, 0, 0, tiled=True)


def exchange_sum(term, axis):
    tiles = lax.all_to_all(term, axis, 0, 0, tiled=True)
    return jnp.sum(tiles.astype(F32), axis=0)


def hop_sum(term, axis):
    n = lax.axis_size(axis)
    me = lax.axis_index(axis)

    def block(by):
        at = (me + by) & (n - 1)
        start = (at, *(0 for _ in term.shape[1:]))
        part = lax.dynamic_slice(term, start, (1, *term.shape[1:]), allow_negative_indices=False)
        return part[0]

    arrived = [shift(block(by), axis, by) for by in range(1, n)]
    return sum((a.astype(F32) for a in arrived), block(0).astype(F32))


def rows_times(left, right):
    return lax.dot_general(left, right, (((1,), (1,)), ((), ())), preferred_element_type=F32)


def over_tokens(left, right):
    return lax.dot_general(left, right, (((0,), (0,)), ((), ())), preferred_element_type=F32)


def copies(sources, target, sems, index):
    waits, row = [], 0
    for i, source in enumerate(sources):
        rows = source.shape[1]
        copy = pltpu.make_async_copy(source.at[index], target.at[pl.ds(row, rows)], sems.at[i])
        copy.start()
        waits.append((row, copy))
        row += rows
    return waits


def settle(waits, upto):
    while waits and waits[0][0] < upto:
        waits.pop(0)[1].wait()


def relu_times(rows, weight):
    return jnp.maximum(jnp.dot(rows, weight, preferred_element_type=F32), 0.0)


def pre_kernel(*refs):
    pieces, (w, down_out, relu_out) = refs[:10], refs[10:13]
    saved, cot, up, relu, hid, dt, in_sems, sems = refs[13:]
    up_copy = pltpu.make_async_copy(w, up, sems.at[0])
    up_copy.start()
    saved_waits = copies(pieces, saved, in_sems.at[0], 0)
    cot_waits = copies(pieces, cot, in_sems.at[1], 1)
    up_copy.wait()
    for t in range(0, saved.shape[0], TILE):
        settle(saved_waits, t + TILE)
        at = pl.ds(t, TILE)
        r = relu_times(saved[at], up[...])
        relu[at] = r
        hid[at] = (r * r).astype(BF16)
    settle(cot_waits, cot.shape[0])
    relu_copy = pltpu.make_async_copy(relu, relu_out, sems.at[1])
    block = dt.shape[0] // 8

    @pl.loop(0, 8)
    def _(i):
        at = pl.ds(pl.multiple_of(i * block, block), block)
        dt[at] = over_tokens(cot[:, at], hid[...]).astype(BF16)

    relu_copy.start()
    out_copy = pltpu.make_async_copy(dt, down_out, sems.at[2])
    out_copy.start()
    relu_copy.wait()
    out_copy.wait()


def place_down(parts, down, sems):
    n = len(parts)
    waits = []
    for k, part in enumerate(parts):
        at = (lax.axis_index("x") + (n - k)) & (n - 1)
        copy = pltpu.make_async_copy(part, down.at[:, at], sems.at[k])
        copy.start()
        waits.append(copy)
    return waits


def up_kernel(*refs):
    pieces, parts, (relu_in, up_out, pg_out) = refs[:10], refs[10:14], refs[14:17]
    saved, cot, down, relu, pg, ut, in_sems, w_sems, sems = refs[17:]
    down_waits = place_down(parts, down, w_sems)
    cot_waits = copies(pieces, cot, in_sems.at[1], 1)
    relu_copy = pltpu.make_async_copy(relu_in, relu, sems.at[0])
    relu_copy.start()
    saved_waits = copies(pieces, saved, in_sems.at[0], 0)
    for copy in down_waits:
        copy.wait()
    weight = down[...].reshape(-1, down.shape[-1])
    for t in range(0, cot.shape[0], TILE):
        settle(cot_waits, t + TILE)
        at = pl.ds(t, TILE)
        grad = jnp.dot(cot[at], weight, preferred_element_type=F32)
        if t == 0:
            relu_copy.wait()
        pg[at] = (2.0 * relu[at] * grad).astype(BF16)
    settle(saved_waits, saved.shape[0])
    nx, nz, part = ut.shape[:3]

    @pl.loop(0, nz)
    def _(i):
        at = pl.ds(pl.multiple_of(i * nx * part, nx * part), nx * part)
        term = over_tokens(saved[:, at], pg[...]).astype(BF16)
        for j in range(nx):
            ut[j, i] = term[j * part : (j + 1) * part]

    pg_copy = pltpu.make_async_copy(pg, pg_out, sems.at[1])
    pg_copy.start()
    ut_copy = pltpu.make_async_copy(ut, up_out, sems.at[2])
    ut_copy.start()
    pg_copy.wait()
    ut_copy.wait()


def rows_kernel(pg_in, w, mine_out, theirs_out, pg, up, mine, theirs, sems):
    pg_copy = pltpu.make_async_copy(pg_in, pg, sems.at[0])
    up_copy = pltpu.make_async_copy(w, up, sems.at[1])
    pg_copy.start()
    up_copy.start()
    pg_copy.wait()
    up_copy.wait()
    first = pltpu.make_async_copy(mine, mine_out, sems.at[2])
    second = pltpu.make_async_copy(theirs, theirs_out, sems.at[3])
    outputs(pg, mine.shape[0], up, theirs)
    outputs(pg, 0, up, mine)
    second.start()
    first.start()
    first.wait()
    second.wait()


def flat_rows(weight, first, count):
    each = weight.shape[1] * weight.shape[2]
    return weight[first // each : (first + count) // each].reshape(count, weight.shape[-1])


def outputs(hidden, first, weight, out):
    @pl.loop(0, out.shape[0], step=TILE)
    def _(t):
        rows = hidden[pl.ds(pl.multiple_of(first + t, TILE), TILE)]
        for n in range(0, out.shape[1], 512):
            block = weight[n : n + 512] if len(weight.shape) == 2 else flat_rows(weight, n, 512)
            part = rows_times(rows, block)
            out[pl.ds(pl.multiple_of(t, TILE), TILE), n : n + 512] = part.astype(BF16)


def ahead_kernel(*refs):
    pieces, parts, (w, mine_out, theirs_out) = refs[:2], refs[2:6], refs[6:9]
    rows, up, down, hid, mine, theirs, in_sems, w_sems, sems = refs[9:]
    up_copy = pltpu.make_async_copy(w, up, sems.at[0])
    up_copy.start()
    waits = copies(pieces, rows, in_sems, 0)
    down_waits = place_down(parts, down, w_sems)
    up_copy.wait()
    for t in range(0, rows.shape[0], TILE):
        settle(waits, t + TILE)
        at = pl.ds(t, TILE)
        r = relu_times(rows[at], up[...])
        hid[at] = (r * r).astype(BF16)
    for copy in down_waits:
        copy.wait()
    first = pltpu.make_async_copy(mine, mine_out, sems.at[1])
    second = pltpu.make_async_copy(theirs, theirs_out, sems.at[2])
    outputs(hid, mine.shape[0], down, theirs)
    outputs(hid, 0, down, mine)
    second.start()
    first.start()
    first.wait()
    second.wait()


def call(kernel, operands, outs, scratch, flops):
    hbm = pl.BlockSpec(memory_space=pltpu.HBM)
    return pl.pallas_call(
        kernel,
        out_shape=[jax.ShapeDtypeStruct(*s) for s in outs],
        in_specs=[hbm] * len(operands),
        out_specs=[hbm] * len(outs),
        scratch_shapes=[pltpu.VMEM(*s) for s in scratch[0]]
        + [pltpu.SemaphoreType.DMA(s) for s in scratch[1]],
        cost_estimate=pl.CostEstimate(flops=flops, bytes_accessed=12 << 20, transcendentals=0),
        compiler_params=pltpu.CompilerParams(vmem_limit_bytes=60 * 1024 * 1024),
    )(*operands)


def products(pieces, later, up, down, nz, nx):
    rows = sum(p.shape[1] for p in pieces)
    depth, cols = up.shape
    n = len(pieces)
    flops = 2 * rows * depth * cols
    group, weight, wide = ((rows, depth), BF16), ((depth, cols), BF16), ((rows, cols), BF16)
    relu = (wide[0], F32)
    part = depth // (nx * nz)
    split, up_shape = ((nz, nx, part, cols), BF16), ((nx, nz, part, cols), BF16)
    half = ((rows // 2, depth), BF16)

    def pre():
        scratch = (group, group, weight, relu, wide, weight), ((2, n), (3,))
        return call(pre_kernel, (*pieces, up), (weight, relu), scratch, 2 * flops)

    def up_term(relu_part):
        scratch = (group, group, split, relu, wide, up_shape), ((2, n), (nx,), (3,))
        operands = (*pieces, *down, relu_part)
        return call(up_kernel, operands, (up_shape, wide), scratch, 2 * flops)

    def row_grad(pre_grad):
        scratch = (wide, weight, half, half), ((4,),)
        return call(rows_kernel, (pre_grad, up), (half, half), scratch, flops)

    def ahead():
        scratch = (group, weight, split, wide, half, half), ((2,), (nx,), (3,))
        operands = (*later, *down, up)
        return call(ahead_kernel, operands, (half, half), scratch, 2 * flops)

    return pre, up_term, row_grad, ahead


def body(later_rows, earlier_rows, cotangent, up_weight, down_weight, up_total, down_total):
    n_dev = math.prod(lax.axis_size(a) for a in ALL)
    nz, nx = lax.axis_size("z"), lax.axis_size("x")
    factor = 1.0 / math.sqrt(later_rows.shape[0] * n_dev)
    up = gather(up_weight, "x").reshape(-1, up_weight.shape[1])
    up = lax.all_gather(up, "z", axis=0, tiled=True)
    down = gather(down_weight, "z")
    down = (down, *(shift(down, "x", by) for by in range(1, nx)))
    pieces = gather_tokens((earlier_rows, cotangent))
    later = gather_later(later_rows)
    pre, grad_up, grad_rows, ahead = products(pieces, later, up, down, nz, nx)
    down_term, relu = pre()
    down_term = lax.psum_scatter(down_term, "z", scatter_dimension=0, tiled=True)
    up_term, pre_grad = grad_up(relu)
    up_term = exchange_sum(up_term, "x").astype(BF16)
    up_term = exchange_sum(up_term, "z")
    mine, theirs = grad_rows(pre_grad)
    earlier_grad = scatter_tokens(mine, theirs)
    mine, theirs = ahead()
    later_out = scatter_tokens(mine, theirs)
    down_term = hop_sum(down_term.reshape(-1, *down_weight.shape), "x")
    up_updated = up_total + up_term * factor
    down_updated = down_total + down_term * factor
    return later_out, earlier_grad, up_updated, down_updated


def solution(mesh):
    n_tp = mesh.shape["tp"]
    finer = Mesh(mesh.devices.reshape(8, 4, n_tp // 2, 2), ALL)
    rows, weight = P(ALL, None), P(FS, ("y", "c"))
    return jax.shard_map(
        body,
        mesh=finer,
        in_specs=(rows, rows, rows, weight, weight, weight, weight),
        out_specs=(rows, rows, weight, weight),
        check_vma=False,
    )
```

time: 202 us -> 239 us (1.18)
  waiting for transfers between devices: 82.1 us -> 100 us
  starting transfers between devices: 32.3 us -> 48.7 us
  local copies, waits for them, and re-layouts: 2.2 us -> 6.81 us
  blocking collectives: 13.7 us -> 10.9 us
    all_to_all x2, waiting for transfers between devices: 13.1 us -> 29.6 us  [exchange_sum(): tiles = lax.all_to_all(term, axis, 0, 0, tiled=True)]
    all_to_all x0 -> x1, starting transfers between devices: none -> 8.47 us  [gather(): lax.all_to_all(jnp.broadcast_to(x[None], (n, *x.shape)), axis, 0, 0, tile...]
    ppermute x22 -> x27, starting transfers between devices: 20.1 us -> 27.8 us  [shift(): return lax.ppermute(x, axis, [(i, (i + by) % n) for i in range(n)])]
    concatenate x5 -> x0, other arithmetic: 3.52 us -> none  [the longest x2 1.67 us: scatter_tokens(): jnp.concatenate([plus(ahead[:half], from_behind), ahead[half:]], axis=0)]
    all_to_all x1, blocking collectives: 13.7 us -> 10.9 us  [gather(): lax.all_to_all(jnp.broadcast_to(x[None], (n, *x.shape)), axis, 0, 0, tile...]
    ppermute x22 -> x27, waiting for transfers between devices: 69 us -> 70.7 us  [shift(): return lax.ppermute(x, axis, [(i, (i + by) % n) for i in range(n)])]
    convert_element_type x4 -> x2, other arithmetic: 5.64 us -> 6.41 us  [plus(): return (a.astype(F32) + b.astype(F32)).astype(BF16)]
  transfers between devices with their start and end apart: 26 -> 32, of which waited for: 16 -> 14; matrix products, arithmetic and copies ran while one was open for 8% -> 9% of each run, Pallas kernels for 14% -> 16%
where the time goes in v5:
time: 239 us; the launch traced here: 238 us
  waiting for transfers between devices  100 us (42%)
  starting transfers between devices  48.7 us (20%)
  Pallas kernels  38.6 us (16%)
  other arithmetic  18.4 us (8%)
  between operations  14.2 us (6%)
  blocking collectives  10.9 us (5%)
  local copies, waits for them, and re-layouts  6.81 us (3%)
    ppermute x27, waiting for transfers between devices, shift(): return lax.ppermute(x, axis, [(i, (i + by) % n) for i in range(n)])  70.7 us
    pallas_call x4, Pallas kernels, call(): pl.pallas_call(kernel, out_shape=[jax.ShapeDtypeStruct(*s) for s in outs]...  38.6 us
    all_to_all x2, waiting for transfers between devices, exchange_sum(): tiles = lax.all_to_all(term, axis, 0, 0, tiled=True)  29.6 us
    ppermute x27, starting transfers between devices, shift(): return lax.ppermute(x, axis, [(i, (i + by) % n) for i in range(n)])  27.8 us
    all_to_all x2, starting transfers between devices, exchange_sum(): tiles = lax.all_to_all(term, axis, 0, 0, tiled=True)  12.3 us
    all_to_all x1, blocking collectives, gather(): lax.all_to_all(jnp.broadcast_to(x[None], (n, *x.shape)), axis, 0, 0, tile...  10.9 us
    all_to_all x1, starting transfers between devices, gather(): lax.all_to_all(jnp.broadcast_to(x[None], (n, *x.shape)), axis, 0, 0, tile...  8.47 us
    convert_element_type x2, other arithmetic, plus(): return (a.astype(F32) + b.astype(F32)).astype(BF16)  6.41 us
  transfers between devices with their start and end apart: 32, of which 14 were waited for; matrix products, arithmetic and copies ran while one was open for 9% of the time, Pallas kernels for 16%

profile of v5, /device:TPU:8, one launch (start us, length us, event | category | flops | bytes accessed | tf_op | source)
XLA Modules:
  0.0 237.8 jit_solution(11535738314908361636)
XLA Ops:
  8.1 10.9 %all_to_all.20 = bf16[4,64,512]{2,1,0:T(8,128)(2,1)} all-to-all(bf16[4,64,512]{2,1,0:T(8,128)(2,1)S(1)} %broadcast_in_dim.8), channel_id=1, replica_groups=mesh['z'=8,'x'=4,'y'=4,'c'=2] {'x'}, dimensions={0} | all-to-all | bytes 524288 | tf_op jit(solution)/shard_map/all_to_all | solution.py:58
  24.8 21.7 %collective-permute-done.11.refs_1_ = bf16[2,128,2048]{2,1,0:T(8,128)(2,1)S(1)} collective-permute-done((bf16[2,128,2048]{2,1,0:T(8,128)(2,1)S(1)}, bf16[2,128,2048]{2,1,0:T(8,128)(2,1)S(1)}, u32[]{:S(2)}, u32[]{:S(2)}) %collective-permute-start.11) | collective-permute-done | bytes 1048608 | tf_op jit(solution)/shard_map/ppermute | solution.py:21
  47.5 2.3 collective-permute-start.2
  50.7 8.5 %all-to-all-start = ((bf16[8,64,512]{2,1,0:T(8,128)(2,1)}), bf16[8,64,512]{2,1,0:T(8,128)(2,1)}, u32[]{:S(2)}, u32[]{:S(2)}) async-start(bf16[8,64,512]{2,1,0:T(8,128)(2,1)} %broadcast_in_dim.7), calls=%async_computation | async-start | bytes 1048576 | tf_op jit(solution)/shard_map/all_to_all | solution.py:58
  63.7 7.6 %collective-permute-done.2 = bf16[128,2048]{1,0:T(8,128)(2,1)S(1)} collective-permute-done((bf16[128,2048]{1,0:T(8,128)(2,1)S(1)}, bf16[128,2048]{1,0:T(8,128)(2,1)S(1)}, u32[]{:S(2)}, u32[]{:S(2)}) %collective-permute-start.2) | collective-permute-done | bytes 524320 | tf_op jit(solution)/shard_map/ppermute | solution.py:21
  74.4 3.4 %collective-permute-done.13.refs_3_ = bf16[2,64,2048]{2,1,0:T(8,128)(2,1)} collective-permute-done((bf16[2,64,2048]{2,1,0:T(8,128)(2,1)S(1)}, bf16[2,64,2048]{2,1,0:T(8,128)(2,1)}, u32[]{:S(2)}, u32[]{:S(2)}) %collective-permute-start.13) | collective-permute-done | bytes 524320 | tf_op jit(solution)/shard_map/ppermute | solution.py:21
  83.1 2.0 collective-permute-start.6
  85.1 12.1 %shard_map.103 = (bf16[2048,512]{1,0:T(8,128)(2,1)}, f32[1024,512]{1,0:T(8,128)}) custom-call(bf16[2,128,2048]{2,1,0:T(8,128)(2,1)} %copy-done.2, bf16[2,128,2048]{2,1,0:T(8,128)(2,1)} %copy-done.7, bf16[2,128,2048]{2,1,0:T(8,128)(2,1)} %collective-permute-done.12.refs_2_, bf16[2,64,2048]{2,1,0:T(8,128)(2,1)} %collective-permute-done.13.refs_3_, ...), custom_call_target="tpu_custom_call" | custom-call | flops 4294967296 | bytes 12582912 | tf_op jit(solution)/shard_map/pallas_call | solution.py:244
  97.3 9.3 %collective-permute-done.4.refs_3_.refs_11_ = bf16[8,64,512]{2,1,0:T(8,128)(2,1)S(1)} collective-permute-done((bf16[8,64,512]{2,1,0:T(8,128)(2,1)}, bf16[8,64,512]{2,1,0:T(8,128)(2,1)S(1)}, u32[]{:S(2)}, u32[]{:S(2)}) %collective-permute-start.4) | collective-permute-done | bytes 524320 | tf_op jit(solution)/shard_map/ppermute | solution.py:21
  107.3 12.3 %shard_map.104 = (bf16[4,8,64,512]{3,2,1,0:T(8,128)(2,1)}, bf16[1024,512]{1,0:T(8,128)(2,1)}) custom-call(bf16[2,128,2048]{2,1,0:T(8,128)(2,1)} %copy-done.2, bf16[2,128,2048]{2,1,0:T(8,128)(2,1)} %copy-done.7, bf16[2,128,2048]{2,1,0:T(8,128)(2,1)} %collective-permute-done.12.refs_2_, bf16[2,64,2048]{2,1,0:T(8,128)(2,1)} %collective-permute-done.13.refs_3_, ...), custom_call_target="tpu_custom_call" | custom-call | flops 4294967296 | bytes 12582912 | tf_op jit(solution)/shard_map/pallas_call | solution.py:244
  119.6 5.7 %shard_map.105 = (bf16[512,2048]{1,0:T(8,128)(2,1)}, bf16[512,2048]{1,0:T(8,128)(2,1)}) custom-call(bf16[1024,512]{1,0:T(8,128)(2,1)} %get-tuple-element.15.pg_in, bf16[2048,512]{1,0:T(8,128)(2,1)} %all-gather.2.cloned.1.call-done.refs_6_.refs_10_.w), custom_call_target="tpu_custom_call" | custom-call | flops 2147483648 | bytes 12582912 | tf_op jit(solution)/shard_map/pallas_call | solution.py:244
  125.4 8.5 %shard_map.102 = (bf16[512,2048]{1,0:T(8,128)(2,1)}, bf16[512,2048]{1,0:T(8,128)(2,1)}) custom-call(bf16[1,512,2048]{2,1,0:T(8,128)(2,1)} %copy-done, bf16[1,512,2048]{2,1,0:T(8,128)(2,1)} %collective-permute-done.3.refs_1_, bf16[8,64,512]{2,1,0:T(8,128)(2,1)} %all-to-all-done.refs_2_.refs_10_, bf16[8,64,512]{2,1,0:T(8,128)(2,1)} %copy-done.11, ...), custom_call_target="tpu_custom_call" | custom-call | flops 4294967296 | bytes 12582912 | tf_op jit(solution)/shard_map/pallas_call | solution.py:244
  134.5 4.0 %all-to-all-start.2 = ((bf16[4,8,64,512]{3,2,1,0:T(8,128)(2,1)}), bf16[4,8,64,512]{3,2,1,0:T(8,128)(2,1)S(1)}, u32[]{:S(2)}, u32[]{:S(2)}) async-start(bf16[4,8,64,512]{3,2,1,0:T(8,128)(2,1)} %get-tuple-element.18), calls=%async_computation.2 | async-start | bytes 4194304 | tf_op jit(solution)/shard_map/all_to_all | solution.py:62
  138.6 26.5 %all-to-all-done.2 = bf16[4,8,64,512]{3,2,1,0:T(8,128)(2,1)S(1)} async-done(((bf16[4,8,64,512]{3,2,1,0:T(8,128)(2,1)}), bf16[4,8,64,512]{3,2,1,0:T(8,128)(2,1)S(1)}, u32[]{:S(2)}, u32[]{:S(2)}) %all-to-all-start.2) | async-done | bytes 2097184 | tf_op jit(solution)/shard_map/all_to_all | solution.py:62
  166.4 8.3 %all-to-all-start.3 = ((bf16[8,64,512]{2,1,0:T(8,128)(2,1)}), bf16[8,64,512]{2,1,0:T(8,128)(2,1)S(1)}, u32[]{:S(2)}, u32[]{:S(2)}) async-start(bf16[8,64,512]{2,1,0:T(8,128)(2,1)} %reduce_sum.21), calls=%async_computation.3 | async-start | bytes 1048576 | tf_op jit(solution)/shard_map/all_to_all | solution.py:62
  174.7 3.5 %add_convert_fusion.3 = (bf16[128,2048]{1,0:T(8,128)(2,1)}, bf16[128,2048]{1,0:T(8,128)(2,1)}, bf16[128,2048]{1,0:T(8,128)(2,1)}) fusion(bf16[512,2048]{1,0:T(8,128)(2,1)} %collective-permute-done.20, bf16[512,2048]{1,0:T(8,128)(2,1)} %get-tuple-element.16), kind=kLoop, calls=%fused_computation.6 | loop fusion | flops 3145728 | bytes 4718592 | tf_op jit(solution)/shard_map/convert_element_type | solution.py:43
  180.2 2.3 collective-permute-start.23
  182.4 3.0 %add_convert_fusion.7 = (bf16[128,2048]{1,0:T(8,128)(2,1)}, bf16[128,2048]{1,0:T(8,128)(2,1)}, bf16[128,2048]{1,0:T(8,128)(2,1)S(1)}) fusion(bf16[512,2048]{1,0:T(8,128)(2,1)} %collective-permute-done.7, bf16[512,2048]{1,0:T(8,128)(2,1)S(1)} %copy-done.1), kind=kLoop, calls=%fused_computation.10 | loop fusion | flops 3145728 | bytes 4718592 | tf_op jit(solution)/shard_map/convert_element_type | solution.py:43
  188.2 3.0 %all-to-all-done.3 = bf16[8,64,512]{2,1,0:T(8,128)(2,1)S(1)} async-done(((bf16[8,64,512]{2,1,0:T(8,128)(2,1)}), bf16[8,64,512]{2,1,0:T(8,128)(2,1)S(1)}, u32[]{:S(2)}, u32[]{:S(2)}) %all-to-all-start.3) | async-done | bytes 524320 | tf_op jit(solution)/shard_map/all_to_all | solution.py:62
  192.0 22.3 %collective-permute-done.21 = bf16[128,2048]{1,0:T(8,128)(2,1)} collective-permute-done((bf16[128,2048]{1,0:T(8,128)(2,1)}, bf16[128,2048]{1,0:T(8,128)(2,1)}, u32[]{:S(2)}, u32[]{:S(2)}) %collective-permute-start.21) | collective-permute-done | bytes 524320 | tf_op jit(solution)/shard_map/ppermute | solution.py:21
  214.3 4.2 %collective-permute-start.9 = (bf16[128,2048]{1,0:T(8,128)(2,1)S(1)}, bf16[128,2048]{1,0:T(8,128)(2,1)S(1)}, u32[]{:S(2)}, u32[]{:S(2)}) collective-permute-start(bf16[128,2048]{1,0:T(8,128)(2,1)S(1)} %get-tuple-element.25), channel_id=1, source_target_pairs={{0,6},{2,0},{4,2},{6,4},{1,7},{3,1},{5,3},{7,5},{8,14},{10,8},{12,... | collective-permute-start | bytes 1572872 | tf_op jit(solution)/shard_map/ppermute | solution.py:21
  218.5 2.9 %add_convert_fusion = bf16[128,2048]{1,0:T(8,128)(2,1)} fusion(bf16[128,2048]{1,0:T(8,128)(2,1)} %collective-permute-done.23, bf16[128,2048]{1,0:T(8,128)(2,1)} %collective-permute-done.22, bf16[128,2048]{1,0:T(8,128)(2,1)} %collective-permute-done.21, bf16[512,2048]{1,0:T(8,128)(2,1)} %collective-permute-done.20, bf16[512,2048]{1,0:T(8,128)(2,1)} %get-tuple-element.16), kind=kLoop, calls=%fused_computation.3 | loop fusion | flops 2621440 | bytes 3145728 | tf_op jit(solution)/shard_map/convert_element_type | solution.py:53
  223.0 2.1 collective-permute-start.25
  225.8 2.6 %add_convert_fusion.4 = bf16[128,2048]{1,0:T(8,128)(2,1)} fusion(bf16[128,2048]{1,0:T(8,128)(2,1)} %collective-permute-done.10, bf16[128,2048]{1,0:T(8,128)(2,1)S(1)} %collective-permute-done.9, bf16[128,2048]{1,0:T(8,128)(2,1)} %collective-permute-done.8, bf16[512,2048]{1,0:T(8,128)(2,1)} %collective-permute-done.7, bf16[512,2048]{1,0:T(8,128)(2,1)S(1)} %copy-done.1), kind=kLoop, calls=%fused_computation.7 | loop fusion | flops 2621440 | bytes 3145728 | tf_op jit(solution)/shard_map/convert_element_type | solution.py:53
  (88 shorter events, 34.7 us)
Async XLA Ops:
  7.2 77.9 %all-gather.2.cloned.1.call-start = ((), (), s32[]{:S(2)}) async-start(), calls=%async_computation.5 | async-start | bytes 2359296 | tf_op jit(solution)/shard_map/all_gather | solution.py:293
  20.4 26.1 %collective-permute-start.11 = (bf16[2,128,2048]{2,1,0:T(8,128)(2,1)S(1)}, bf16[2,128,2048]{2,1,0:T(8,128)(2,1)S(1)}, u32[]{:S(2)}, u32[]{:S(2)}) collective-permute-start(bf16[2,128,2048]{2,1,0:T(8,128)(2,1)S(1)} %pad_maximum_fusion.refs_0_), channel_id=1, source_target_pairs={{0,2},{2,4},{4,6},{6,0},{1,3},{3,5},{5,7},{7,1},{8,10},{10,12},{12... | collective-permute-start | bytes 3145736 | tf_op jit(solution)/shard_map/ppermute | solution.py:21
  22.0 38.2 %collective-permute-start.12 = (bf16[2,128,2048]{2,1,0:T(8,128)(2,1)S(1)}, bf16[2,128,2048]{2,1,0:T(8,128)(2,1)}, u32[]{:S(2)}, u32[]{:S(2)}) collective-permute-start(bf16[2,128,2048]{2,1,0:T(8,128)(2,1)S(1)} %pad_maximum_fusion.refs_0_), channel_id=1, source_target_pairs={{0,6},{2,0},{4,2},{6,4},{1,7},{3,1},{5,3},{7,5},{8,14},{10,8},{12,... | collective-permute-start | bytes 3145736 | tf_op jit(solution)/shard_map/ppermute | solution.py:21
  22.5 51.3 %collective-permute-start.15 = (bf16[2,128,2048]{2,1,0:T(8,128)(2,1)S(1)}, bf16[2,128,2048]{2,1,0:T(8,128)(2,1)}, u32[]{:S(2)}, u32[]{:S(2)}) collective-permute-start(bf16[2,128,2048]{2,1,0:T(8,128)(2,1)S(1)} %pad_maximum_fusion.refs_0_), channel_id=1, source_target_pairs={{0,1},{1,0},{2,3},{3,2},{4,5},{5,4},{6,7},{7,6},{8,9},{9,8},{10,11... | collective-permute-start | bytes 3145736 | tf_op jit(solution)/shard_map/ppermute | solution.py:21
  22.5 41.1 %collective-permute-start = (bf16[128,2048]{1,0:T(8,128)(2,1)S(1)}, bf16[128,2048]{1,0:T(8,128)(2,1)S(1)}, u32[]{:S(2)}, u32[]{:S(2)}) collective-permute-start(bf16[128,2048]{1,0:T(8,128)(2,1)S(1)} %copy-done.3), channel_id=1, source_target_pairs={{0,2},{2,4},{4,6},{6,0},{1,3},{3,5},{5,7},{7,1},{8,10},{10,12},{12... | collective-permute-start | bytes 1572872 | tf_op jit(solution)/shard_map/ppermute | solution.py:21
  24.0 39.5 %collective-permute-start.1 = (bf16[128,2048]{1,0:T(8,128)(2,1)S(1)}, bf16[128,2048]{1,0:T(8,128)(2,1)S(1)}, u32[]{:S(2)}, u32[]{:S(2)}) collective-permute-start(bf16[128,2048]{1,0:T(8,128)(2,1)S(1)} %copy-done.3), channel_id=1, source_target_pairs={{0,6},{2,0},{4,2},{6,4},{1,7},{3,1},{5,3},{7,5},{8,14},{10,8},{12,... | collective-permute-start | bytes 1572872 | tf_op jit(solution)/shard_map/ppermute | solution.py:21
  47.5 23.8 %collective-permute-start.2 = (bf16[128,2048]{1,0:T(8,128)(2,1)S(1)}, bf16[128,2048]{1,0:T(8,128)(2,1)S(1)}, u32[]{:S(2)}, u32[]{:S(2)}) collective-permute-start(bf16[128,2048]{1,0:T(8,128)(2,1)S(1)} %copy-done.3), channel_id=1, source_target_pairs={{0,4},{2,6},{4,0},{6,2},{1,5},{3,7},{5,1},{7,3},{8,12},{10,14},{12... | collective-permute-start | bytes 1572872 | tf_op jit(solution)/shard_map/ppermute | solution.py:21
  50.7 28.8 %all-to-all-start = ((bf16[8,64,512]{2,1,0:T(8,128)(2,1)}), bf16[8,64,512]{2,1,0:T(8,128)(2,1)}, u32[]{:S(2)}, u32[]{:S(2)}) async-start(bf16[8,64,512]{2,1,0:T(8,128)(2,1)} %broadcast_in_dim.7), calls=%async_computation | async-start | bytes 1048576 | tf_op jit(solution)/shard_map/all_to_all | solution.py:58
  59.1 162.3 %reduce-scatter.2.cloned.1.call-start = ((), (), s32[]{:S(2)}) async-start(), calls=%async_computation.6 | async-start | bytes 2359296 | tf_op jit(solution)/shard_map/reduce_scatter | solution.py:300
  60.3 17.5 %collective-permute-start.13 = (bf16[2,64,2048]{2,1,0:T(8,128)(2,1)S(1)}, bf16[2,64,2048]{2,1,0:T(8,128)(2,1)}, u32[]{:S(2)}, u32[]{:S(2)}) collective-permute-start(bf16[2,64,2048]{2,1,0:T(8,128)(2,1)S(1)} %slice.76), channel_id=1, source_target_pairs={{0,2},{2,4},{4,6},{6,0},{1,3},{3,5},{5,7},{7,1},{8,10},{10,12},{12... | collective-permute-start | bytes 1572872 | tf_op jit(solution)/shard_map/ppermute | solution.py:21
  63.6 19.5 %collective-permute-start.16 = (bf16[2,128,2048]{2,1,0:T(8,128)(2,1)}, bf16[2,128,2048]{2,1,0:T(8,128)(2,1)}, u32[]{:S(2)}, u32[]{:S(2)}) collective-permute-start(bf16[2,128,2048]{2,1,0:T(8,128)(2,1)} %copy-done.7), channel_id=1, source_target_pairs={{0,1},{1,0},{2,3},{3,2},{4,5},{5,4},{6,7},{7,6},{8,9},{9,8},{10,11... | collective-permute-start | bytes 3145736 | tf_op jit(solution)/shard_map/ppermute | solution.py:21
  73.8 51.7 %collective-permute-start.3 = (bf16[1,512,2048]{2,1,0:T(8,128)(2,1)S(1)}, bf16[1,512,2048]{2,1,0:T(8,128)(2,1)}, u32[]{:S(2)}, u32[]{:S(2)}) collective-permute-start(bf16[1,512,2048]{2,1,0:T(8,128)(2,1)S(1)} %maximum_bitcast_fusion.refs_0_), channel_id=1, source_target_pairs={{0,1},{1,0},{2,3},{3,2},{4,5},{5,4},{6,7},{7,6},{8,9},{9,8},{10,11... | collective-permute-start | bytes 6291464 | tf_op jit(solution)/shard_map/ppermute | solution.py:21
  79.9 26.6 %collective-permute-start.4 = (bf16[8,64,512]{2,1,0:T(8,128)(2,1)}, bf16[8,64,512]{2,1,0:T(8,128)(2,1)S(1)}, u32[]{:S(2)}, u32[]{:S(2)}) collective-permute-start(bf16[8,64,512]{2,1,0:T(8,128)(2,1)} %all-to-all-done.refs_2_.refs_10_), channel_id=1, source_target_pairs={{0,8},{8,16},{16,24},{24,0},{1,9},{9,17},{17,25},{25,1},{2,10},{10... | collective-permute-start | bytes 1572872 | tf_op jit(solution)/shard_map/ppermute | solution.py:21
  81.7 24.9 %collective-permute-start.5 = (bf16[8,64,512]{2,1,0:T(8,128)(2,1)}, bf16[8,64,512]{2,1,0:T(8,128)(2,1)}, u32[]{:S(2)}, u32[]{:S(2)}) collective-permute-start(bf16[8,64,512]{2,1,0:T(8,128)(2,1)} %all-to-all-done.refs_2_.refs_10_), channel_id=1, source_target_pairs={{0,16},{8,24},{16,0},{24,8},{1,17},{9,25},{17,1},{25,9},{2,18},{10... | collective-permute-start | bytes 1572872 | tf_op jit(solution)/shard_map/ppermute | solution.py:21
  83.1 24.2 %collective-permute-start.6 = (bf16[8,64,512]{2,1,0:T(8,128)(2,1)}, bf16[8,64,512]{2,1,0:T(8,128)(2,1)}, u32[]{:S(2)}, u32[]{:S(2)}) collective-permute-start(bf16[8,64,512]{2,1,0:T(8,128)(2,1)} %all-to-all-done.refs_2_.refs_10_), channel_id=1, source_target_pairs={{0,24},{8,0},{16,8},{24,16},{1,25},{9,1},{17,9},{25,17},{2,26},{10... | collective-permute-start | bytes 1572872 | tf_op jit(solution)/shard_map/ppermute | solution.py:21
  125.3 49.3 %collective-permute-start.20 = (bf16[512,2048]{1,0:T(8,128)(2,1)}, bf16[512,2048]{1,0:T(8,128)(2,1)}, u32[]{:S(2)}, u32[]{:S(2)}) collective-permute-start(bf16[512,2048]{1,0:T(8,128)(2,1)} %get-tuple-element.17), channel_id=1, source_target_pairs={{0,1},{1,0},{2,3},{3,2},{4,5},{5,4},{6,7},{7,6},{8,9},{9,8},{10,11... | collective-permute-start | bytes 6291464 | tf_op jit(solution)/shard_map/ppermute | solution.py:21
  133.9 48.5 %collective-permute-start.7 = (bf16[512,2048]{1,0:T(8,128)(2,1)}, bf16[512,2048]{1,0:T(8,128)(2,1)}, u32[]{:S(2)}, u32[]{:S(2)}) collective-permute-start(bf16[512,2048]{1,0:T(8,128)(2,1)} %get-tuple-element.13), channel_id=1, source_target_pairs={{0,1},{1,0},{2,3},{3,2},{4,5},{5,4},{6,7},{7,6},{8,9},{9,8},{10,11... | collective-permute-start | bytes 6291464 | tf_op jit(solution)/shard_map/ppermute | solution.py:21
  134.5 30.6 %all-to-all-start.2 = ((bf16[4,8,64,512]{3,2,1,0:T(8,128)(2,1)}), bf16[4,8,64,512]{3,2,1,0:T(8,128)(2,1)S(1)}, u32[]{:S(2)}, u32[]{:S(2)}) async-start(bf16[4,8,64,512]{3,2,1,0:T(8,128)(2,1)} %get-tuple-element.18), calls=%async_computation.2 | async-start | bytes 4194304 | tf_op jit(solution)/shard_map/all_to_all | solution.py:62
  166.4 24.9 %all-to-all-start.3 = ((bf16[8,64,512]{2,1,0:T(8,128)(2,1)}), bf16[8,64,512]{2,1,0:T(8,128)(2,1)S(1)}, u32[]{:S(2)}, u32[]{:S(2)}) async-start(bf16[8,64,512]{2,1,0:T(8,128)(2,1)} %reduce_sum.21), calls=%async_computation.3 | async-start | bytes 1048576 | tf_op jit(solution)/shard_map/all_to_all | solution.py:62
  178.1 36.1 %collective-permute-start.21 = (bf16[128,2048]{1,0:T(8,128)(2,1)}, bf16[128,2048]{1,0:T(8,128)(2,1)}, u32[]{:S(2)}, u32[]{:S(2)}) collective-permute-start(bf16[128,2048]{1,0:T(8,128)(2,1)} %get-tuple-element.20), channel_id=1, source_target_pairs={{0,2},{2,4},{4,6},{6,0},{1,3},{3,5},{5,7},{7,1},{8,10},{10,12},{12... | collective-permute-start | bytes 1572872 | tf_op jit(solution)/shard_map/ppermute | solution.py:21
  179.7 38.8 %collective-permute-start.22 = (bf16[128,2048]{1,0:T(8,128)(2,1)}, bf16[128,2048]{1,0:T(8,128)(2,1)}, u32[]{:S(2)}, u32[]{:S(2)}) collective-permute-start(bf16[128,2048]{1,0:T(8,128)(2,1)} %get-tuple-element.22), channel_id=1, source_target_pairs={{0,6},{2,0},{4,2},{6,4},{1,7},{3,1},{5,3},{7,5},{8,14},{10,8},{12,... | collective-permute-start | bytes 1572872 | tf_op jit(solution)/shard_map/ppermute | solution.py:21
  180.2 38.3 %collective-permute-start.23 = (bf16[128,2048]{1,0:T(8,128)(2,1)}, bf16[128,2048]{1,0:T(8,128)(2,1)}, u32[]{:S(2)}, u32[]{:S(2)}) collective-permute-start(bf16[128,2048]{1,0:T(8,128)(2,1)} %get-tuple-element.21), channel_id=1, source_target_pairs={{0,4},{2,6},{4,0},{6,2},{1,5},{3,7},{5,1},{7,3},{8,12},{10,14},{12... | collective-permute-start | bytes 1572872 | tf_op jit(solution)/shard_map/ppermute | solution.py:21
  185.4 39.7 %collective-permute-start.10 = (bf16[128,2048]{1,0:T(8,128)(2,1)}, bf16[128,2048]{1,0:T(8,128)(2,1)}, u32[]{:S(2)}, u32[]{:S(2)}) collective-permute-start(bf16[128,2048]{1,0:T(8,128)(2,1)} %get-tuple-element.24), channel_id=1, source_target_pairs={{0,4},{2,6},{4,0},{6,2},{1,5},{3,7},{5,1},{7,3},{8,12},{10,14},{12... | collective-permute-start | bytes 1572872 | tf_op jit(solution)/shard_map/ppermute | solution.py:21
  186.7 39.1 %collective-permute-start.8 = (bf16[128,2048]{1,0:T(8,128)(2,1)}, bf16[128,2048]{1,0:T(8,128)(2,1)}, u32[]{:S(2)}, u32[]{:S(2)}) collective-permute-start(bf16[128,2048]{1,0:T(8,128)(2,1)} %get-tuple-element.23), channel_id=1, source_target_pairs={{0,2},{2,4},{4,6},{6,0},{1,3},{3,5},{5,7},{7,1},{8,10},{10,12},{12... | collective-permute-start | bytes 1572872 | tf_op jit(solution)/shard_map/ppermute | solution.py:21
  (21 other events, 243.7 us)
Sparse Core Ops, SparseCore 0:
  19.2 43.6 all-gather.1
  97.4 43.3 reduce-scatter.1

commit v6 on v5

--- a/solution.py
+++ b/solution.py
@@ -120,19 +120,28 @@
         relu[at] = r
         hid[at] = (r * r).astype(BF16)
     settle(cot_waits, cot.shape[0])
+    nx, nz, part = dt.shape[:3]
+
+    def terms(first, last):
+        @pl.loop(first, last)
+        def _(i):
+            at = pl.ds(pl.multiple_of(i * nx * part, nx * part), nx * part)
+            term = over_tokens(cot[:, at], hid[...]).astype(BF16)
+            for j in range(nx):
+                dt[j, i] = term[j * part : (j + 1) * part]
+
+        piece = pl.ds(first, last - first)
+        return pltpu.make_async_copy(dt.at[:, piece], down_out.at[:, piece], sems.at[first and 3 or 2])
+
+    early = terms(0, nz * 3 // 4)
     relu_copy = pltpu.make_async_copy(relu, relu_out, sems.at[1])
-    block = dt.shape[0] // 8
-
-    @pl.loop(0, 8)
-    def _(i):
-        at = pl.ds(pl.multiple_of(i * block, block), block)
-        dt[at] = over_tokens(cot[:, at], hid[...]).astype(BF16)
-
     relu_copy.start()
-    out_copy = pltpu.make_async_copy(dt, down_out, sems.at[2])
-    out_copy.start()
+    early.start()
+    late = terms(nz * 3 // 4, nz)
+    late.start()
     relu_copy.wait()
-    out_copy.wait()
+    early.wait()
+    late.wait()
 
 
 def place_down(parts, down, sems):
@@ -146,14 +155,15 @@
     return waits
 
 
-def up_kernel(*refs):
-    pieces, parts, (relu_in, up_out, pg_out) = refs[:10], refs[10:14], refs[14:17]
-    saved, cot, down, relu, pg, ut, in_sems, w_sems, sems = refs[17:]
+def grad_kernel(*refs):
+    pieces, parts, (relu_in, w, pg_out, mine_out, theirs_out) = refs[:10], refs[10:14], refs[14:19]
+    cot, down, up, relu, pg, mine, theirs, in_sems, w_sems, sems = refs[19:]
     down_waits = place_down(parts, down, w_sems)
-    cot_waits = copies(pieces, cot, in_sems.at[1], 1)
+    cot_waits = copies(pieces, cot, in_sems, 1)
     relu_copy = pltpu.make_async_copy(relu_in, relu, sems.at[0])
     relu_copy.start()
-    saved_waits = copies(pieces, saved, in_sems.at[0], 0)
+    up_copy = pltpu.make_async_copy(w, up, sems.at[1])
+    up_copy.start()
     for copy in down_waits:
         copy.wait()
     weight = down[...].reshape(-1, down.shape[-1])
@@ -164,39 +174,43 @@
         if t == 0:
             relu_copy.wait()
         pg[at] = (2.0 * relu[at] * grad).astype(BF16)
-    settle(saved_waits, saved.shape[0])
-    nx, nz, part = ut.shape[:3]
-
-    @pl.loop(0, nz)
-    def _(i):
-        at = pl.ds(pl.multiple_of(i * nx * part, nx * part), nx * part)
-        term = over_tokens(saved[:, at], pg[...]).astype(BF16)
-        for j in range(nx):
-            ut[j, i] = term[j * part : (j + 1) * part]
-
-    pg_copy = pltpu.make_async_copy(pg, pg_out, sems.at[1])
+    up_copy.wait()
+    pg_copy = pltpu.make_async_copy(pg, pg_out, sems.at[2])
+    first = pltpu.make_async_copy(mine, mine_out, sems.at[3])
+    second = pltpu.make_async_copy(theirs, theirs_out, sems.at[4])
+    outputs(pg, mine.shape[0], up, theirs, pg_copy)
+    outputs(pg, 0, up, mine, second)
+    first.start()
+    for copy in (pg_copy, second, first):
+        copy.wait()
+
+
+def up_kernel(*refs):
+    pieces, (pg_in, up_out) = refs[:10], refs[10:12]
+    saved, pg, ut, in_sems, sems = refs[12:]
+    pg_copy = pltpu.make_async_copy(pg_in, pg, sems.at[0])
     pg_copy.start()
-    ut_copy = pltpu.make_async_copy(ut, up_out, sems.at[2])
-    ut_copy.start()
+    waits = copies(pieces, saved, in_sems, 0)
     pg_copy.wait()
-    ut_copy.wait()
-
-
-def rows_kernel(pg_in, w, mine_out, theirs_out, pg, up, mine, theirs, sems):
-    pg_copy = pltpu.make_async_copy(pg_in, pg, sems.at[0])
-    up_copy = pltpu.make_async_copy(w, up, sems.at[1])
-    pg_copy.start()
-    up_copy.start()
-    pg_copy.wait()
-    up_copy.wait()
-    first = pltpu.make_async_copy(mine, mine_out, sems.at[2])
-    second = pltpu.make_async_copy(theirs, theirs_out, sems.at[3])
-    outputs(pg, mine.shape[0], up, theirs)
-    outputs(pg, 0, up, mine)
-    second.start()
-    first.start()
-    first.wait()
-    second.wait()
+    settle(waits, saved.shape[0])
+    block = 256
+    depth = ut.shape[0]
+
+    def terms(first, last):
+        @pl.loop(first, last, step=block)
+        def _(i):
+            at = pl.ds(pl.multiple_of(i, block), block)
+            ut[at] = over_tokens(saved[:, at], pg[...]).astype(BF16)
+
+        piece = pl.ds(first, last - first)
+        return pltpu.make_async_copy(ut.at[piece], up_out.at[piece], sems.at[first and 2 or 1])
+
+    early = terms(0, depth * 3 // 4)
+    early.start()
+    late = terms(depth * 3 // 4, depth)
+    late.start()
+    early.wait()
+    late.wait()
 
 
 def flat_rows(weight, first, count):
@@ -204,14 +218,13 @@
     return weight[first // each : (first + count) // each].reshape(count, weight.shape[-1])
 
 
-def outputs(hidden, first, weight, out):
-    @pl.loop(0, out.shape[0], step=TILE)
-    def _(t):
-        rows = hidden[pl.ds(pl.multiple_of(first + t, TILE), TILE)]
-        for n in range(0, out.shape[1], 512):
-            block = weight[n : n + 512] if len(weight.shape) == 2 else flat_rows(weight, n, 512)
-            part = rows_times(rows, block)
-            out[pl.ds(pl.multiple_of(t, TILE), TILE), n : n + 512] = part.astype(BF16)
+def outputs(hidden, first, weight, out, copy=None):
+    rows = hidden[pl.ds(first, out.shape[0])]
+    for n in range(0, out.shape[1], 512):
+        block = weight[n : n + 512] if len(weight.shape) == 2 else flat_rows(weight, n, 512)
+        out[:, n : n + 512] = rows_times(rows, block).astype(BF16)
+        if copy is not None and n == 512:
+            copy.start()
 
 
 def ahead_kernel(*refs):
@@ -232,8 +245,7 @@
     first = pltpu.make_async_copy(mine, mine_out, sems.at[1])
     second = pltpu.make_async_copy(theirs, theirs_out, sems.at[2])
     outputs(hid, mine.shape[0], down, theirs)
-    outputs(hid, 0, down, mine)
-    second.start()
+    outputs(hid, 0, down, mine, second)
     first.start()
     first.wait()
     second.wait()
@@ -261,28 +273,28 @@
     group, weight, wide = ((rows, depth), BF16), ((depth, cols), BF16), ((rows, cols), BF16)
     relu = (wide[0], F32)
     part = depth // (nx * nz)
-    split, up_shape = ((nz, nx, part, cols), BF16), ((nx, nz, part, cols), BF16)
+    split, swapped = ((nz, nx, part, cols), BF16), ((nx, nz, part, cols), BF16)
     half = ((rows // 2, depth), BF16)
 
     def pre():
-        scratch = (group, group, weight, relu, wide, weight), ((2, n), (3,))
-        return call(pre_kernel, (*pieces, up), (weight, relu), scratch, 2 * flops)
-
-    def up_term(relu_part):
-        scratch = (group, group, split, relu, wide, up_shape), ((2, n), (nx,), (3,))
-        operands = (*pieces, *down, relu_part)
-        return call(up_kernel, operands, (up_shape, wide), scratch, 2 * flops)
-
-    def row_grad(pre_grad):
-        scratch = (wide, weight, half, half), ((4,),)
-        return call(rows_kernel, (pre_grad, up), (half, half), scratch, flops)
+        scratch = (group, group, weight, relu, wide, swapped), ((2, n), (4,))
+        return call(pre_kernel, (*pieces, up), (swapped, relu), scratch, 2 * flops)
+
+    def grad(relu_part):
+        scratch = (group, split, weight, relu, wide, half, half), ((n,), (nx,), (5,))
+        operands = (*pieces, *down, relu_part, up)
+        return call(grad_kernel, operands, (wide, half, half), scratch, 2 * flops)
+
+    def up_term(pre_grad):
+        scratch = (group, wide, weight), ((n,), (3,))
+        return call(up_kernel, (*pieces, pre_grad), (weight,), scratch, flops)[0]
 
     def ahead():
         scratch = (group, weight, split, wide, half, half), ((2,), (nx,), (3,))
         operands = (*later, *down, up)
         return call(ahead_kernel, operands, (half, half), scratch, 2 * flops)
 
-    return pre, up_term, row_grad, ahead
+    return pre, grad, up_term, ahead
 
 
 def body(later_rows, earlier_rows, cotangent, up_weight, down_weight, up_total, down_total):
@@ -295,17 +307,17 @@
     down = (down, *(shift(down, "x", by) for by in range(1, nx)))
     pieces = gather_tokens((earlier_rows, cotangent))
     later = gather_later(later_rows)
-    pre, grad_up, grad_rows, ahead = products(pieces, later, up, down, nz, nx)
+    pre, grad, grad_up, ahead = products(pieces, later, up, down, nz, nx)
     down_term, relu = pre()
-    down_term = lax.psum_scatter(down_term, "z", scatter_dimension=0, tiled=True)
-    up_term, pre_grad = grad_up(relu)
-    up_term = exchange_sum(up_term, "x").astype(BF16)
-    up_term = exchange_sum(up_term, "z")
-    mine, theirs = grad_rows(pre_grad)
+    down_term = exchange_sum(down_term, "x").astype(BF16)
+    pre_grad, mine, theirs = grad(relu)
     earlier_grad = scatter_tokens(mine, theirs)
+    up_term = grad_up(pre_grad)
+    up_term = lax.psum_scatter(up_term, "z", scatter_dimension=0, tiled=True)
+    down_term = exchange_sum(down_term, "z")
     mine, theirs = ahead()
     later_out = scatter_tokens(mine, theirs)
-    down_term = hop_sum(down_term.reshape(-1, *down_weight.shape), "x")
+    up_term = hop_sum(up_term.reshape(-1, *up_weight.shape), "x")
     up_updated = up_total + up_term * factor
     down_updated = down_total + down_term * factor
     return later_out, earlier_grad, up_updated, down_updated

time: 239 us -> 251 us (1.050)
  waiting for transfers between devices: 100 us -> 119 us
  starting transfers between devices: 48.7 us -> 43.1 us
    all_to_all x1, waiting for transfers between devices: 0.01 us -> 13.9 us  [gather(): lax.all_to_all(jnp.broadcast_to(x[None], (n, *x.shape)), axis, 0, 0, tile...]
    all_to_all x2, starting transfers between devices: 12.3 us -> 7.37 us  [exchange_sum(): tiles = lax.all_to_all(term, axis, 0, 0, tiled=True)]
    ppermute x27, waiting for transfers between devices: 70.7 us -> 75.6 us  [shift(): return lax.ppermute(x, axis, [(i, (i + by) % n) for i in range(n)])]
  transfers between devices with their start and end apart: 32 -> 32, of which waited for: 14 -> 10; matrix products, arithmetic and copies ran while one was open for 9% -> 9% of each run, Pallas kernels for 16% -> 15%
where the time goes in v6:
time: 251 us; the launch traced here: 250 us
  waiting for transfers between devices  119 us (47%)
  starting transfers between devices  43.1 us (17%)
  Pallas kernels  37.2 us (15%)
  other arithmetic  20 us (8%)
  between operations  14.2 us (6%)
  blocking collectives  10.9 us (4%)
  local copies, waits for them, and re-layouts  5.95 us (2%)
    ppermute x27, waiting for transfers between devices, shift(): return lax.ppermute(x, axis, [(i, (i + by) % n) for i in range(n)])  75.6 us
    pallas_call x4, Pallas kernels, call(): pl.pallas_call(kernel, out_shape=[jax.ShapeDtypeStruct(*s) for s in outs]...  37.2 us
    all_to_all x2, waiting for transfers between devices, exchange_sum(): tiles = lax.all_to_all(term, axis, 0, 0, tiled=True)  29.3 us
    ppermute x27, starting transfers between devices, shift(): return lax.ppermute(x, axis, [(i, (i + by) % n) for i in range(n)])  28.3 us
    all_to_all x1, waiting for transfers between devices, gather(): lax.all_to_all(jnp.broadcast_to(x[None], (n, *x.shape)), axis, 0, 0, tile...  13.9 us
    all_to_all x1, blocking collectives, gather(): lax.all_to_all(jnp.broadcast_to(x[None], (n, *x.shape)), axis, 0, 0, tile...  10.9 us
    all_to_all x2, starting transfers between devices, exchange_sum(): tiles = lax.all_to_all(term, axis, 0, 0, tiled=True)  7.37 us
    all_to_all x1, starting transfers between devices, gather(): lax.all_to_all(jnp.broadcast_to(x[None], (n, *x.shape)), axis, 0, 0, tile...  7.35 us
  transfers between devices with their start and end apart: 32, of which 10 were waited for; matrix products, arithmetic and copies ran while one was open for 9% of the time, Pallas kernels for 15%

profile of v6, /device:TPU:8, one launch (start us, length us, event | category | flops | bytes accessed | tf_op | source)
XLA Modules:
  0.0 250.1 jit_solution(14448942097158694478)
XLA Ops:
  8.1 10.9 %all_to_all.20 = bf16[4,64,512]{2,1,0:T(8,128)(2,1)} all-to-all(bf16[4,64,512]{2,1,0:T(8,128)(2,1)S(1)} %broadcast_in_dim.8), channel_id=1, replica_groups=mesh['z'=8,'x'=4,'y'=4,'c'=2] {'x'}, dimensions={0} | all-to-all | bytes 524288 | tf_op jit(solution)/shard_map/all_to_all | solution.py:58
  24.7 21.8 %collective-permute-done.11.refs_1_ = bf16[2,128,2048]{2,1,0:T(8,128)(2,1)S(1)} collective-permute-done((bf16[2,128,2048]{2,1,0:T(8,128)(2,1)S(1)}, bf16[2,128,2048]{2,1,0:T(8,128)(2,1)S(1)}, u32[]{:S(2)}, u32[]{:S(2)}) %collective-permute-start.11) | collective-permute-done | bytes 1048608 | tf_op jit(solution)/shard_map/ppermute | solution.py:21
  46.4 2.3 collective-permute-start.2
  51.8 15.9 %collective-permute-done = bf16[128,2048]{1,0:T(8,128)(2,1)S(1)} collective-permute-done((bf16[128,2048]{1,0:T(8,128)(2,1)}, bf16[128,2048]{1,0:T(8,128)(2,1)S(1)}, u32[]{:S(2)}, u32[]{:S(2)}) %collective-permute-start) | collective-permute-done | bytes 524320 | tf_op jit(solution)/shard_map/ppermute | solution.py:21
  67.7 2.7 %collective-permute-start.14 = (bf16[2,64,2048]{2,1,0:T(8,128)(2,1)}, bf16[2,64,2048]{2,1,0:T(8,128)(2,1)}, u32[]{:S(2)}, u32[]{:S(2)}) collective-permute-start(bf16[2,64,2048]{2,1,0:T(8,128)(2,1)} %slice.77), channel_id=1, source_target_pairs={{0,6},{2,0},{4,2},{6,4},{1,7},{3,1},{5,3},{7,5},{8,14},{10,8},{12,... | collective-permute-start | bytes 1572872 | tf_op jit(solution)/shard_map/ppermute | solution.py:21
  72.1 7.3 %all-to-all-start = ((bf16[8,64,512]{2,1,0:T(8,128)(2,1)}), bf16[8,64,512]{2,1,0:T(8,128)(2,1)}, u32[]{:S(2)}, u32[]{:S(2)}) async-start(bf16[8,64,512]{2,1,0:T(8,128)(2,1)} %broadcast_in_dim.7), calls=%async_computation | async-start | bytes 1048576 | tf_op jit(solution)/shard_map/all_to_all | solution.py:58
  79.8 3.2 %maximum_bitcast_fusion.refs_0_ = bf16[1,512,2048]{2,1,0:T(8,128)(2,1)} fusion(bf16[128,2048]{1,0:T(8,128)(2,1)} %collective-permute-done.2, bf16[128,2048]{1,0:T(8,128)(2,1)} %copy-done.7, bf16[128,2048]{1,0:T(8,128)(2,1)} %copy-done.6, bf16[128,2048]{1,0:T(8,128)(2,1)} %param.7), kind=kLoop, calls=%fused_computation | loop fusion | flops 8388608 | bytes 4194304 | tf_op jit(solution)/shard_map/broadcast_in_dim | solution.py:38
  83.8 13.9 %all-to-all-done.refs_2_.refs_10_ = bf16[8,64,512]{2,1,0:T(8,128)(2,1)} async-done(((bf16[8,64,512]{2,1,0:T(8,128)(2,1)}), bf16[8,64,512]{2,1,0:T(8,128)(2,1)}, u32[]{:S(2)}, u32[]{:S(2)}) %all-to-all-start) | async-done | bytes 524320 | tf_op jit(solution)/shard_map/all_to_all | solution.py:58
  101.3 11.5 %shard_map.103 = (bf16[4,8,64,512]{3,2,1,0:T(8,128)(2,1)}, f32[1024,512]{1,0:T(8,128)}) custom-call(bf16[2,128,2048]{2,1,0:T(8,128)(2,1)} %copy-done, bf16[2,128,2048]{2,1,0:T(8,128)(2,1)} %copy-done.1, bf16[2,128,2048]{2,1,0:T(8,128)(2,1)} %copy-done.2, bf16[2,64,2048]{2,1,0:T(8,128)(2,1)} %collective-permute-done.13.refs_3_, ...), custom_call_target="tpu_custom_call" | custom-call | flops 4294967296 | bytes 12582912 | tf_op jit(solution)/shard_map/pallas_call | solution.py:256
  112.7 11.6 %collective-permute-done.4.refs_3_.refs_11_ = bf16[8,64,512]{2,1,0:T(8,128)(2,1)} collective-permute-done((bf16[8,64,512]{2,1,0:T(8,128)(2,1)}, bf16[8,64,512]{2,1,0:T(8,128)(2,1)}, u32[]{:S(2)}, u32[]{:S(2)}) %collective-permute-start.4) | collective-permute-done | bytes 524320 | tf_op jit(solution)/shard_map/ppermute | solution.py:21
  125.7 10.0 %shard_map.104 = (bf16[1024,512]{1,0:T(8,128)(2,1)}, bf16[512,2048]{1,0:T(8,128)(2,1)}, bf16[512,2048]{1,0:T(8,128)(2,1)}) custom-call(bf16[2,128,2048]{2,1,0:T(8,128)(2,1)} %copy-done, bf16[2,128,2048]{2,1,0:T(8,128)(2,1)} %copy-done.1, bf16[2,128,2048]{2,1,0:T(8,128)(2,1)} %copy-done.2, bf16[2,64,2048]{2,1,0:T(8,128)(2,1)} %collective-permute-done.13.refs_3_, ...), custom_call_target="tpu_custom_call" | custom-call | flops 4294967296 | bytes 12582912 | tf_op jit(solution)/shard_map/pallas_call | solution.py:256
  135.6 7.3 %shard_map.105 = bf16[2048,512]{1,0:T(8,128)(2,1)} custom-call(bf16[2,128,2048]{2,1,0:T(8,128)(2,1)} %copy-done, bf16[2,128,2048]{2,1,0:T(8,128)(2,1)} %copy-done.1, bf16[2,128,2048]{2,1,0:T(8,128)(2,1)} %copy-done.2, bf16[2,64,2048]{2,1,0:T(8,128)(2,1)} %collective-permute-done.13.refs_3_, bf16[2,64,2048]{2,1,0:T(8,128)(2,1)} %collective-permute-done.14.refs_4_, ...), custom_call_target="tpu_custom_call" | custom-call | flops 2147483648 | bytes 12582912 | tf_op jit(solution)/shard_map/pallas_call | solution.py:256
  143.0 8.5 %shard_map.102 = (bf16[512,2048]{1,0:T(8,128)(2,1)}, bf16[512,2048]{1,0:T(8,128)(2,1)}) custom-call(bf16[1,512,2048]{2,1,0:T(8,128)(2,1)} %maximum_bitcast_fusion.refs_0_, bf16[1,512,2048]{2,1,0:T(8,128)(2,1)} %collective-permute-done.3.refs_1_, bf16[8,64,512]{2,1,0:T(8,128)(2,1)} %all-to-all-done.refs_2_.refs_10_, ...), custom_call_target="tpu_custom_call" | custom-call | flops 4294967296 | bytes 12582912 | tf_op jit(solution)/shard_map/pallas_call | solution.py:256
  152.1 3.9 %all-to-all-start.2 = ((bf16[4,8,64,512]{3,2,1,0:T(8,128)(2,1)}), bf16[4,8,64,512]{3,2,1,0:T(8,128)(2,1)S(1)}, u32[]{:S(2)}, u32[]{:S(2)}) async-start(bf16[4,8,64,512]{3,2,1,0:T(8,128)(2,1)} %get-tuple-element.17), calls=%async_computation.3 | async-start | bytes 4194304 | tf_op jit(solution)/shard_map/all_to_all | solution.py:62
  156.0 26.5 %all-to-all-done.2 = bf16[4,8,64,512]{3,2,1,0:T(8,128)(2,1)S(1)} async-done(((bf16[4,8,64,512]{3,2,1,0:T(8,128)(2,1)}), bf16[4,8,64,512]{3,2,1,0:T(8,128)(2,1)S(1)}, u32[]{:S(2)}, u32[]{:S(2)}) %all-to-all-start.2) | async-done | bytes 2097184 | tf_op jit(solution)/shard_map/all_to_all | solution.py:62
  183.8 3.5 %all-to-all-start.3 = ((bf16[8,64,512]{2,1,0:T(8,128)(2,1)}), bf16[8,64,512]{2,1,0:T(8,128)(2,1)S(1)}, u32[]{:S(2)}, u32[]{:S(2)}) async-start(bf16[8,64,512]{2,1,0:T(8,128)(2,1)} %reduce_sum.21), calls=%async_computation.4 | async-start | bytes 1048576 | tf_op jit(solution)/shard_map/all_to_all | solution.py:62
  187.4 3.5 %add_convert_fusion.3 = (bf16[128,2048]{1,0:T(8,128)(2,1)}, bf16[128,2048]{1,0:T(8,128)(2,1)}, bf16[128,2048]{1,0:T(8,128)(2,1)}) fusion(bf16[512,2048]{1,0:T(8,128)(2,1)} %collective-permute-done.20, bf16[512,2048]{1,0:T(8,128)(2,1)} %get-tuple-element.14), kind=kLoop, calls=%fused_computation.6 | loop fusion | flops 3145728 | bytes 4718592 | tf_op jit(solution)/shard_map/convert_element_type | solution.py:43
  192.8 2.7 %collective-permute-start.23 = (bf16[128,2048]{1,0:T(8,128)(2,1)}, bf16[128,2048]{1,0:T(8,128)(2,1)}, u32[]{:S(2)}, u32[]{:S(2)}) collective-permute-start(bf16[128,2048]{1,0:T(8,128)(2,1)} %get-tuple-element.19), channel_id=1, source_target_pairs={{0,4},{2,6},{4,0},{6,2},{1,5},{3,7},{5,1},{7,3},{8,12},{10,14},{12... | collective-permute-start | bytes 1572872 | tf_op jit(solution)/shard_map/ppermute | solution.py:21
  195.5 2.9 %add_convert_fusion.7 = (bf16[128,2048]{1,0:T(8,128)(2,1)}, bf16[128,2048]{1,0:T(8,128)(2,1)}, bf16[128,2048]{1,0:T(8,128)(2,1)S(1)}) fusion(bf16[512,2048]{1,0:T(8,128)(2,1)} %collective-permute-done.7, bf16[512,2048]{1,0:T(8,128)(2,1)S(1)} %copy-done.3), kind=kLoop, calls=%fused_computation.10 | loop fusion | flops 3145728 | bytes 4718592 | tf_op jit(solution)/shard_map/convert_element_type | solution.py:43
  201.3 2.8 %all-to-all-done.3 = bf16[8,64,512]{2,1,0:T(8,128)(2,1)S(1)} async-done(((bf16[8,64,512]{2,1,0:T(8,128)(2,1)}), bf16[8,64,512]{2,1,0:T(8,128)(2,1)S(1)}, u32[]{:S(2)}, u32[]{:S(2)}) %all-to-all-start.3) | async-done | bytes 524320 | tf_op jit(solution)/shard_map/all_to_all | solution.py:62
  204.8 22.9 %collective-permute-done.21 = bf16[128,2048]{1,0:T(8,128)(2,1)} collective-permute-done((bf16[128,2048]{1,0:T(8,128)(2,1)}, bf16[128,2048]{1,0:T(8,128)(2,1)}, u32[]{:S(2)}, u32[]{:S(2)}) %collective-permute-start.21) | collective-permute-done | bytes 524320 | tf_op jit(solution)/shard_map/ppermute | solution.py:21
  229.0 2.9 %add_convert_fusion = bf16[128,2048]{1,0:T(8,128)(2,1)} fusion(bf16[128,2048]{1,0:T(8,128)(2,1)} %collective-permute-done.23, bf16[128,2048]{1,0:T(8,128)(2,1)} %collective-permute-done.22, bf16[128,2048]{1,0:T(8,128)(2,1)} %collective-permute-done.21, bf16[512,2048]{1,0:T(8,128)(2,1)} %collective-permute-done.20, bf16[512,2048]{1,0:T(8,128)(2,1)} %get-tuple-element.14), kind=kLoop, calls=%fused_computation.3 | loop fusion | flops 2621440 | bytes 3145728 | tf_op jit(solution)/shard_map/convert_element_type | solution.py:53
  233.5 2.1 collective-permute-start.25
  239.2 2.6 %add_convert_fusion.4 = bf16[128,2048]{1,0:T(8,128)(2,1)} fusion(bf16[128,2048]{1,0:T(8,128)(2,1)} %collective-permute-done.10, bf16[128,2048]{1,0:T(8,128)(2,1)S(1)} %collective-permute-done.9, bf16[128,2048]{1,0:T(8,128)(2,1)} %collective-permute-done.8, bf16[512,2048]{1,0:T(8,128)(2,1)} %collective-permute-done.7, bf16[512,2048]{1,0:T(8,128)(2,1)S(1)} %copy-done.3), kind=kLoop, calls=%fused_computation.7 | loop fusion | flops 2621440 | bytes 3145728 | tf_op jit(solution)/shard_map/convert_element_type | solution.py:53
  (86 shorter events, 33.0 us)
Async XLA Ops:
  7.2 94.1 %all-gather.2.cloned.1.call-start = ((), (), s32[]{:S(2)}) async-start(), calls=%async_computation.5 | async-start | bytes 2359296 | tf_op jit(solution)/shard_map/all_gather | solution.py:305
  20.3 26.1 %collective-permute-start.11 = (bf16[2,128,2048]{2,1,0:T(8,128)(2,1)S(1)}, bf16[2,128,2048]{2,1,0:T(8,128)(2,1)S(1)}, u32[]{:S(2)}, u32[]{:S(2)}) collective-permute-start(bf16[2,128,2048]{2,1,0:T(8,128)(2,1)S(1)} %pad_maximum_fusion.refs_0_), channel_id=1, source_target_pairs={{0,2},{2,4},{4,6},{6,0},{1,3},{3,5},{5,7},{7,1},{8,10},{10,12},{12... | collective-permute-start | bytes 3145736 | tf_op jit(solution)/shard_map/ppermute | solution.py:21
  22.0 27.6 %collective-permute-start.12 = (bf16[2,128,2048]{2,1,0:T(8,128)(2,1)S(1)}, bf16[2,128,2048]{2,1,0:T(8,128)(2,1)S(1)}, u32[]{:S(2)}, u32[]{:S(2)}) collective-permute-start(bf16[2,128,2048]{2,1,0:T(8,128)(2,1)S(1)} %pad_maximum_fusion.refs_0_), channel_id=1, source_target_pairs={{0,6},{2,0},{4,2},{6,4},{1,7},{3,1},{5,3},{7,5},{8,14},{10,8},{12,... | collective-permute-start | bytes 3145736 | tf_op jit(solution)/shard_map/ppermute | solution.py:21
  22.4 60.5 %collective-permute-start.15 = (bf16[2,128,2048]{2,1,0:T(8,128)(2,1)S(1)}, bf16[2,128,2048]{2,1,0:T(8,128)(2,1)}, u32[]{:S(2)}, u32[]{:S(2)}) collective-permute-start(bf16[2,128,2048]{2,1,0:T(8,128)(2,1)S(1)} %pad_maximum_fusion.refs_0_), channel_id=1, source_target_pairs={{0,1},{1,0},{2,3},{3,2},{4,5},{5,4},{6,7},{7,6},{8,9},{9,8},{10,11... | collective-permute-start | bytes 3145736 | tf_op jit(solution)/shard_map/ppermute | solution.py:21
  22.4 45.2 %collective-permute-start = (bf16[128,2048]{1,0:T(8,128)(2,1)}, bf16[128,2048]{1,0:T(8,128)(2,1)S(1)}, u32[]{:S(2)}, u32[]{:S(2)}) collective-permute-start(bf16[128,2048]{1,0:T(8,128)(2,1)} %param.7), channel_id=1, source_target_pairs={{0,2},{2,4},{4,6},{6,0},{1,3},{3,5},{5,7},{7,1},{8,10},{10,12},{12... | collective-permute-start | bytes 1572872 | tf_op jit(solution)/shard_map/ppermute | solution.py:21
  24.0 46.4 %collective-permute-start.1 = (bf16[128,2048]{1,0:T(8,128)(2,1)}, bf16[128,2048]{1,0:T(8,128)(2,1)S(1)}, u32[]{:S(2)}, u32[]{:S(2)}) collective-permute-start(bf16[128,2048]{1,0:T(8,128)(2,1)} %param.7), channel_id=1, source_target_pairs={{0,6},{2,0},{4,2},{6,4},{1,7},{3,1},{5,3},{7,5},{8,14},{10,8},{12,... | collective-permute-start | bytes 1572872 | tf_op jit(solution)/shard_map/ppermute | solution.py:21
  46.4 33.0 %collective-permute-start.2 = (bf16[128,2048]{1,0:T(8,128)(2,1)}, bf16[128,2048]{1,0:T(8,128)(2,1)}, u32[]{:S(2)}, u32[]{:S(2)}) collective-permute-start(bf16[128,2048]{1,0:T(8,128)(2,1)} %param.7), channel_id=1, source_target_pairs={{0,4},{2,6},{4,0},{6,2},{1,5},{3,7},{5,1},{7,3},{8,12},{10,14},{12... | collective-permute-start | bytes 1572872 | tf_op jit(solution)/shard_map/ppermute | solution.py:21
  49.6 33.7 %collective-permute-start.13 = (bf16[2,64,2048]{2,1,0:T(8,128)(2,1)}, bf16[2,64,2048]{2,1,0:T(8,128)(2,1)}, u32[]{:S(2)}, u32[]{:S(2)}) collective-permute-start(bf16[2,64,2048]{2,1,0:T(8,128)(2,1)} %slice.76), channel_id=1, source_target_pairs={{0,2},{2,4},{4,6},{6,0},{1,3},{3,5},{5,7},{7,1},{8,10},{10,12},{12... | collective-permute-start | bytes 1572872 | tf_op jit(solution)/shard_map/ppermute | solution.py:21
  71.2 29.1 %collective-permute-start.16 = (bf16[2,128,2048]{2,1,0:T(8,128)(2,1)S(1)}, bf16[2,128,2048]{2,1,0:T(8,128)(2,1)}, u32[]{:S(2)}, u32[]{:S(2)}) collective-permute-start(bf16[2,128,2048]{2,1,0:T(8,128)(2,1)S(1)} %collective-permute-done.11.refs_1_), channel_id=1, source_target_pairs={{0,1},{1,0},{2,3},{3,2},{4,5},{5,4},{6,7},{7,6},{8,9},{9,8},{10,11... | collective-permute-start | bytes 3145736 | tf_op jit(solution)/shard_map/ppermute | solution.py:21
  72.1 25.7 %all-to-all-start = ((bf16[8,64,512]{2,1,0:T(8,128)(2,1)}), bf16[8,64,512]{2,1,0:T(8,128)(2,1)}, u32[]{:S(2)}, u32[]{:S(2)}) async-start(bf16[8,64,512]{2,1,0:T(8,128)(2,1)} %broadcast_in_dim.7), calls=%async_computation | async-start | bytes 1048576 | tf_op jit(solution)/shard_map/all_to_all | solution.py:58
  79.4 152.5 %reduce-scatter.2.cloned.1.call-start = ((), (), s32[]{:S(2)}) async-start(), calls=%async_computation.6 | async-start | bytes 2359296 | tf_op jit(solution)/shard_map/reduce_scatter | solution.py:316
  79.5 21.8 %collective-permute-start.17 = (bf16[2,128,2048]{2,1,0:T(8,128)(2,1)S(1)}, bf16[2,128,2048]{2,1,0:T(8,128)(2,1)}, u32[]{:S(2)}, u32[]{:S(2)}) collective-permute-start(bf16[2,128,2048]{2,1,0:T(8,128)(2,1)S(1)} %collective-permute-done.12.refs_2_), channel_id=1, source_target_pairs={{0,1},{1,0},{2,3},{3,2},{4,5},{5,4},{6,7},{7,6},{8,9},{9,8},{10,11... | collective-permute-start | bytes 3145736 | tf_op jit(solution)/shard_map/ppermute | solution.py:21
  83.0 60.1 %collective-permute-start.3 = (bf16[1,512,2048]{2,1,0:T(8,128)(2,1)}, bf16[1,512,2048]{2,1,0:T(8,128)(2,1)}, u32[]{:S(2)}, u32[]{:S(2)}) collective-permute-start(bf16[1,512,2048]{2,1,0:T(8,128)(2,1)} %maximum_bitcast_fusion.refs_0_), channel_id=1, source_target_pairs={{0,1},{1,0},{2,3},{3,2},{4,5},{5,4},{6,7},{7,6},{8,9},{9,8},{10,11... | collective-permute-start | bytes 6291464 | tf_op jit(solution)/shard_map/ppermute | solution.py:21
  97.7 26.6 %collective-permute-start.4 = (bf16[8,64,512]{2,1,0:T(8,128)(2,1)}, bf16[8,64,512]{2,1,0:T(8,128)(2,1)}, u32[]{:S(2)}, u32[]{:S(2)}) collective-permute-start(bf16[8,64,512]{2,1,0:T(8,128)(2,1)} %all-to-all-done.refs_2_.refs_10_), channel_id=1, source_target_pairs={{0,8},{8,16},{16,24},{24,0},{1,9},{9,17},{17,25},{25,1},{2,10},{10... | collective-permute-start | bytes 1572872 | tf_op jit(solution)/shard_map/ppermute | solution.py:21
  98.3 26.1 %collective-permute-start.5 = (bf16[8,64,512]{2,1,0:T(8,128)(2,1)}, bf16[8,64,512]{2,1,0:T(8,128)(2,1)}, u32[]{:S(2)}, u32[]{:S(2)}) collective-permute-start(bf16[8,64,512]{2,1,0:T(8,128)(2,1)} %all-to-all-done.refs_2_.refs_10_), channel_id=1, source_target_pairs={{0,16},{8,24},{16,0},{24,8},{1,17},{9,25},{17,1},{25,9},{2,18},{10... | collective-permute-start | bytes 1572872 | tf_op jit(solution)/shard_map/ppermute | solution.py:21
  100.4 24.5 %collective-permute-start.6 = (bf16[8,64,512]{2,1,0:T(8,128)(2,1)}, bf16[8,64,512]{2,1,0:T(8,128)(2,1)S(1)}, u32[]{:S(2)}, u32[]{:S(2)}) collective-permute-start(bf16[8,64,512]{2,1,0:T(8,128)(2,1)} %all-to-all-done.refs_2_.refs_10_), channel_id=1, source_target_pairs={{0,24},{8,0},{16,8},{24,16},{1,25},{9,1},{17,9},{25,17},{2,26},{10... | collective-permute-start | bytes 1572872 | tf_op jit(solution)/shard_map/ppermute | solution.py:21
  142.9 44.4 %collective-permute-start.20 = (bf16[512,2048]{1,0:T(8,128)(2,1)}, bf16[512,2048]{1,0:T(8,128)(2,1)}, u32[]{:S(2)}, u32[]{:S(2)}) collective-permute-start(bf16[512,2048]{1,0:T(8,128)(2,1)} %get-tuple-element.15), channel_id=1, source_target_pairs={{0,1},{1,0},{2,3},{3,2},{4,5},{5,4},{6,7},{7,6},{8,9},{9,8},{10,11... | collective-permute-start | bytes 6291464 | tf_op jit(solution)/shard_map/ppermute | solution.py:21
  151.6 44.0 %collective-permute-start.7 = (bf16[512,2048]{1,0:T(8,128)(2,1)}, bf16[512,2048]{1,0:T(8,128)(2,1)}, u32[]{:S(2)}, u32[]{:S(2)}) collective-permute-start(bf16[512,2048]{1,0:T(8,128)(2,1)} %get-tuple-element.12), channel_id=1, source_target_pairs={{0,1},{1,0},{2,3},{3,2},{4,5},{5,4},{6,7},{7,6},{8,9},{9,8},{10,11... | collective-permute-start | bytes 6291464 | tf_op jit(solution)/shard_map/ppermute | solution.py:21
  152.1 30.4 %all-to-all-start.2 = ((bf16[4,8,64,512]{3,2,1,0:T(8,128)(2,1)}), bf16[4,8,64,512]{3,2,1,0:T(8,128)(2,1)S(1)}, u32[]{:S(2)}, u32[]{:S(2)}) async-start(bf16[4,8,64,512]{3,2,1,0:T(8,128)(2,1)} %get-tuple-element.17), calls=%async_computation.3 | async-start | bytes 4194304 | tf_op jit(solution)/shard_map/all_to_all | solution.py:62
  190.8 36.9 %collective-permute-start.21 = (bf16[128,2048]{1,0:T(8,128)(2,1)}, bf16[128,2048]{1,0:T(8,128)(2,1)}, u32[]{:S(2)}, u32[]{:S(2)}) collective-permute-start(bf16[128,2048]{1,0:T(8,128)(2,1)} %get-tuple-element.18), channel_id=1, source_target_pairs={{0,2},{2,4},{4,6},{6,0},{1,3},{3,5},{5,7},{7,1},{8,10},{10,12},{12... | collective-permute-start | bytes 1572872 | tf_op jit(solution)/shard_map/ppermute | solution.py:21
  192.8 36.2 %collective-permute-start.22 = (bf16[128,2048]{1,0:T(8,128)(2,1)}, bf16[128,2048]{1,0:T(8,128)(2,1)}, u32[]{:S(2)}, u32[]{:S(2)}) collective-permute-start(bf16[128,2048]{1,0:T(8,128)(2,1)} %get-tuple-element.20), channel_id=1, source_target_pairs={{0,6},{2,0},{4,2},{6,4},{1,7},{3,1},{5,3},{7,5},{8,14},{10,8},{12,... | collective-permute-start | bytes 1572872 | tf_op jit(solution)/shard_map/ppermute | solution.py:21
  192.8 36.2 %collective-permute-start.23 = (bf16[128,2048]{1,0:T(8,128)(2,1)}, bf16[128,2048]{1,0:T(8,128)(2,1)}, u32[]{:S(2)}, u32[]{:S(2)}) collective-permute-start(bf16[128,2048]{1,0:T(8,128)(2,1)} %get-tuple-element.19), channel_id=1, source_target_pairs={{0,4},{2,6},{4,0},{6,2},{1,5},{3,7},{5,1},{7,3},{8,12},{10,14},{12... | collective-permute-start | bytes 1572872 | tf_op jit(solution)/shard_map/ppermute | solution.py:21
  198.5 37.1 %collective-permute-start.10 = (bf16[128,2048]{1,0:T(8,128)(2,1)}, bf16[128,2048]{1,0:T(8,128)(2,1)}, u32[]{:S(2)}, u32[]{:S(2)}) collective-permute-start(bf16[128,2048]{1,0:T(8,128)(2,1)} %get-tuple-element.22), channel_id=1, source_target_pairs={{0,4},{2,6},{4,0},{6,2},{1,5},{3,7},{5,1},{7,3},{8,12},{10,14},{12... | collective-permute-start | bytes 1572872 | tf_op jit(solution)/shard_map/ppermute | solution.py:21
  199.3 38.3 %collective-permute-start.8 = (bf16[128,2048]{1,0:T(8,128)(2,1)}, bf16[128,2048]{1,0:T(8,128)(2,1)}, u32[]{:S(2)}, u32[]{:S(2)}) collective-permute-start(bf16[128,2048]{1,0:T(8,128)(2,1)} %get-tuple-element.21), channel_id=1, source_target_pairs={{0,2},{2,4},{4,6},{6,0},{1,3},{3,5},{5,7},{7,1},{8,10},{10,12},{12... | collective-permute-start | bytes 1572872 | tf_op jit(solution)/shard_map/ppermute | solution.py:21
  (20 other events, 321.9 us)
Sparse Core Ops, SparseCore 0:
  19.1 41.9 all-gather.1
  143.0 38.7 reduce-scatter.1

commit v7 on v6

v7 whole, which is shorter than its diff:
```python
import math

import jax
import jax.numpy as jnp
from jax import lax
from jax.experimental import pallas as pl
from jax.experimental.pallas import tpu as pltpu
from jax.sharding import Mesh
from jax.sharding import PartitionSpec as P


FS = ("z", "x")
ALL = ("z", "x", "y", "c")
F32 = jnp.float32
BF16 = jnp.bfloat16
TILE = 512


def shift(x, axis, by):
    n = lax.axis_size(axis)
    return lax.ppermute(x, axis, [(i, (i + by) % n) for i in range(n)])


def gather_tokens(arrays):
    own = jnp.stack(arrays)
    half = own.shape[1] // 2
    behind, ahead = shift(own, "y", 1), shift(own, "y", -1)
    far_lo, far_hi = shift(behind[:, :half], "y", 1), shift(ahead[:, half:], "y", -1)
    pieces = (own, behind, ahead, far_lo, far_hi)
    partners = []
    for piece in pieces:
        partners.append(shift(piece, "c", 1))
    return (*pieces, *partners)


def gather_later(own):
    behind, ahead, far = (shift(own, "y", by) for by in (1, -1, 2))
    mine = jnp.concatenate((own, behind, ahead, far), axis=0)[None]
    return mine, shift(mine, "c", 1)


def plus(a, b):
    return (a.astype(F32) + b.astype(F32)).astype(BF16)


def scatter_tokens(mine, partners):
    partners = shift(partners, "c", 1)
    rows = mine.shape[0] // 4
    at = [slice(i * rows, (i + 1) * rows) for i in range(4)]
    behind, ahead, far = (plus(mine[i], partners[i]) for i in at[1:])
    arrived = (shift(ahead, "y", 1), shift(behind, "y", -1), shift(far, "y", 2))
    total = mine[at[0]].astype(F32) + partners[at[0]].astype(F32)
    return sum((a.astype(F32) for a in arrived), total).astype(BF16)


def gather(x, axis):
    n = lax.axis_size(axis)
    return lax.all_to_all(jnp.broadcast_to(x[None], (n, *x.shape)), axis, 0, 0, tiled=True)


def exchange_sum(term, axis):
    tiles = lax.all_to_all(term, axis, 0, 0, tiled=True)
    return jnp.sum(tiles.astype(F32), axis=0)


def hop_sum(term, axis):
    n = lax.axis_size(axis)
    me = lax.axis_index(axis)

    def block(by):
        at = (me + by) & (n - 1)
        start = (at, *(0 for _ in term.shape[1:]))
        part = lax.dynamic_slice(term, start, (1, *term.shape[1:]), allow_negative_indices=False)
        return part[0]

    arrived = [shift(block(by), axis, by) for by in range(1, n)]
    return sum((a.astype(F32) for a in arrived), block(0).astype(F32))


def rows_times(left, right):
    return lax.dot_general(left, right, (((1,), (1,)), ((), ())), preferred_element_type=F32)


def over_tokens(left, right):
    return lax.dot_general(left, right, (((0,), (0,)), ((), ())), preferred_element_type=F32)


def copies(sources, target, sems, index):
    waits, row = [], 0
    for i, source in enumerate(sources):
        rows = source.shape[1]
        copy = pltpu.make_async_copy(source.at[index], target.at[pl.ds(row, rows)], sems.at[i])
        copy.start()
        waits.append((row, copy))
        row += rows
    return waits


def settle(waits, upto):
    while waits and waits[0][0] < upto:
        waits.pop(0)[1].wait()


def relu_times(rows, weight):
    return jnp.maximum(jnp.dot(rows, weight, preferred_element_type=F32), 0.0)


def place_weights(first, parts, target, col, width, sems):
    n = len(parts)
    pairs = [(first.at[:, :, :, pl.ds(col, width)], target.at[:, :, :, pl.ds(0, width)])]
    for k, part in enumerate(parts):
        at = (lax.axis_index("x") + (n - k)) & (n - 1)
        pairs.append((part.at[:, :, pl.ds(col, width)], target.at[:, at, :, pl.ds(width, width)]))
    waits = [pltpu.make_async_copy(a, b, sems.at[i]) for i, (a, b) in enumerate(pairs)]
    for copy in waits:
        copy.start()
    return waits


def half_products(pieces, weight_copies, saved, cot, weight, hid, pg, pg_out, store, flush, in_sems, sem):
    for copy in weight_copies:
        copy.start()
    saved_waits = copies(pieces, saved, in_sems.at[0], 0)
    cot_waits = copies(pieces, cot, in_sems.at[1], 1)
    for copy in weight_copies:
        copy.wait()
    width = hid.shape[1]
    both = weight[...].reshape(-1, 2 * width)
    for t in range(0, saved.shape[0], TILE):
        at = pl.ds(t, TILE)
        settle(saved_waits, t + TILE)
        r = relu_times(saved[at], both[:, :width])
        hid[at] = (r * r).astype(BF16)
        settle(cot_waits, t + TILE)
        grad = jnp.dot(cot[at], both[:, width:], preferred_element_type=F32)
        pg[at] = (2.0 * r * grad).astype(BF16)
    nz, block = weight.shape[0], weight.shape[1] * weight.shape[2]

    def terms(first, last):
        @pl.loop(first, last)
        def _(i):
            at = pl.ds(pl.multiple_of(i * block, block), block)
            store(i, 0, over_tokens(saved[:, at], pg[...]).astype(BF16))
            store(i, width, over_tokens(cot[:, at], hid[...]).astype(BF16))

        return flush(first, last)

    early = terms(0, nz * 3 // 4)
    pg_copy = pltpu.make_async_copy(pg, pg_out, sem)
    pg_copy.start()
    early.start()
    late = terms(nz * 3 // 4, nz)
    late.start()
    for copy in (pg_copy, early, late):
        copy.wait()


def first_kernel(*refs):
    pieces, (w, out, pg_out) = refs[:10], refs[10:13]
    saved, cot, weight, hid, pg, term, in_sems, sems = refs[13:]
    block = weight.shape[1] * weight.shape[2]

    def store(i, col, value):
        rows = pl.ds(pl.multiple_of(i * block, block), block)
        term[rows, col : col + value.shape[1]] = value

    def flush(first, last):
        rows = pl.ds(first * block, (last - first) * block)
        return pltpu.make_async_copy(term.at[rows], out.at[rows], sems.at[2 if first else 1])

    weight_copies = [pltpu.make_async_copy(w, weight, sems.at[0])]
    half_products(
        pieces, weight_copies, saved, cot, weight, hid, pg, pg_out, store, flush, in_sems, sems.at[3]
    )


def second_kernel(*refs):
    pieces, parts, (out, pg_out) = refs[:10], refs[10:14], refs[14:16]
    saved, cot, weight, hid, pg, term, in_sems, w_sems, sems = refs[16:]
    nx, _, part = term.shape[:3]

    def store(i, col, value):
        for j in range(nx):
            term[j, i, :, col : col + value.shape[1]] = value[j * part : (j + 1) * part]

    def flush(first, last):
        at = pl.ds(first, last - first)
        return pltpu.make_async_copy(term.at[:, at], out.at[:, at], sems.at[2 if first else 1])

    weight_copies = []
    for k, piece in enumerate(parts):
        at = (lax.axis_index("x") + (nx - k)) & (nx - 1)
        weight_copies.append(pltpu.make_async_copy(piece, weight.at[:, at], w_sems.at[k]))
    half_products(
        pieces, weight_copies, saved, cot, weight, hid, pg, pg_out, store, flush, in_sems, sems.at[3]
    )


def rows_kernel(*refs):
    (pg_a, pg_b, first), parts, (mine_out, theirs_out) = refs[:3], refs[3:7], refs[7:9]
    pg, up, mine, theirs, w_sems, sems = refs[9:]
    width = pg.shape[1] // 2
    a = pltpu.make_async_copy(pg_a, pg.at[:, pl.ds(0, width)], sems.at[0])
    b = pltpu.make_async_copy(pg_b, pg.at[:, pl.ds(width, width)], sems.at[1])
    a.start()
    b.start()
    waits = place_weights(first, parts, up, 0, width, w_sems)
    for copy in (a, b, *waits):
        copy.wait()
    mine_copy = pltpu.make_async_copy(mine, mine_out, sems.at[2])
    theirs_copy = pltpu.make_async_copy(theirs, theirs_out, sems.at[3])
    outputs(pg, mine.shape[0], up, theirs)
    outputs(pg, 0, up, mine, theirs_copy)
    mine_copy.start()
    theirs_copy.wait()
    mine_copy.wait()


def flat_rows(weight, first, count):
    each = weight.shape[1] * weight.shape[2]
    return weight[first // each : (first + count) // each].reshape(count, weight.shape[-1])


def outputs(hidden, first, weight, out, copy=None):
    rows = hidden[pl.ds(first, out.shape[0])]
    for n in range(0, out.shape[1], 512):
        out[:, n : n + 512] = rows_times(rows, flat_rows(weight, n, 512)).astype(BF16)
        if copy is not None and n == 512:
            copy.start()


def ahead_kernel(*refs):
    pieces, first, parts, (mine_out, theirs_out) = refs[:2], refs[2], refs[3:7], refs[7:9]
    rows, up, down, hid, mine, theirs, in_sems, w_sems, sems = refs[9:]
    width = hid.shape[1] // 2
    up_waits = place_weights(first, parts, up, 0, width, w_sems.at[0])
    waits = copies(pieces, rows, in_sems, 0)
    down_waits = place_weights(first, parts, down, width, width, w_sems.at[1])
    for copy in up_waits:
        copy.wait()
    weight = up[...].reshape(-1, 2 * width)
    for t in range(0, rows.shape[0], TILE):
        settle(waits, t + TILE)
        at = pl.ds(t, TILE)
        r = relu_times(rows[at], weight)
        hid[at] = (r * r).astype(BF16)
    for copy in down_waits:
        copy.wait()
    mine_copy = pltpu.make_async_copy(mine, mine_out, sems.at[0])
    theirs_copy = pltpu.make_async_copy(theirs, theirs_out, sems.at[1])
    outputs(hid, mine.shape[0], down, theirs)
    outputs(hid, 0, down, mine, theirs_copy)
    mine_copy.start()
    theirs_copy.wait()
    mine_copy.wait()


def call(kernel, operands, outs, scratch, flops):
    hbm = pl.BlockSpec(memory_space=pltpu.HBM)
    return pl.pallas_call(
        kernel,
        out_shape=[jax.ShapeDtypeStruct(*s) for s in outs],
        in_specs=[hbm] * len(operands),
        out_specs=[hbm] * len(outs),
        scratch_shapes=[pltpu.VMEM(*s) for s in scratch[0]]
        + [pltpu.SemaphoreType.DMA(s) for s in scratch[1]],
        cost_estimate=pl.CostEstimate(flops=flops, bytes_accessed=12 << 20, transcendentals=0),
        compiler_params=pltpu.CompilerParams(vmem_limit_bytes=60 * 1024 * 1024),
    )(*operands)


def products(pieces, later, first, parts):
    rows = sum(p.shape[1] for p in pieces)
    nz, nx, part, cols = first.shape
    depth, width = nz * nx * part, cols // 2
    n = len(pieces)
    flops = 2 * rows * depth * cols
    group, wide = ((rows, depth), BF16), ((rows, cols), BF16)
    split, swapped, flat = (
        ((nz, nx, part, cols), BF16),
        ((nx, nz, part, cols), BF16),
        ((depth, cols), BF16),
    )
    narrow, half = ((rows, width), BF16), ((rows // 2, depth), BF16)

    def one():
        scratch = (group, group, split, narrow, narrow, flat), ((2, n), (4,))
        return call(first_kernel, (*pieces, first), (flat, narrow), scratch, 2 * flops)

    def two():
        scratch = (group, group, split, narrow, narrow, swapped), ((2, n), (nx,), (4,))
        return call(second_kernel, (*pieces, *parts), (swapped, narrow), scratch, 2 * flops)

    def row_grad(pg_a, pg_b):
        scratch = (wide, split, half, half), ((nx + 1,), (4,))
        return call(rows_kernel, (pg_a, pg_b, first, *parts), (half, half), scratch, flops)

    def ahead():
        scratch = (group, split, split, wide, half, half), ((2,), (2, nx + 1), (2,))
        return call(ahead_kernel, (*later, first, *parts), (half, half), scratch, 2 * flops)

    return one, two, row_grad, ahead


def body(later_rows, earlier_rows, cotangent, up_weight, down_weight, up_total, down_total):
    n_dev = math.prod(lax.axis_size(a) for a in ALL)
    nz, nx = lax.axis_size("z"), lax.axis_size("x")
    factor = 1.0 / math.sqrt(later_rows.shape[0] * n_dev)
    width = up_weight.shape[1] // 2
    low = jnp.concatenate((up_weight[:, :width], down_weight[:, :width]), axis=1)
    high = jnp.concatenate((up_weight[:, width:], down_weight[:, width:]), axis=1)
    low = gather(low, "x").reshape(-1, low.shape[1])
    low = lax.all_gather(low, "z", axis=0, tiled=True).reshape(nz, nx, *high.shape)
    high = gather(high, "z")
    high = (high, *(shift(high, "x", by) for by in range(1, nx)))
    pieces = gather_tokens((earlier_rows, cotangent))
    later = gather_later(later_rows)
    one, two, row_grad, ahead = products(pieces, later, low, high)
    low_terms, low_pg = one()
    low_terms = lax.psum_scatter(low_terms, "z", scatter_dimension=0, tiled=True)
    high_terms, high_pg = two()
    high_terms = exchange_sum(high_terms, "x").astype(BF16)
    mine, theirs = row_grad(low_pg, high_pg)
    earlier_grad = scatter_tokens(mine, theirs)
    high_terms = exchange_sum(high_terms, "z")
    mine, theirs = ahead()
    later_out = scatter_tokens(mine, theirs)
    low_terms = hop_sum(low_terms.reshape(-1, *up_weight.shape), "x")
    up_term = jnp.concatenate((low_terms[:, :width], high_terms[:, :width]), axis=1)
    down_term = jnp.concatenate((low_terms[:, width:], high_terms[:, width:]), axis=1)
    up_updated = up_total + up_term * factor
    down_updated = down_total + down_term * factor
    return later_out, earlier_grad, up_updated, down_updated


def solution(mesh):
    n_tp = mesh.shape["tp"]
    finer = Mesh(mesh.devices.reshape(8, 4, n_tp // 2, 2), ALL)
    rows, weight = P(ALL, None), P(FS, ("y", "c"))
    return jax.shard_map(
        body,
        mesh=finer,
        in_specs=(rows, rows, rows, weight, weight, weight, weight),
        out_specs=(rows, rows, weight, weight),
        check_vma=False,
    )
```

time: 251 us -> 247 us (0.984)
  waiting for transfers between devices: 119 us -> 75.1 us
  starting transfers between devices: 43.1 us -> 77.5 us
  Pallas kernels: 37.2 us -> 43 us
    ppermute x27, starting transfers between devices: 28.3 us -> 58.7 us  [shift(): return lax.ppermute(x, axis, [(i, (i + by) % n) for i in range(n)])]
    ppermute x27, waiting for transfers between devices: 75.6 us -> 51.4 us  [shift(): return lax.ppermute(x, axis, [(i, (i + by) % n) for i in range(n)])]
    all_to_all x1, waiting for transfers between devices: 13.9 us -> 0.01 us  [gather(): lax.all_to_all(jnp.broadcast_to(x[None], (n, *x.shape)), axis, 0, 0, tile...]
    pallas_call x4, Pallas kernels: 37.2 us -> 43 us  [call(): pl.pallas_call(kernel, out_shape=[jax.ShapeDtypeStruct(*s) for s in outs]...]
    all_to_all x2, waiting for transfers between devices: 29.3 us -> 23.6 us  [exchange_sum(): tiles = lax.all_to_all(term, axis, 0, 0, tiled=True)]
    all_to_all x2, starting transfers between devices: 7.37 us -> 10.3 us  [exchange_sum(): tiles = lax.all_to_all(term, axis, 0, 0, tiled=True)]
  transfers between devices with their start and end apart: 32 -> 32, of which waited for: 10 -> 9; matrix products, arithmetic and copies ran while one was open for 9% -> 8% of each run, Pallas kernels for 15% -> 18%
where the time goes in v7:
time: 247 us; the launch traced here: 245 us
  starting transfers between devices  77.5 us (31%)
  waiting for transfers between devices  75.1 us (30%)
  Pallas kernels  43 us (17%)
  other arithmetic  18 us (7%)
  between operations  14.3 us (6%)
  blocking collectives  10.9 us (4%)
  local copies, waits for them, and re-layouts  6.64 us (3%)
    ppermute x27, starting transfers between devices, shift(): return lax.ppermute(x, axis, [(i, (i + by) % n) for i in range(n)])  58.7 us
    ppermute x27, waiting for transfers between devices, shift(): return lax.ppermute(x, axis, [(i, (i + by) % n) for i in range(n)])  51.4 us
    pallas_call x4, Pallas kernels, call(): pl.pallas_call(kernel, out_shape=[jax.ShapeDtypeStruct(*s) for s in outs]...  43 us
    all_to_all x2, waiting for transfers between devices, exchange_sum(): tiles = lax.all_to_all(term, axis, 0, 0, tiled=True)  23.6 us
    all_to_all x1, blocking collectives, gather(): lax.all_to_all(jnp.broadcast_to(x[None], (n, *x.shape)), axis, 0, 0, tile...  10.9 us
    all_to_all x2, starting transfers between devices, exchange_sum(): tiles = lax.all_to_all(term, axis, 0, 0, tiled=True)  10.3 us
    all_to_all x1, starting transfers between devices, gather(): lax.all_to_all(jnp.broadcast_to(x[None], (n, *x.shape)), axis, 0, 0, tile...  8.47 us
    convert_element_type x2, other arithmetic, plus(): return (a.astype(F32) + b.astype(F32)).astype(BF16)  5.31 us
  transfers between devices with their start and end apart: 32, of which 9 were waited for; matrix products, arithmetic and copies ran while one was open for 8% of the time, Pallas kernels for 18%

profile of v7, /device:TPU:8, one launch (start us, length us, event | category | flops | bytes accessed | tf_op | source)
XLA Modules:
  0.0 245.3 jit_solution(9209732107586577852)
XLA Ops:
  8.1 10.9 %all_to_all.20 = bf16[4,64,512]{2,1,0:T(8,128)(2,1)} all-to-all(bf16[4,64,512]{2,1,0:T(8,128)(2,1)S(1)} %broadcast_in_dim.7), channel_id=1, replica_groups=mesh['z'=8,'x'=4,'y'=4,'c'=2] {'x'}, dimensions={0} | all-to-all | bytes 524288 | tf_op jit(solution)/shard_map/all_to_all | solution.py:58
  22.8 8.5 %all-to-all-start.1 = ((bf16[8,64,512]{2,1,0:T(8,128)(2,1)}), bf16[8,64,512]{2,1,0:T(8,128)(2,1)S(1)}, u32[]{:S(2)}, u32[]{:S(2)}) async-start(bf16[8,64,512]{2,1,0:T(8,128)(2,1)} %broadcast_in_dim.8), calls=%async_computation.1 | async-start | bytes 1048576 | tf_op jit(solution)/shard_map/all_to_all | solution.py:58
  33.8 21.4 %collective-permute-done = bf16[128,2048]{1,0:T(8,128)(2,1)S(1)} collective-permute-done((bf16[128,2048]{1,0:T(8,128)(2,1)S(1)}, bf16[128,2048]{1,0:T(8,128)(2,1)S(1)}, u32[]{:S(2)}, u32[]{:S(2)}) %collective-permute-start) | collective-permute-done | bytes 524320 | tf_op jit(solution)/shard_map/ppermute | solution.py:21
  57.5 10.4 %collective-permute-done.1 = bf16[128,2048]{1,0:T(8,128)(2,1)S(1)} collective-permute-done((bf16[128,2048]{1,0:T(8,128)(2,1)S(1)}, bf16[128,2048]{1,0:T(8,128)(2,1)S(1)}, u32[]{:S(2)}, u32[]{:S(2)}) %collective-permute-start.1) | collective-permute-done | bytes 524320 | tf_op jit(solution)/shard_map/ppermute | solution.py:21
  73.5 4.1 %collective-permute-done.2 = bf16[128,2048]{1,0:T(8,128)(2,1)} collective-permute-done((bf16[128,2048]{1,0:T(8,128)(2,1)S(1)}, bf16[128,2048]{1,0:T(8,128)(2,1)}, u32[]{:S(2)}, u32[]{:S(2)}) %collective-permute-start.2) | collective-permute-done | bytes 524320 | tf_op jit(solution)/shard_map/ppermute | solution.py:21
  77.6 5.1 %collective-permute-start.14 = (bf16[2,64,2048]{2,1,0:T(8,128)(2,1)S(1)}, bf16[2,64,2048]{2,1,0:T(8,128)(2,1)S(1)}, u32[]{:S(2)}, u32[]{:S(2)}) collective-permute-start(bf16[2,64,2048]{2,1,0:T(8,128)(2,1)S(1)} %slice.109), channel_id=1, source_target_pairs={{0,6},{2,0},{4,2},{6,4},{1,7},{3,1},{5,3},{7,5},{8,14},{10,8},{12,... | collective-permute-start | bytes 1572872 | tf_op jit(solution)/shard_map/ppermute | solution.py:21
  82.7 6.2 %collective-permute-done.4.refs_4_.refs_11_ = bf16[8,64,512]{2,1,0:T(8,128)(2,1)S(1)} collective-permute-done((bf16[8,64,512]{2,1,0:T(8,128)(2,1)S(1)}, bf16[8,64,512]{2,1,0:T(8,128)(2,1)S(1)}, u32[]{:S(2)}, u32[]{:S(2)}) %collective-permute-start.4) | collective-permute-done | bytes 524320 | tf_op jit(solution)/shard_map/ppermute | solution.py:21
  90.2 2.6 %maximum_bitcast_fusion.refs_0_ = bf16[1,512,2048]{2,1,0:T(8,128)(2,1)} fusion(bf16[128,2048]{1,0:T(8,128)(2,1)} %collective-permute-done.2, bf16[128,2048]{1,0:T(8,128)(2,1)S(1)} %collective-permute-done.1, bf16[128,2048]{1,0:T(8,128)(2,1)S(1)} %collective-permute-done, bf16[128,2048]{1,0:T(8,128)(2,1)S(1)} %copy-done.3), kind=kLoop, calls=%fused_computation | loop fusion | flops 8388608 | bytes 4194304 | tf_op jit(solution)/shard_map/broadcast_in_dim | solution.py:38
  93.8 4.2 %collective-permute-done.18.refs_8_ = bf16[2,64,2048]{2,1,0:T(8,128)(2,1)S(1)} collective-permute-done((bf16[2,64,2048]{2,1,0:T(8,128)(2,1)S(1)}, bf16[2,64,2048]{2,1,0:T(8,128)(2,1)S(1)}, u32[]{:S(2)}, u32[]{:S(2)}) %collective-permute-start.18) | collective-permute-done | bytes 524320 | tf_op jit(solution)/shard_map/ppermute | solution.py:21
  99.5 14.3 %shard_map.104 = (bf16[4,8,64,512]{3,2,1,0:T(8,128)(2,1)}, bf16[1024,256]{1,0:T(8,128)(2,1)}) custom-call(bf16[2,128,2048]{2,1,0:T(8,128)(2,1)} %copy-done.1, bf16[2,128,2048]{2,1,0:T(8,128)(2,1)} %collective-permute-done.11.refs_1_, bf16[2,128,2048]{2,1,0:T(8,128)(2,1)} %collective-permute-done.12.refs_2_, bf16[2,64,2048]{2,1,0:T(8,128)(2,1)} %copy-done.9, ...), custom_call_target="tpu_custom_call" | custom-call | flops 4294967296 | bytes 12582912 | tf_op jit(solution)/shard_map/pallas_call | solution.py:260
  113.8 3.6 %all-to-all-start.2 = ((bf16[4,8,64,512]{3,2,1,0:T(8,128)(2,1)}), bf16[4,8,64,512]{3,2,1,0:T(8,128)(2,1)S(1)}, u32[]{:S(2)}, u32[]{:S(2)}) async-start(bf16[4,8,64,512]{3,2,1,0:T(8,128)(2,1)} %get-tuple-element.19), calls=%async_computation.3 | async-start | bytes 4194304 | tf_op jit(solution)/shard_map/all_to_all | solution.py:62
  117.5 14.4 %shard_map.103 = (bf16[2048,512]{1,0:T(8,128)(2,1)}, bf16[1024,256]{1,0:T(8,128)(2,1)}) custom-call(bf16[2,128,2048]{2,1,0:T(8,128)(2,1)} %copy-done.1, bf16[2,128,2048]{2,1,0:T(8,128)(2,1)} %collective-permute-done.11.refs_1_, bf16[2,128,2048]{2,1,0:T(8,128)(2,1)} %collective-permute-done.12.refs_2_, bf16[2,64,2048]{2,1,0:T(8,128)(2,1)} %copy-done.9, ...), custom_call_target="tpu_custom_call" | custom-call | flops 4294967296 | bytes 12582912 | tf_op jit(solution)/shard_map/pallas_call | solution.py:260
  132.0 5.7 %shard_map.105 = (bf16[512,2048]{1,0:T(8,128)(2,1)}, bf16[512,2048]{1,0:T(8,128)(2,1)}) custom-call(bf16[1024,256]{1,0:T(8,128)(2,1)} %get-tuple-element.14.refs_0_, bf16[1024,256]{1,0:T(8,128)(2,1)} %get-tuple-element.15.refs_1_, bf16[8,4,64,512]{3,2,1,0:T(8,128)(2,1)} %bitcast.22, bf16[8,64,512]{2,1,0:T(8,128)(2,1)} %copy-done.2, ...), custom_call_target="tpu_custom_call" | custom-call | flops 2147483648 | bytes 12582912 | tf_op jit(solution)/shard_map/pallas_call | solution.py:260
  138.1 8.6 %shard_map.102 = (bf16[512,2048]{1,0:T(8,128)(2,1)}, bf16[512,2048]{1,0:T(8,128)(2,1)}) custom-call(bf16[1,512,2048]{2,1,0:T(8,128)(2,1)} %maximum_bitcast_fusion.refs_0_, bf16[1,512,2048]{2,1,0:T(8,128)(2,1)} %collective-permute-done.3.refs_1_, bf16[8,4,64,512]{3,2,1,0:T(8,128)(2,1)} %bitcast.23, bf16[8,64,512]{2,1,0:T(8,128)(2,1)} %copy-done.2, ...), custom_call_target="tpu_custom_call" | custom-call | flops 4294967296 | bytes 12582912 | tf_op jit(solution)/shard_map/pallas_call | solution.py:260
  148.5 6.6 %all-to-all-start.3 = ((bf16[8,64,512]{2,1,0:T(8,128)(2,1)}), bf16[8,64,512]{2,1,0:T(8,128)(2,1)S(1)}, u32[]{:S(2)}, u32[]{:S(2)}) async-start(bf16[8,64,512]{2,1,0:T(8,128)(2,1)} %reduce_sum.21), calls=%async_computation.4 | async-start | bytes 1048576 | tf_op jit(solution)/shard_map/all_to_all | solution.py:62
  155.1 23.6 %all-to-all-done.3 = bf16[8,64,512]{2,1,0:T(8,128)(2,1)S(1)} async-done(((bf16[8,64,512]{2,1,0:T(8,128)(2,1)}), bf16[8,64,512]{2,1,0:T(8,128)(2,1)S(1)}, u32[]{:S(2)}, u32[]{:S(2)}) %all-to-all-start.3) | async-done | bytes 524320 | tf_op jit(solution)/shard_map/all_to_all | solution.py:62
  178.8 2.6 %add_convert_fusion.3 = (bf16[128,2048]{1,0:T(8,128)(2,1)S(1)}, bf16[128,2048]{1,0:T(8,128)(2,1)S(1)}, bf16[128,2048]{1,0:T(8,128)(2,1)S(1)}) fusion(bf16[512,2048]{1,0:T(8,128)(2,1)} %collective-permute-done.20, bf16[512,2048]{1,0:T(8,128)(2,1)} %get-tuple-element.16), kind=kLoop, calls=%fused_computation.6 | loop fusion | flops 3145728 | bytes 4718592 | tf_op jit(solution)/shard_map/convert_element_type | solution.py:43
  182.3 3.5 %collective-permute-start.22 = (bf16[128,2048]{1,0:T(8,128)(2,1)S(1)}, bf16[128,2048]{1,0:T(8,128)(2,1)S(1)}, u32[]{:S(2)}, u32[]{:S(2)}) collective-permute-start(bf16[128,2048]{1,0:T(8,128)(2,1)S(1)} %get-tuple-element.22), channel_id=1, source_target_pairs={{0,6},{2,0},{4,2},{6,4},{1,7},{3,1},{5,3},{7,5},{8,14},{10,8},{12,... | collective-permute-start | bytes 1572872 | tf_op jit(solution)/shard_map/ppermute | solution.py:21
  185.8 4.3 %collective-permute-start.23 = (bf16[128,2048]{1,0:T(8,128)(2,1)S(1)}, bf16[128,2048]{1,0:T(8,128)(2,1)S(1)}, u32[]{:S(2)}, u32[]{:S(2)}) collective-permute-start(bf16[128,2048]{1,0:T(8,128)(2,1)S(1)} %get-tuple-element.21), channel_id=1, source_target_pairs={{0,4},{2,6},{4,0},{6,2},{1,5},{3,7},{5,1},{7,3},{8,12},{10,14},{12... | collective-permute-start | bytes 1572872 | tf_op jit(solution)/shard_map/ppermute | solution.py:21
  190.1 2.7 %add_convert_fusion.7 = (bf16[128,2048]{1,0:T(8,128)(2,1)S(1)}, bf16[128,2048]{1,0:T(8,128)(2,1)}, bf16[128,2048]{1,0:T(8,128)(2,1)S(1)}) fusion(bf16[512,2048]{1,0:T(8,128)(2,1)} %collective-permute-done.7, bf16[512,2048]{1,0:T(8,128)(2,1)S(1)} %copy-done), kind=kLoop, calls=%fused_computation.10 | loop fusion | flops 3145728 | bytes 4718592 | tf_op jit(solution)/shard_map/convert_element_type | solution.py:43
  194.9 3.6 %collective-permute-done.21 = bf16[128,2048]{1,0:T(8,128)(2,1)S(1)} collective-permute-done((bf16[128,2048]{1,0:T(8,128)(2,1)S(1)}, bf16[128,2048]{1,0:T(8,128)(2,1)S(1)}, u32[]{:S(2)}, u32[]{:S(2)}) %collective-permute-start.21) | collective-permute-done | bytes 524320 | tf_op jit(solution)/shard_map/ppermute | solution.py:21
  198.5 24.5 %collective-permute-start.9 = (bf16[128,2048]{1,0:T(8,128)(2,1)S(1)}, bf16[128,2048]{1,0:T(8,128)(2,1)}, u32[]{:S(2)}, u32[]{:S(2)}) collective-permute-start(bf16[128,2048]{1,0:T(8,128)(2,1)S(1)} %get-tuple-element.25), channel_id=1, source_target_pairs={{0,6},{2,0},{4,2},{6,4},{1,7},{3,1},{5,3},{7,5},{8,14},{10,8},{12,... | collective-permute-start | bytes 1572872 | tf_op jit(solution)/shard_map/ppermute | solution.py:21
  228.4 2.7 %collective-permute-start.25 = (bf16[64,512]{1,0:T(8,128)(2,1)S(1)}, bf16[64,512]{1,0:T(8,128)(2,1)S(1)}, u32[]{:S(2)}, u32[]{:S(2)}) collective-permute-start(bf16[64,512]{1,0:T(8,128)(2,1)S(1)} %get-tuple-element.28), channel_id=1, source_target_pairs={{0,16},{8,24},{16,0},{24,8},{1,17},{9,25},{17,1},{25,9},{2,18},{10... | collective-permute-start | bytes 196616 | tf_op jit(solution)/shard_map/ppermute | solution.py:21
  233.4 2.7 %add_convert_fusion.4 = bf16[128,2048]{1,0:T(8,128)(2,1)} fusion(bf16[128,2048]{1,0:T(8,128)(2,1)} %collective-permute-done.10, bf16[128,2048]{1,0:T(8,128)(2,1)} %collective-permute-done.9, bf16[128,2048]{1,0:T(8,128)(2,1)} %collective-permute-done.8, bf16[512,2048]{1,0:T(8,128)(2,1)} %collective-permute-done.7, bf16[512,2048]{1,0:T(8,128)(2,1)S(1)} %copy-done), kind=kLoop, calls=%fused_computation.7 | loop fusion | flops 2621440 | bytes 3145728 | tf_op jit(solution)/shard_map/convert_element_type | solution.py:53
  (94 shorter events, 34.3 us)
Async XLA Ops:
  7.2 110.4 %all-gather.2.cloned.1.call-start = ((), (), s32[]{:S(2)}) async-start(), calls=%async_computation.5 | async-start | bytes 2359296 | tf_op jit(solution)/shard_map/all_gather | solution.py:313
  20.3 48.1 %collective-permute-start.11 = (bf16[2,128,2048]{2,1,0:T(8,128)(2,1)S(1)}, bf16[2,128,2048]{2,1,0:T(8,128)(2,1)}, u32[]{:S(2)}, u32[]{:S(2)}) collective-permute-start(bf16[2,128,2048]{2,1,0:T(8,128)(2,1)S(1)} %pad_maximum_fusion.refs_0_), channel_id=1, source_target_pairs={{0,2},{2,4},{4,6},{6,0},{1,3},{3,5},{5,7},{7,1},{8,10},{10,12},{12... | collective-permute-start | bytes 3145736 | tf_op jit(solution)/shard_map/ppermute | solution.py:21
  22.8 45.0 %all-to-all-start.1 = ((bf16[8,64,512]{2,1,0:T(8,128)(2,1)}), bf16[8,64,512]{2,1,0:T(8,128)(2,1)S(1)}, u32[]{:S(2)}, u32[]{:S(2)}) async-start(bf16[8,64,512]{2,1,0:T(8,128)(2,1)} %broadcast_in_dim.8), calls=%async_computation.1 | async-start | bytes 1048576 | tf_op jit(solution)/shard_map/all_to_all | solution.py:58
  31.3 39.2 %collective-permute-start.12 = (bf16[2,128,2048]{2,1,0:T(8,128)(2,1)S(1)}, bf16[2,128,2048]{2,1,0:T(8,128)(2,1)}, u32[]{:S(2)}, u32[]{:S(2)}) collective-permute-start(bf16[2,128,2048]{2,1,0:T(8,128)(2,1)S(1)} %pad_maximum_fusion.refs_0_), channel_id=1, source_target_pairs={{0,6},{2,0},{4,2},{6,4},{1,7},{3,1},{5,3},{7,5},{8,14},{10,8},{12,... | collective-permute-start | bytes 3145736 | tf_op jit(solution)/shard_map/ppermute | solution.py:21
  31.8 23.4 %collective-permute-start = (bf16[128,2048]{1,0:T(8,128)(2,1)S(1)}, bf16[128,2048]{1,0:T(8,128)(2,1)S(1)}, u32[]{:S(2)}, u32[]{:S(2)}) collective-permute-start(bf16[128,2048]{1,0:T(8,128)(2,1)S(1)} %copy-done.3), channel_id=1, source_target_pairs={{0,2},{2,4},{4,6},{6,0},{1,3},{3,5},{5,7},{7,1},{8,10},{10,12},{12... | collective-permute-start | bytes 1572872 | tf_op jit(solution)/shard_map/ppermute | solution.py:21
  33.3 34.5 %collective-permute-start.1 = (bf16[128,2048]{1,0:T(8,128)(2,1)S(1)}, bf16[128,2048]{1,0:T(8,128)(2,1)S(1)}, u32[]{:S(2)}, u32[]{:S(2)}) collective-permute-start(bf16[128,2048]{1,0:T(8,128)(2,1)S(1)} %copy-done.3), channel_id=1, source_target_pairs={{0,6},{2,0},{4,2},{6,4},{1,7},{3,1},{5,3},{7,5},{8,14},{10,8},{12,... | collective-permute-start | bytes 1572872 | tf_op jit(solution)/shard_map/ppermute | solution.py:21
  33.8 43.8 %collective-permute-start.15 = (bf16[2,128,2048]{2,1,0:T(8,128)(2,1)S(1)}, bf16[2,128,2048]{2,1,0:T(8,128)(2,1)}, u32[]{:S(2)}, u32[]{:S(2)}) collective-permute-start(bf16[2,128,2048]{2,1,0:T(8,128)(2,1)S(1)} %pad_maximum_fusion.refs_0_), channel_id=1, source_target_pairs={{0,1},{1,0},{2,3},{3,2},{4,5},{5,4},{6,7},{7,6},{8,9},{9,8},{10,11... | collective-permute-start | bytes 3145736 | tf_op jit(solution)/shard_map/ppermute | solution.py:21
  55.2 22.4 %collective-permute-start.2 = (bf16[128,2048]{1,0:T(8,128)(2,1)S(1)}, bf16[128,2048]{1,0:T(8,128)(2,1)}, u32[]{:S(2)}, u32[]{:S(2)}) collective-permute-start(bf16[128,2048]{1,0:T(8,128)(2,1)S(1)} %copy-done.3), channel_id=1, source_target_pairs={{0,4},{2,6},{4,0},{6,2},{1,5},{3,7},{5,1},{7,3},{8,12},{10,14},{12... | collective-permute-start | bytes 1572872 | tf_op jit(solution)/shard_map/ppermute | solution.py:21
  67.9 21.0 %collective-permute-start.4 = (bf16[8,64,512]{2,1,0:T(8,128)(2,1)S(1)}, bf16[8,64,512]{2,1,0:T(8,128)(2,1)S(1)}, u32[]{:S(2)}, u32[]{:S(2)}) collective-permute-start(bf16[8,64,512]{2,1,0:T(8,128)(2,1)S(1)} %all-to-all-done.1.refs_3_.refs_10_), channel_id=1, source_target_pairs={{0,8},{8,16},{16,24},{24,0},{1,9},{9,17},{17,25},{25,1},{2,10},{10... | collective-permute-start | bytes 1572872 | tf_op jit(solution)/shard_map/ppermute | solution.py:21
  68.4 20.5 %collective-permute-start.5 = (bf16[8,64,512]{2,1,0:T(8,128)(2,1)S(1)}, bf16[8,64,512]{2,1,0:T(8,128)(2,1)S(1)}, u32[]{:S(2)}, u32[]{:S(2)}) collective-permute-start(bf16[8,64,512]{2,1,0:T(8,128)(2,1)S(1)} %all-to-all-done.1.refs_3_.refs_10_), channel_id=1, source_target_pairs={{0,16},{8,24},{16,0},{24,8},{1,17},{9,25},{17,1},{25,9},{2,18},{10... | collective-permute-start | bytes 1572872 | tf_op jit(solution)/shard_map/ppermute | solution.py:21
  70.5 22.3 %collective-permute-start.6 = (bf16[8,64,512]{2,1,0:T(8,128)(2,1)S(1)}, bf16[8,64,512]{2,1,0:T(8,128)(2,1)S(1)}, u32[]{:S(2)}, u32[]{:S(2)}) collective-permute-start(bf16[8,64,512]{2,1,0:T(8,128)(2,1)S(1)} %all-to-all-done.1.refs_3_.refs_10_), channel_id=1, source_target_pairs={{0,24},{8,0},{16,8},{24,16},{1,25},{9,1},{17,9},{25,17},{2,26},{10... | collective-permute-start | bytes 1572872 | tf_op jit(solution)/shard_map/ppermute | solution.py:21
  77.6 15.8 %collective-permute-start.14 = (bf16[2,64,2048]{2,1,0:T(8,128)(2,1)S(1)}, bf16[2,64,2048]{2,1,0:T(8,128)(2,1)S(1)}, u32[]{:S(2)}, u32[]{:S(2)}) collective-permute-start(bf16[2,64,2048]{2,1,0:T(8,128)(2,1)S(1)} %slice.109), channel_id=1, source_target_pairs={{0,6},{2,0},{4,2},{6,4},{1,7},{3,1},{5,3},{7,5},{8,14},{10,8},{12,... | collective-permute-start | bytes 1572872 | tf_op jit(solution)/shard_map/ppermute | solution.py:21
  92.8 45.4 %collective-permute-start.3 = (bf16[1,512,2048]{2,1,0:T(8,128)(2,1)}, bf16[1,512,2048]{2,1,0:T(8,128)(2,1)}, u32[]{:S(2)}, u32[]{:S(2)}) collective-permute-start(bf16[1,512,2048]{2,1,0:T(8,128)(2,1)} %maximum_bitcast_fusion.refs_0_), channel_id=1, source_target_pairs={{0,1},{1,0},{2,3},{3,2},{4,5},{5,4},{6,7},{7,6},{8,9},{9,8},{10,11... | collective-permute-start | bytes 6291464 | tf_op jit(solution)/shard_map/ppermute | solution.py:21
  113.8 33.4 %all-to-all-start.2 = ((bf16[4,8,64,512]{3,2,1,0:T(8,128)(2,1)}), bf16[4,8,64,512]{3,2,1,0:T(8,128)(2,1)S(1)}, u32[]{:S(2)}, u32[]{:S(2)}) async-start(bf16[4,8,64,512]{3,2,1,0:T(8,128)(2,1)} %get-tuple-element.19), calls=%async_computation.3 | async-start | bytes 4194304 | tf_op jit(solution)/shard_map/all_to_all | solution.py:62
  117.5 107.9 %reduce-scatter.2.cloned.1.call-start = ((), (), s32[]{:S(2)}) async-start(), calls=%async_computation.6 | async-start | bytes 2359296 | tf_op jit(solution)/shard_map/reduce_scatter | solution.py:320
  137.7 41.1 %collective-permute-start.20 = (bf16[512,2048]{1,0:T(8,128)(2,1)}, bf16[512,2048]{1,0:T(8,128)(2,1)}, u32[]{:S(2)}, u32[]{:S(2)}) collective-permute-start(bf16[512,2048]{1,0:T(8,128)(2,1)} %get-tuple-element.17), channel_id=1, source_target_pairs={{0,1},{1,0},{2,3},{3,2},{4,5},{5,4},{6,7},{7,6},{8,9},{9,8},{10,11... | collective-permute-start | bytes 6291464 | tf_op jit(solution)/shard_map/ppermute | solution.py:21
  146.7 43.4 %collective-permute-start.7 = (bf16[512,2048]{1,0:T(8,128)(2,1)}, bf16[512,2048]{1,0:T(8,128)(2,1)}, u32[]{:S(2)}, u32[]{:S(2)}) collective-permute-start(bf16[512,2048]{1,0:T(8,128)(2,1)} %get-tuple-element.13), channel_id=1, source_target_pairs={{0,1},{1,0},{2,3},{3,2},{4,5},{5,4},{6,7},{7,6},{8,9},{9,8},{10,11... | collective-permute-start | bytes 6291464 | tf_op jit(solution)/shard_map/ppermute | solution.py:21
  148.5 30.2 %all-to-all-start.3 = ((bf16[8,64,512]{2,1,0:T(8,128)(2,1)}), bf16[8,64,512]{2,1,0:T(8,128)(2,1)S(1)}, u32[]{:S(2)}, u32[]{:S(2)}) async-start(bf16[8,64,512]{2,1,0:T(8,128)(2,1)} %reduce_sum.21), calls=%async_computation.4 | async-start | bytes 1048576 | tf_op jit(solution)/shard_map/all_to_all | solution.py:62
  181.4 17.1 %collective-permute-start.21 = (bf16[128,2048]{1,0:T(8,128)(2,1)S(1)}, bf16[128,2048]{1,0:T(8,128)(2,1)S(1)}, u32[]{:S(2)}, u32[]{:S(2)}) collective-permute-start(bf16[128,2048]{1,0:T(8,128)(2,1)S(1)} %get-tuple-element.20), channel_id=1, source_target_pairs={{0,2},{2,4},{4,6},{6,0},{1,3},{3,5},{5,7},{7,1},{8,10},{10,12},{12... | collective-permute-start | bytes 1572872 | tf_op jit(solution)/shard_map/ppermute | solution.py:21
  182.3 40.7 %collective-permute-start.22 = (bf16[128,2048]{1,0:T(8,128)(2,1)S(1)}, bf16[128,2048]{1,0:T(8,128)(2,1)S(1)}, u32[]{:S(2)}, u32[]{:S(2)}) collective-permute-start(bf16[128,2048]{1,0:T(8,128)(2,1)S(1)} %get-tuple-element.22), channel_id=1, source_target_pairs={{0,6},{2,0},{4,2},{6,4},{1,7},{3,1},{5,3},{7,5},{8,14},{10,8},{12,... | collective-permute-start | bytes 1572872 | tf_op jit(solution)/shard_map/ppermute | solution.py:21
  185.8 37.2 %collective-permute-start.23 = (bf16[128,2048]{1,0:T(8,128)(2,1)S(1)}, bf16[128,2048]{1,0:T(8,128)(2,1)S(1)}, u32[]{:S(2)}, u32[]{:S(2)}) collective-permute-start(bf16[128,2048]{1,0:T(8,128)(2,1)S(1)} %get-tuple-element.21), channel_id=1, source_target_pairs={{0,4},{2,6},{4,0},{6,2},{1,5},{3,7},{5,1},{7,3},{8,12},{10,14},{12... | collective-permute-start | bytes 1572872 | tf_op jit(solution)/shard_map/ppermute | solution.py:21
  192.8 38.3 %collective-permute-start.10 = (bf16[128,2048]{1,0:T(8,128)(2,1)}, bf16[128,2048]{1,0:T(8,128)(2,1)}, u32[]{:S(2)}, u32[]{:S(2)}) collective-permute-start(bf16[128,2048]{1,0:T(8,128)(2,1)} %get-tuple-element.24), channel_id=1, source_target_pairs={{0,4},{2,6},{4,0},{6,2},{1,5},{3,7},{5,1},{7,3},{8,12},{10,14},{12... | collective-permute-start | bytes 1572872 | tf_op jit(solution)/shard_map/ppermute | solution.py:21
  192.8 39.7 %collective-permute-start.8 = (bf16[128,2048]{1,0:T(8,128)(2,1)S(1)}, bf16[128,2048]{1,0:T(8,128)(2,1)}, u32[]{:S(2)}, u32[]{:S(2)}) collective-permute-start(bf16[128,2048]{1,0:T(8,128)(2,1)S(1)} %get-tuple-element.23), channel_id=1, source_target_pairs={{0,2},{2,4},{4,6},{6,0},{1,3},{3,5},{5,7},{7,1},{8,10},{10,12},{12... | collective-permute-start | bytes 1572872 | tf_op jit(solution)/shard_map/ppermute | solution.py:21
  198.5 35.0 %collective-permute-start.9 = (bf16[128,2048]{1,0:T(8,128)(2,1)S(1)}, bf16[128,2048]{1,0:T(8,128)(2,1)}, u32[]{:S(2)}, u32[]{:S(2)}) collective-permute-start(bf16[128,2048]{1,0:T(8,128)(2,1)S(1)} %get-tuple-element.25), channel_id=1, source_target_pairs={{0,6},{2,0},{4,2},{6,4},{1,7},{3,1},{5,3},{7,5},{8,14},{10,8},{12,... | collective-permute-start | bytes 1572872 | tf_op jit(solution)/shard_map/ppermute | solution.py:21
  (21 other events, 219.3 us)
Sparse Core Ops, SparseCore 0:
  19.1 49.0 all-gather.1
  132.1 56.6 reduce-scatter.1

commit v8 on v7

--- a/solution.py
+++ b/solution.py
@@ -81,10 +81,6 @@
     return lax.dot_general(left, right, (((1,), (1,)), ((), ())), preferred_element_type=F32)
 
 
-def over_tokens(left, right):
-    return lax.dot_general(left, right, (((0,), (0,)), ((), ())), preferred_element_type=F32)
-
-
 def copies(sources, target, sems, index):
     waits, row = [], 0
     for i, source in enumerate(sources):
@@ -117,31 +113,36 @@
     return waits
 
 
-def half_products(pieces, weight_copies, saved, cot, weight, hid, pg, pg_out, store, flush, in_sems, sem):
+def half_products(pieces, weight_copies, saved, cot, weight, hid, pg_t, pg, pg_out, store, flush, in_sems, sem):
     for copy in weight_copies:
         copy.start()
     saved_waits = copies(pieces, saved, in_sems.at[0], 0)
+    for copy in weight_copies:
+        copy.wait()
     cot_waits = copies(pieces, cot, in_sems.at[1], 1)
-    for copy in weight_copies:
-        copy.wait()
-    width = hid.shape[1]
+    width = hid.shape[0]
     both = weight[...].reshape(-1, 2 * width)
     for t in range(0, saved.shape[0], TILE):
         at = pl.ds(t, TILE)
         settle(saved_waits, t + TILE)
         r = relu_times(saved[at], both[:, :width])
-        hid[at] = (r * r).astype(BF16)
+        hid[:, at] = (r * r).astype(BF16).T
         settle(cot_waits, t + TILE)
         grad = jnp.dot(cot[at], both[:, width:], preferred_element_type=F32)
-        pg[at] = (2.0 * r * grad).astype(BF16)
+        piece = (2.0 * r * grad).astype(BF16)
+        pg[at] = piece
+        pg_t[:, at] = piece.T
     nz, block = weight.shape[0], weight.shape[1] * weight.shape[2]
 
     def terms(first, last):
-        @pl.loop(first, last)
+        @pl.loop(first, last, step=2)
         def _(i):
-            at = pl.ds(pl.multiple_of(i * block, block), block)
-            store(i, 0, over_tokens(saved[:, at], pg[...]).astype(BF16))
-            store(i, width, over_tokens(cot[:, at], hid[...]).astype(BF16))
+            at = pl.ds(pl.multiple_of(i * block, 2 * block), 2 * block)
+            up = jnp.dot(pg_t[...], saved[:, at], preferred_element_type=F32).astype(BF16).T
+            down = jnp.dot(hid[...], cot[:, at], preferred_element_type=F32).astype(BF16).T
+            for j in range(2):
+                store(i + j, 0, up[j * block : (j + 1) * block])
+                store(i + j, width, down[j * block : (j + 1) * block])
 
         return flush(first, last)
 
@@ -157,7 +158,7 @@
 
 def first_kernel(*refs):
     pieces, (w, out, pg_out) = refs[:10], refs[10:13]
-    saved, cot, weight, hid, pg, term, in_sems, sems = refs[13:]
+    saved, cot, weight, hid, pg_t, pg, term, in_sems, sems = refs[13:]
     block = weight.shape[1] * weight.shape[2]
 
     def store(i, col, value):
@@ -170,13 +171,13 @@
 
     weight_copies = [pltpu.make_async_copy(w, weight, sems.at[0])]
     half_products(
-        pieces, weight_copies, saved, cot, weight, hid, pg, pg_out, store, flush, in_sems, sems.at[3]
+        pieces, weight_copies, saved, cot, weight, hid, pg_t, pg, pg_out, store, flush, in_sems, sems.at[3]
     )
 
 
 def second_kernel(*refs):
     pieces, parts, (out, pg_out) = refs[:10], refs[10:14], refs[14:16]
-    saved, cot, weight, hid, pg, term, in_sems, w_sems, sems = refs[16:]
+    saved, cot, weight, hid, pg_t, pg, term, in_sems, w_sems, sems = refs[16:]
     nx, _, part = term.shape[:3]
 
     def store(i, col, value):
@@ -192,7 +193,7 @@
         at = (lax.axis_index("x") + (nx - k)) & (nx - 1)
         weight_copies.append(pltpu.make_async_copy(piece, weight.at[:, at], w_sems.at[k]))
     half_products(
-        pieces, weight_copies, saved, cot, weight, hid, pg, pg_out, store, flush, in_sems, sems.at[3]
+        pieces, weight_copies, saved, cot, weight, hid, pg_t, pg, pg_out, store, flush, in_sems, sems.at[3]
     )
 
 
@@ -281,14 +282,15 @@
         ((nx, nz, part, cols), BF16),
         ((depth, cols), BF16),
     )
-    narrow, half = ((rows, width), BF16), ((rows // 2, depth), BF16)
+    narrow, turned = ((rows, width), BF16), ((width, rows), BF16)
+    half = ((rows // 2, depth), BF16)
 
     def one():
-        scratch = (group, group, split, narrow, narrow, flat), ((2, n), (4,))
+        scratch = (group, group, split, turned, turned, narrow, flat), ((2, n), (4,))
         return call(first_kernel, (*pieces, first), (flat, narrow), scratch, 2 * flops)
 
     def two():
-        scratch = (group, group, split, narrow, narrow, swapped), ((2, n), (nx,), (4,))
+        scratch = (group, group, split, turned, turned, narrow, swapped), ((2, n), (nx,), (4,))
         return call(second_kernel, (*pieces, *parts), (swapped, narrow), scratch, 2 * flops)
 
     def row_grad(pg_a, pg_b):

time: 247 us -> 243 us (0.984)
  Pallas kernels: 43 us -> 38.9 us
    pallas_call x4, Pallas kernels: 43 us -> 38.9 us  [call(): pl.pallas_call(kernel, out_shape=[jax.ShapeDtypeStruct(*s) for s in outs]...]
  transfers between devices with their start and end apart: 32 -> 32, of which waited for: 9 -> 9; matrix products, arithmetic and copies ran while one was open for 8% -> 8% of each run, Pallas kernels for 18% -> 16%
where the time goes in v8:
time: 243 us; the launch traced here: 241 us
  starting transfers between devices  77.4 us (32%)
  waiting for transfers between devices  75.1 us (31%)
  Pallas kernels  38.9 us (16%)
  other arithmetic  18 us (7%)
  between operations  14.3 us (6%)
  blocking collectives  10.9 us (4%)
  local copies, waits for them, and re-layouts  6.64 us (3%)
    ppermute x27, starting transfers between devices, shift(): return lax.ppermute(x, axis, [(i, (i + by) % n) for i in range(n)])  58.6 us
    ppermute x27, waiting for transfers between devices, shift(): return lax.ppermute(x, axis, [(i, (i + by) % n) for i in range(n)])  51.5 us
    pallas_call x4, Pallas kernels, call(): pl.pallas_call(kernel, out_shape=[jax.ShapeDtypeStruct(*s) for s in outs]...  38.9 us
    all_to_all x2, waiting for transfers between devices, exchange_sum(): tiles = lax.all_to_all(term, axis, 0, 0, tiled=True)  23.6 us
    all_to_all x1, blocking collectives, gather(): lax.all_to_all(jnp.broadcast_to(x[None], (n, *x.shape)), axis, 0, 0, tile...  10.9 us
    all_to_all x2, starting transfers between devices, exchange_sum(): tiles = lax.all_to_all(term, axis, 0, 0, tiled=True)  10.3 us
    all_to_all x1, starting transfers between devices, gather(): lax.all_to_all(jnp.broadcast_to(x[None], (n, *x.shape)), axis, 0, 0, tile...  8.47 us
    convert_element_type x2, other arithmetic, plus(): return (a.astype(F32) + b.astype(F32)).astype(BF16)  5.31 us
  transfers between devices with their start and end apart: 32, of which 9 were waited for; matrix products, arithmetic and copies ran while one was open for 8% of the time, Pallas kernels for 16%

profile of v8, /device:TPU:8, one launch (start us, length us, event | category | flops | bytes accessed | tf_op | source)
XLA Modules:
  0.0 241.3 jit_solution(2801881392911334349)
XLA Ops:
  8.1 10.9 %all_to_all.20 = bf16[4,64,512]{2,1,0:T(8,128)(2,1)} all-to-all(bf16[4,64,512]{2,1,0:T(8,128)(2,1)S(1)} %broadcast_in_dim.7), channel_id=1, replica_groups=mesh['z'=8,'x'=4,'y'=4,'c'=2] {'x'}, dimensions={0} | all-to-all | bytes 524288 | tf_op jit(solution)/shard_map/all_to_all | solution.py:58
  22.8 8.5 %all-to-all-start.1 = ((bf16[8,64,512]{2,1,0:T(8,128)(2,1)}), bf16[8,64,512]{2,1,0:T(8,128)(2,1)S(1)}, u32[]{:S(2)}, u32[]{:S(2)}) async-start(bf16[8,64,512]{2,1,0:T(8,128)(2,1)} %broadcast_in_dim.8), calls=%async_computation.1 | async-start | bytes 1048576 | tf_op jit(solution)/shard_map/all_to_all | solution.py:58
  33.8 21.4 %collective-permute-done = bf16[128,2048]{1,0:T(8,128)(2,1)S(1)} collective-permute-done((bf16[128,2048]{1,0:T(8,128)(2,1)S(1)}, bf16[128,2048]{1,0:T(8,128)(2,1)S(1)}, u32[]{:S(2)}, u32[]{:S(2)}) %collective-permute-start) | collective-permute-done | bytes 524320 | tf_op jit(solution)/shard_map/ppermute | solution.py:21
  57.5 10.4 %collective-permute-done.1 = bf16[128,2048]{1,0:T(8,128)(2,1)S(1)} collective-permute-done((bf16[128,2048]{1,0:T(8,128)(2,1)S(1)}, bf16[128,2048]{1,0:T(8,128)(2,1)S(1)}, u32[]{:S(2)}, u32[]{:S(2)}) %collective-permute-start.1) | collective-permute-done | bytes 524320 | tf_op jit(solution)/shard_map/ppermute | solution.py:21
  73.5 4.1 %collective-permute-done.2 = bf16[128,2048]{1,0:T(8,128)(2,1)} collective-permute-done((bf16[128,2048]{1,0:T(8,128)(2,1)S(1)}, bf16[128,2048]{1,0:T(8,128)(2,1)}, u32[]{:S(2)}, u32[]{:S(2)}) %collective-permute-start.2) | collective-permute-done | bytes 524320 | tf_op jit(solution)/shard_map/ppermute | solution.py:21
  77.6 5.1 %collective-permute-start.14 = (bf16[2,64,2048]{2,1,0:T(8,128)(2,1)S(1)}, bf16[2,64,2048]{2,1,0:T(8,128)(2,1)S(1)}, u32[]{:S(2)}, u32[]{:S(2)}) collective-permute-start(bf16[2,64,2048]{2,1,0:T(8,128)(2,1)S(1)} %slice.109), channel_id=1, source_target_pairs={{0,6},{2,0},{4,2},{6,4},{1,7},{3,1},{5,3},{7,5},{8,14},{10,8},{12,... | collective-permute-start | bytes 1572872 | tf_op jit(solution)/shard_map/ppermute | solution.py:21
  82.7 6.2 %collective-permute-done.4.refs_4_.refs_11_ = bf16[8,64,512]{2,1,0:T(8,128)(2,1)S(1)} collective-permute-done((bf16[8,64,512]{2,1,0:T(8,128)(2,1)S(1)}, bf16[8,64,512]{2,1,0:T(8,128)(2,1)S(1)}, u32[]{:S(2)}, u32[]{:S(2)}) %collective-permute-start.4) | collective-permute-done | bytes 524320 | tf_op jit(solution)/shard_map/ppermute | solution.py:21
  90.2 2.6 %maximum_bitcast_fusion.refs_0_ = bf16[1,512,2048]{2,1,0:T(8,128)(2,1)} fusion(bf16[128,2048]{1,0:T(8,128)(2,1)} %collective-permute-done.2, bf16[128,2048]{1,0:T(8,128)(2,1)S(1)} %collective-permute-done.1, bf16[128,2048]{1,0:T(8,128)(2,1)S(1)} %collective-permute-done, bf16[128,2048]{1,0:T(8,128)(2,1)S(1)} %copy-done.3), kind=kLoop, calls=%fused_computation | loop fusion | flops 8388608 | bytes 4194304 | tf_op jit(solution)/shard_map/broadcast_in_dim | solution.py:38
  93.8 4.2 %collective-permute-done.18.refs_8_ = bf16[2,64,2048]{2,1,0:T(8,128)(2,1)S(1)} collective-permute-done((bf16[2,64,2048]{2,1,0:T(8,128)(2,1)S(1)}, bf16[2,64,2048]{2,1,0:T(8,128)(2,1)S(1)}, u32[]{:S(2)}, u32[]{:S(2)}) %collective-permute-start.18) | collective-permute-done | bytes 524320 | tf_op jit(solution)/shard_map/ppermute | solution.py:21
  99.5 12.3 %shard_map.104 = (bf16[4,8,64,512]{3,2,1,0:T(8,128)(2,1)}, bf16[1024,256]{1,0:T(8,128)(2,1)}) custom-call(bf16[2,128,2048]{2,1,0:T(8,128)(2,1)} %copy-done.1, bf16[2,128,2048]{2,1,0:T(8,128)(2,1)} %collective-permute-done.11.refs_1_, bf16[2,128,2048]{2,1,0:T(8,128)(2,1)} %collective-permute-done.12.refs_2_, bf16[2,64,2048]{2,1,0:T(8,128)(2,1)} %copy-done.9, ...), custom_call_target="tpu_custom_call" | custom-call | flops 4294967296 | bytes 12582912 | tf_op jit(solution)/shard_map/pallas_call | solution.py:261
  111.8 3.6 %all-to-all-start.2 = ((bf16[4,8,64,512]{3,2,1,0:T(8,128)(2,1)}), bf16[4,8,64,512]{3,2,1,0:T(8,128)(2,1)S(1)}, u32[]{:S(2)}, u32[]{:S(2)}) async-start(bf16[4,8,64,512]{3,2,1,0:T(8,128)(2,1)} %get-tuple-element.19), calls=%async_computation.3 | async-start | bytes 4194304 | tf_op jit(solution)/shard_map/all_to_all | solution.py:62
  115.5 12.4 %shard_map.103 = (bf16[2048,512]{1,0:T(8,128)(2,1)}, bf16[1024,256]{1,0:T(8,128)(2,1)}) custom-call(bf16[2,128,2048]{2,1,0:T(8,128)(2,1)} %copy-done.1, bf16[2,128,2048]{2,1,0:T(8,128)(2,1)} %collective-permute-done.11.refs_1_, bf16[2,128,2048]{2,1,0:T(8,128)(2,1)} %collective-permute-done.12.refs_2_, bf16[2,64,2048]{2,1,0:T(8,128)(2,1)} %copy-done.9, ...), custom_call_target="tpu_custom_call" | custom-call | flops 4294967296 | bytes 12582912 | tf_op jit(solution)/shard_map/pallas_call | solution.py:261
  127.9 5.7 %shard_map.105 = (bf16[512,2048]{1,0:T(8,128)(2,1)}, bf16[512,2048]{1,0:T(8,128)(2,1)}) custom-call(bf16[1024,256]{1,0:T(8,128)(2,1)} %get-tuple-element.14.refs_0_, bf16[1024,256]{1,0:T(8,128)(2,1)} %get-tuple-element.15.refs_1_, bf16[8,4,64,512]{3,2,1,0:T(8,128)(2,1)} %bitcast.22, bf16[8,64,512]{2,1,0:T(8,128)(2,1)} %copy-done.2, ...), custom_call_target="tpu_custom_call" | custom-call | flops 2147483648 | bytes 12582912 | tf_op jit(solution)/shard_map/pallas_call | solution.py:261
  134.1 8.6 %shard_map.102 = (bf16[512,2048]{1,0:T(8,128)(2,1)}, bf16[512,2048]{1,0:T(8,128)(2,1)}) custom-call(bf16[1,512,2048]{2,1,0:T(8,128)(2,1)} %maximum_bitcast_fusion.refs_0_, bf16[1,512,2048]{2,1,0:T(8,128)(2,1)} %collective-permute-done.3.refs_1_, bf16[8,4,64,512]{3,2,1,0:T(8,128)(2,1)} %bitcast.23, bf16[8,64,512]{2,1,0:T(8,128)(2,1)} %copy-done.2, ...), custom_call_target="tpu_custom_call" | custom-call | flops 4294967296 | bytes 12582912 | tf_op jit(solution)/shard_map/pallas_call | solution.py:261
  144.4 6.6 %all-to-all-start.3 = ((bf16[8,64,512]{2,1,0:T(8,128)(2,1)}), bf16[8,64,512]{2,1,0:T(8,128)(2,1)S(1)}, u32[]{:S(2)}, u32[]{:S(2)}) async-start(bf16[8,64,512]{2,1,0:T(8,128)(2,1)} %reduce_sum.21), calls=%async_computation.4 | async-start | bytes 1048576 | tf_op jit(solution)/shard_map/all_to_all | solution.py:62
  151.0 23.6 %all-to-all-done.3 = bf16[8,64,512]{2,1,0:T(8,128)(2,1)S(1)} async-done(((bf16[8,64,512]{2,1,0:T(8,128)(2,1)}), bf16[8,64,512]{2,1,0:T(8,128)(2,1)S(1)}, u32[]{:S(2)}, u32[]{:S(2)}) %all-to-all-start.3) | async-done | bytes 524320 | tf_op jit(solution)/shard_map/all_to_all | solution.py:62
  174.7 2.6 %add_convert_fusion.3 = (bf16[128,2048]{1,0:T(8,128)(2,1)S(1)}, bf16[128,2048]{1,0:T(8,128)(2,1)S(1)}, bf16[128,2048]{1,0:T(8,128)(2,1)S(1)}) fusion(bf16[512,2048]{1,0:T(8,128)(2,1)} %collective-permute-done.20, bf16[512,2048]{1,0:T(8,128)(2,1)} %get-tuple-element.16), kind=kLoop, calls=%fused_computation.6 | loop fusion | flops 3145728 | bytes 4718592 | tf_op jit(solution)/shard_map/convert_element_type | solution.py:43
  178.2 3.6 %collective-permute-start.22 = (bf16[128,2048]{1,0:T(8,128)(2,1)S(1)}, bf16[128,2048]{1,0:T(8,128)(2,1)S(1)}, u32[]{:S(2)}, u32[]{:S(2)}) collective-permute-start(bf16[128,2048]{1,0:T(8,128)(2,1)S(1)} %get-tuple-element.22), channel_id=1, source_target_pairs={{0,6},{2,0},{4,2},{6,4},{1,7},{3,1},{5,3},{7,5},{8,14},{10,8},{12,... | collective-permute-start | bytes 1572872 | tf_op jit(solution)/shard_map/ppermute | solution.py:21
  181.7 4.3 %collective-permute-start.23 = (bf16[128,2048]{1,0:T(8,128)(2,1)S(1)}, bf16[128,2048]{1,0:T(8,128)(2,1)S(1)}, u32[]{:S(2)}, u32[]{:S(2)}) collective-permute-start(bf16[128,2048]{1,0:T(8,128)(2,1)S(1)} %get-tuple-element.21), channel_id=1, source_target_pairs={{0,4},{2,6},{4,0},{6,2},{1,5},{3,7},{5,1},{7,3},{8,12},{10,14},{12... | collective-permute-start | bytes 1572872 | tf_op jit(solution)/shard_map/ppermute | solution.py:21
  186.0 2.7 %add_convert_fusion.7 = (bf16[128,2048]{1,0:T(8,128)(2,1)S(1)}, bf16[128,2048]{1,0:T(8,128)(2,1)}, bf16[128,2048]{1,0:T(8,128)(2,1)S(1)}) fusion(bf16[512,2048]{1,0:T(8,128)(2,1)} %collective-permute-done.7, bf16[512,2048]{1,0:T(8,128)(2,1)S(1)} %copy-done), kind=kLoop, calls=%fused_computation.10 | loop fusion | flops 3145728 | bytes 4718592 | tf_op jit(solution)/shard_map/convert_element_type | solution.py:43
  190.8 3.6 %collective-permute-done.21 = bf16[128,2048]{1,0:T(8,128)(2,1)S(1)} collective-permute-done((bf16[128,2048]{1,0:T(8,128)(2,1)S(1)}, bf16[128,2048]{1,0:T(8,128)(2,1)S(1)}, u32[]{:S(2)}, u32[]{:S(2)}) %collective-permute-start.21) | collective-permute-done | bytes 524320 | tf_op jit(solution)/shard_map/ppermute | solution.py:21
  194.4 24.5 %collective-permute-start.9 = (bf16[128,2048]{1,0:T(8,128)(2,1)S(1)}, bf16[128,2048]{1,0:T(8,128)(2,1)}, u32[]{:S(2)}, u32[]{:S(2)}) collective-permute-start(bf16[128,2048]{1,0:T(8,128)(2,1)S(1)} %get-tuple-element.25), channel_id=1, source_target_pairs={{0,6},{2,0},{4,2},{6,4},{1,7},{3,1},{5,3},{7,5},{8,14},{10,8},{12,... | collective-permute-start | bytes 1572872 | tf_op jit(solution)/shard_map/ppermute | solution.py:21
  222.4 4.7 %collective-permute-start.25 = (bf16[64,512]{1,0:T(8,128)(2,1)S(1)}, bf16[64,512]{1,0:T(8,128)(2,1)S(1)}, u32[]{:S(2)}, u32[]{:S(2)}) collective-permute-start(bf16[64,512]{1,0:T(8,128)(2,1)S(1)} %get-tuple-element.28), channel_id=1, source_target_pairs={{0,16},{8,24},{16,0},{24,8},{1,17},{9,25},{17,1},{25,9},{2,18},{10... | collective-permute-start | bytes 196616 | tf_op jit(solution)/shard_map/ppermute | solution.py:21
  229.4 2.7 %add_convert_fusion.4 = bf16[128,2048]{1,0:T(8,128)(2,1)} fusion(bf16[128,2048]{1,0:T(8,128)(2,1)} %collective-permute-done.10, bf16[128,2048]{1,0:T(8,128)(2,1)} %collective-permute-done.9, bf16[128,2048]{1,0:T(8,128)(2,1)} %collective-permute-done.8, bf16[512,2048]{1,0:T(8,128)(2,1)} %collective-permute-done.7, bf16[512,2048]{1,0:T(8,128)(2,1)S(1)} %copy-done), kind=kLoop, calls=%fused_computation.7 | loop fusion | flops 2621440 | bytes 3145728 | tf_op jit(solution)/shard_map/convert_element_type | solution.py:53
  (94 shorter events, 32.3 us)
Async XLA Ops:
  7.2 108.3 %all-gather.2.cloned.1.call-start = ((), (), s32[]{:S(2)}) async-start(), calls=%async_computation.5 | async-start | bytes 2359296 | tf_op jit(solution)/shard_map/all_gather | solution.py:315
  20.3 48.1 %collective-permute-start.11 = (bf16[2,128,2048]{2,1,0:T(8,128)(2,1)S(1)}, bf16[2,128,2048]{2,1,0:T(8,128)(2,1)}, u32[]{:S(2)}, u32[]{:S(2)}) collective-permute-start(bf16[2,128,2048]{2,1,0:T(8,128)(2,1)S(1)} %pad_maximum_fusion.refs_0_), channel_id=1, source_target_pairs={{0,2},{2,4},{4,6},{6,0},{1,3},{3,5},{5,7},{7,1},{8,10},{10,12},{12... | collective-permute-start | bytes 3145736 | tf_op jit(solution)/shard_map/ppermute | solution.py:21
  22.8 45.0 %all-to-all-start.1 = ((bf16[8,64,512]{2,1,0:T(8,128)(2,1)}), bf16[8,64,512]{2,1,0:T(8,128)(2,1)S(1)}, u32[]{:S(2)}, u32[]{:S(2)}) async-start(bf16[8,64,512]{2,1,0:T(8,128)(2,1)} %broadcast_in_dim.8), calls=%async_computation.1 | async-start | bytes 1048576 | tf_op jit(solution)/shard_map/all_to_all | solution.py:58
  31.3 39.2 %collective-permute-start.12 = (bf16[2,128,2048]{2,1,0:T(8,128)(2,1)S(1)}, bf16[2,128,2048]{2,1,0:T(8,128)(2,1)}, u32[]{:S(2)}, u32[]{:S(2)}) collective-permute-start(bf16[2,128,2048]{2,1,0:T(8,128)(2,1)S(1)} %pad_maximum_fusion.refs_0_), channel_id=1, source_target_pairs={{0,6},{2,0},{4,2},{6,4},{1,7},{3,1},{5,3},{7,5},{8,14},{10,8},{12,... | collective-permute-start | bytes 3145736 | tf_op jit(solution)/shard_map/ppermute | solution.py:21
  31.8 23.4 %collective-permute-start = (bf16[128,2048]{1,0:T(8,128)(2,1)S(1)}, bf16[128,2048]{1,0:T(8,128)(2,1)S(1)}, u32[]{:S(2)}, u32[]{:S(2)}) collective-permute-start(bf16[128,2048]{1,0:T(8,128)(2,1)S(1)} %copy-done.3), channel_id=1, source_target_pairs={{0,2},{2,4},{4,6},{6,0},{1,3},{3,5},{5,7},{7,1},{8,10},{10,12},{12... | collective-permute-start | bytes 1572872 | tf_op jit(solution)/shard_map/ppermute | solution.py:21
  33.3 34.5 %collective-permute-start.1 = (bf16[128,2048]{1,0:T(8,128)(2,1)S(1)}, bf16[128,2048]{1,0:T(8,128)(2,1)S(1)}, u32[]{:S(2)}, u32[]{:S(2)}) collective-permute-start(bf16[128,2048]{1,0:T(8,128)(2,1)S(1)} %copy-done.3), channel_id=1, source_target_pairs={{0,6},{2,0},{4,2},{6,4},{1,7},{3,1},{5,3},{7,5},{8,14},{10,8},{12,... | collective-permute-start | bytes 1572872 | tf_op jit(solution)/shard_map/ppermute | solution.py:21
  33.8 43.8 %collective-permute-start.15 = (bf16[2,128,2048]{2,1,0:T(8,128)(2,1)S(1)}, bf16[2,128,2048]{2,1,0:T(8,128)(2,1)}, u32[]{:S(2)}, u32[]{:S(2)}) collective-permute-start(bf16[2,128,2048]{2,1,0:T(8,128)(2,1)S(1)} %pad_maximum_fusion.refs_0_), channel_id=1, source_target_pairs={{0,1},{1,0},{2,3},{3,2},{4,5},{5,4},{6,7},{7,6},{8,9},{9,8},{10,11... | collective-permute-start | bytes 3145736 | tf_op jit(solution)/shard_map/ppermute | solution.py:21
  55.2 22.4 %collective-permute-start.2 = (bf16[128,2048]{1,0:T(8,128)(2,1)S(1)}, bf16[128,2048]{1,0:T(8,128)(2,1)}, u32[]{:S(2)}, u32[]{:S(2)}) collective-permute-start(bf16[128,2048]{1,0:T(8,128)(2,1)S(1)} %copy-done.3), channel_id=1, source_target_pairs={{0,4},{2,6},{4,0},{6,2},{1,5},{3,7},{5,1},{7,3},{8,12},{10,14},{12... | collective-permute-start | bytes 1572872 | tf_op jit(solution)/shard_map/ppermute | solution.py:21
  67.9 21.0 %collective-permute-start.4 = (bf16[8,64,512]{2,1,0:T(8,128)(2,1)S(1)}, bf16[8,64,512]{2,1,0:T(8,128)(2,1)S(1)}, u32[]{:S(2)}, u32[]{:S(2)}) collective-permute-start(bf16[8,64,512]{2,1,0:T(8,128)(2,1)S(1)} %all-to-all-done.1.refs_3_.refs_10_), channel_id=1, source_target_pairs={{0,8},{8,16},{16,24},{24,0},{1,9},{9,17},{17,25},{25,1},{2,10},{10... | collective-permute-start | bytes 1572872 | tf_op jit(solution)/shard_map/ppermute | solution.py:21
  68.4 20.5 %collective-permute-start.5 = (bf16[8,64,512]{2,1,0:T(8,128)(2,1)S(1)}, bf16[8,64,512]{2,1,0:T(8,128)(2,1)S(1)}, u32[]{:S(2)}, u32[]{:S(2)}) collective-permute-start(bf16[8,64,512]{2,1,0:T(8,128)(2,1)S(1)} %all-to-all-done.1.refs_3_.refs_10_), channel_id=1, source_target_pairs={{0,16},{8,24},{16,0},{24,8},{1,17},{9,25},{17,1},{25,9},{2,18},{10... | collective-permute-start | bytes 1572872 | tf_op jit(solution)/shard_map/ppermute | solution.py:21
  70.5 22.3 %collective-permute-start.6 = (bf16[8,64,512]{2,1,0:T(8,128)(2,1)S(1)}, bf16[8,64,512]{2,1,0:T(8,128)(2,1)S(1)}, u32[]{:S(2)}, u32[]{:S(2)}) collective-permute-start(bf16[8,64,512]{2,1,0:T(8,128)(2,1)S(1)} %all-to-all-done.1.refs_3_.refs_10_), channel_id=1, source_target_pairs={{0,24},{8,0},{16,8},{24,16},{1,25},{9,1},{17,9},{25,17},{2,26},{10... | collective-permute-start | bytes 1572872 | tf_op jit(solution)/shard_map/ppermute | solution.py:21
  77.6 15.8 %collective-permute-start.14 = (bf16[2,64,2048]{2,1,0:T(8,128)(2,1)S(1)}, bf16[2,64,2048]{2,1,0:T(8,128)(2,1)S(1)}, u32[]{:S(2)}, u32[]{:S(2)}) collective-permute-start(bf16[2,64,2048]{2,1,0:T(8,128)(2,1)S(1)} %slice.109), channel_id=1, source_target_pairs={{0,6},{2,0},{4,2},{6,4},{1,7},{3,1},{5,3},{7,5},{8,14},{10,8},{12,... | collective-permute-start | bytes 1572872 | tf_op jit(solution)/shard_map/ppermute | solution.py:21
  92.8 41.3 %collective-permute-start.3 = (bf16[1,512,2048]{2,1,0:T(8,128)(2,1)}, bf16[1,512,2048]{2,1,0:T(8,128)(2,1)}, u32[]{:S(2)}, u32[]{:S(2)}) collective-permute-start(bf16[1,512,2048]{2,1,0:T(8,128)(2,1)} %maximum_bitcast_fusion.refs_0_), channel_id=1, source_target_pairs={{0,1},{1,0},{2,3},{3,2},{4,5},{5,4},{6,7},{7,6},{8,9},{9,8},{10,11... | collective-permute-start | bytes 6291464 | tf_op jit(solution)/shard_map/ppermute | solution.py:21
  111.8 31.3 %all-to-all-start.2 = ((bf16[4,8,64,512]{3,2,1,0:T(8,128)(2,1)}), bf16[4,8,64,512]{3,2,1,0:T(8,128)(2,1)S(1)}, u32[]{:S(2)}, u32[]{:S(2)}) async-start(bf16[4,8,64,512]{3,2,1,0:T(8,128)(2,1)} %get-tuple-element.19), calls=%async_computation.3 | async-start | bytes 4194304 | tf_op jit(solution)/shard_map/all_to_all | solution.py:62
  115.4 105.9 %reduce-scatter.2.cloned.1.call-start = ((), (), s32[]{:S(2)}) async-start(), calls=%async_computation.6 | async-start | bytes 2359296 | tf_op jit(solution)/shard_map/reduce_scatter | solution.py:322
  133.6 41.1 %collective-permute-start.20 = (bf16[512,2048]{1,0:T(8,128)(2,1)}, bf16[512,2048]{1,0:T(8,128)(2,1)}, u32[]{:S(2)}, u32[]{:S(2)}) collective-permute-start(bf16[512,2048]{1,0:T(8,128)(2,1)} %get-tuple-element.17), channel_id=1, source_target_pairs={{0,1},{1,0},{2,3},{3,2},{4,5},{5,4},{6,7},{7,6},{8,9},{9,8},{10,11... | collective-permute-start | bytes 6291464 | tf_op jit(solution)/shard_map/ppermute | solution.py:21
  142.7 43.3 %collective-permute-start.7 = (bf16[512,2048]{1,0:T(8,128)(2,1)}, bf16[512,2048]{1,0:T(8,128)(2,1)}, u32[]{:S(2)}, u32[]{:S(2)}) collective-permute-start(bf16[512,2048]{1,0:T(8,128)(2,1)} %get-tuple-element.13), channel_id=1, source_target_pairs={{0,1},{1,0},{2,3},{3,2},{4,5},{5,4},{6,7},{7,6},{8,9},{9,8},{10,11... | collective-permute-start | bytes 6291464 | tf_op jit(solution)/shard_map/ppermute | solution.py:21
  144.4 30.2 %all-to-all-start.3 = ((bf16[8,64,512]{2,1,0:T(8,128)(2,1)}), bf16[8,64,512]{2,1,0:T(8,128)(2,1)S(1)}, u32[]{:S(2)}, u32[]{:S(2)}) async-start(bf16[8,64,512]{2,1,0:T(8,128)(2,1)} %reduce_sum.21), calls=%async_computation.4 | async-start | bytes 1048576 | tf_op jit(solution)/shard_map/all_to_all | solution.py:62
  177.3 17.1 %collective-permute-start.21 = (bf16[128,2048]{1,0:T(8,128)(2,1)S(1)}, bf16[128,2048]{1,0:T(8,128)(2,1)S(1)}, u32[]{:S(2)}, u32[]{:S(2)}) collective-permute-start(bf16[128,2048]{1,0:T(8,128)(2,1)S(1)} %get-tuple-element.20), channel_id=1, source_target_pairs={{0,2},{2,4},{4,6},{6,0},{1,3},{3,5},{5,7},{7,1},{8,10},{10,12},{12... | collective-permute-start | bytes 1572872 | tf_op jit(solution)/shard_map/ppermute | solution.py:21
  178.2 40.7 %collective-permute-start.22 = (bf16[128,2048]{1,0:T(8,128)(2,1)S(1)}, bf16[128,2048]{1,0:T(8,128)(2,1)S(1)}, u32[]{:S(2)}, u32[]{:S(2)}) collective-permute-start(bf16[128,2048]{1,0:T(8,128)(2,1)S(1)} %get-tuple-element.22), channel_id=1, source_target_pairs={{0,6},{2,0},{4,2},{6,4},{1,7},{3,1},{5,3},{7,5},{8,14},{10,8},{12,... | collective-permute-start | bytes 1572872 | tf_op jit(solution)/shard_map/ppermute | solution.py:21
  181.7 37.2 %collective-permute-start.23 = (bf16[128,2048]{1,0:T(8,128)(2,1)S(1)}, bf16[128,2048]{1,0:T(8,128)(2,1)S(1)}, u32[]{:S(2)}, u32[]{:S(2)}) collective-permute-start(bf16[128,2048]{1,0:T(8,128)(2,1)S(1)} %get-tuple-element.21), channel_id=1, source_target_pairs={{0,4},{2,6},{4,0},{6,2},{1,5},{3,7},{5,1},{7,3},{8,12},{10,14},{12... | collective-permute-start | bytes 1572872 | tf_op jit(solution)/shard_map/ppermute | solution.py:21
  188.8 38.3 %collective-permute-start.10 = (bf16[128,2048]{1,0:T(8,128)(2,1)}, bf16[128,2048]{1,0:T(8,128)(2,1)}, u32[]{:S(2)}, u32[]{:S(2)}) collective-permute-start(bf16[128,2048]{1,0:T(8,128)(2,1)} %get-tuple-element.24), channel_id=1, source_target_pairs={{0,4},{2,6},{4,0},{6,2},{1,5},{3,7},{5,1},{7,3},{8,12},{10,14},{12... | collective-permute-start | bytes 1572872 | tf_op jit(solution)/shard_map/ppermute | solution.py:21
  188.8 39.7 %collective-permute-start.8 = (bf16[128,2048]{1,0:T(8,128)(2,1)S(1)}, bf16[128,2048]{1,0:T(8,128)(2,1)}, u32[]{:S(2)}, u32[]{:S(2)}) collective-permute-start(bf16[128,2048]{1,0:T(8,128)(2,1)S(1)} %get-tuple-element.23), channel_id=1, source_target_pairs={{0,2},{2,4},{4,6},{6,0},{1,3},{3,5},{5,7},{7,1},{8,10},{10,12},{12... | collective-permute-start | bytes 1572872 | tf_op jit(solution)/shard_map/ppermute | solution.py:21
  194.4 35.0 %collective-permute-start.9 = (bf16[128,2048]{1,0:T(8,128)(2,1)S(1)}, bf16[128,2048]{1,0:T(8,128)(2,1)}, u32[]{:S(2)}, u32[]{:S(2)}) collective-permute-start(bf16[128,2048]{1,0:T(8,128)(2,1)S(1)} %get-tuple-element.25), channel_id=1, source_target_pairs={{0,6},{2,0},{4,2},{6,4},{1,7},{3,1},{5,3},{7,5},{8,14},{10,8},{12,... | collective-permute-start | bytes 1572872 | tf_op jit(solution)/shard_map/ppermute | solution.py:21
  (21 other events, 221.5 us)
Sparse Core Ops, SparseCore 0:
  19.1 49.0 all-gather.1
  128.0 56.5 reduce-scatter.1

commit v9 on v8

--- a/solution.py
+++ b/solution.py
@@ -81,9 +81,9 @@
     return lax.dot_general(left, right, (((1,), (1,)), ((), ())), preferred_element_type=F32)
 
 
-def copies(sources, target, sems, index):
-    waits, row = [], 0
-    for i, source in enumerate(sources):
+def copies(sources, target, sems, index, skip=0):
+    waits, row = [], sum(source.shape[1] for source in sources[:skip])
+    for i, source in enumerate(sources[skip:], skip):
         rows = source.shape[1]
         copy = pltpu.make_async_copy(source.at[index], target.at[pl.ds(row, rows)], sems.at[i])
         copy.start()
@@ -116,10 +116,12 @@
 def half_products(pieces, weight_copies, saved, cot, weight, hid, pg_t, pg, pg_out, store, flush, in_sems, sem):
     for copy in weight_copies:
         copy.start()
-    saved_waits = copies(pieces, saved, in_sems.at[0], 0)
+    saved_waits = copies(pieces[:5], saved, in_sems.at[0], 0)
     for copy in weight_copies:
         copy.wait()
-    cot_waits = copies(pieces, cot, in_sems.at[1], 1)
+    cot_waits = copies(pieces[:5], cot, in_sems.at[1], 1)
+    saved_waits += copies(pieces, saved, in_sems.at[0], 0, 5)
+    cot_waits += copies(pieces, cot, in_sems.at[1], 1, 5)
     width = hid.shape[0]
     both = weight[...].reshape(-1, 2 * width)
     for t in range(0, saved.shape[0], TILE):

time: 243 us -> 242 us (level)
  waiting for transfers between devices: 75.1 us -> 87.6 us
  starting transfers between devices: 77.4 us -> 65.3 us
    ppermute x27, waiting for transfers between devices: 51.5 us -> 64 us  [shift(): return lax.ppermute(x, axis, [(i, (i + by) % n) for i in range(n)])]
    ppermute x27, starting transfers between devices: 58.6 us -> 46.5 us  [shift(): return lax.ppermute(x, axis, [(i, (i + by) % n) for i in range(n)])]
  transfers between devices with their start and end apart: 32 -> 32, of which waited for: 9 -> 10; matrix products, arithmetic and copies ran while one was open for 8% -> 8% of each run, Pallas kernels for 16% -> 16%
where the time goes in v9:
time: 242 us; the launch traced here: 240 us
  waiting for transfers between devices  87.6 us (36%)
  starting transfers between devices  65.3 us (27%)
  Pallas kernels  37.7 us (16%)
  other arithmetic  18 us (7%)
  between operations  14.3 us (6%)
  blocking collectives  10.9 us (5%)
  local copies, waits for them, and re-layouts  6.64 us (3%)
    ppermute x27, waiting for transfers between devices, shift(): return lax.ppermute(x, axis, [(i, (i + by) % n) for i in range(n)])  64 us
    ppermute x27, starting transfers between devices, shift(): return lax.ppermute(x, axis, [(i, (i + by) % n) for i in range(n)])  46.5 us
    pallas_call x4, Pallas kernels, call(): pl.pallas_call(kernel, out_shape=[jax.ShapeDtypeStruct(*s) for s in outs]...  37.7 us
    all_to_all x2, waiting for transfers between devices, exchange_sum(): tiles = lax.all_to_all(term, axis, 0, 0, tiled=True)  23.6 us
    all_to_all x1, blocking collectives, gather(): lax.all_to_all(jnp.broadcast_to(x[None], (n, *x.shape)), axis, 0, 0, tile...  10.9 us
    all_to_all x2, starting transfers between devices, exchange_sum(): tiles = lax.all_to_all(term, axis, 0, 0, tiled=True)  10.3 us
    all_to_all x1, starting transfers between devices, gather(): lax.all_to_all(jnp.broadcast_to(x[None], (n, *x.shape)), axis, 0, 0, tile...  8.47 us
    convert_element_type x2, other arithmetic, plus(): return (a.astype(F32) + b.astype(F32)).astype(BF16)  5.31 us
  transfers between devices with their start and end apart: 32, of which 10 were waited for; matrix products, arithmetic and copies ran while one was open for 8% of the time, Pallas kernels for 16%

profile of v9, /device:TPU:8, one launch (start us, length us, event | category | flops | bytes accessed | tf_op | source)
XLA Modules:
  0.0 240.4 jit_solution(14697106300184504421)
XLA Ops:
  8.1 10.9 %all_to_all.20 = bf16[4,64,512]{2,1,0:T(8,128)(2,1)} all-to-all(bf16[4,64,512]{2,1,0:T(8,128)(2,1)S(1)} %broadcast_in_dim.7), channel_id=1, replica_groups=mesh['z'=8,'x'=4,'y'=4,'c'=2] {'x'}, dimensions={0} | all-to-all | bytes 524288 | tf_op jit(solution)/shard_map/all_to_all | solution.py:58
  22.8 8.5 %all-to-all-start.1 = ((bf16[8,64,512]{2,1,0:T(8,128)(2,1)}), bf16[8,64,512]{2,1,0:T(8,128)(2,1)S(1)}, u32[]{:S(2)}, u32[]{:S(2)}) async-start(bf16[8,64,512]{2,1,0:T(8,128)(2,1)} %broadcast_in_dim.8), calls=%async_computation.1 | async-start | bytes 1048576 | tf_op jit(solution)/shard_map/all_to_all | solution.py:58
  33.8 21.4 %collective-permute-done = bf16[128,2048]{1,0:T(8,128)(2,1)S(1)} collective-permute-done((bf16[128,2048]{1,0:T(8,128)(2,1)S(1)}, bf16[128,2048]{1,0:T(8,128)(2,1)S(1)}, u32[]{:S(2)}, u32[]{:S(2)}) %collective-permute-start) | collective-permute-done | bytes 524320 | tf_op jit(solution)/shard_map/ppermute | solution.py:21
  57.5 10.4 %collective-permute-done.1 = bf16[128,2048]{1,0:T(8,128)(2,1)S(1)} collective-permute-done((bf16[128,2048]{1,0:T(8,128)(2,1)S(1)}, bf16[128,2048]{1,0:T(8,128)(2,1)S(1)}, u32[]{:S(2)}, u32[]{:S(2)}) %collective-permute-start.1) | collective-permute-done | bytes 524320 | tf_op jit(solution)/shard_map/ppermute | solution.py:21
  73.5 4.1 %collective-permute-done.2 = bf16[128,2048]{1,0:T(8,128)(2,1)} collective-permute-done((bf16[128,2048]{1,0:T(8,128)(2,1)S(1)}, bf16[128,2048]{1,0:T(8,128)(2,1)}, u32[]{:S(2)}, u32[]{:S(2)}) %collective-permute-start.2) | collective-permute-done | bytes 524320 | tf_op jit(solution)/shard_map/ppermute | solution.py:21
  77.6 5.1 %collective-permute-start.14 = (bf16[2,64,2048]{2,1,0:T(8,128)(2,1)S(1)}, bf16[2,64,2048]{2,1,0:T(8,128)(2,1)S(1)}, u32[]{:S(2)}, u32[]{:S(2)}) collective-permute-start(bf16[2,64,2048]{2,1,0:T(8,128)(2,1)S(1)} %slice.109), channel_id=1, source_target_pairs={{0,6},{2,0},{4,2},{6,4},{1,7},{3,1},{5,3},{7,5},{8,14},{10,8},{12,... | collective-permute-start | bytes 1572872 | tf_op jit(solution)/shard_map/ppermute | solution.py:21
  82.7 6.2 %collective-permute-done.4.refs_4_.refs_11_ = bf16[8,64,512]{2,1,0:T(8,128)(2,1)S(1)} collective-permute-done((bf16[8,64,512]{2,1,0:T(8,128)(2,1)S(1)}, bf16[8,64,512]{2,1,0:T(8,128)(2,1)S(1)}, u32[]{:S(2)}, u32[]{:S(2)}) %collective-permute-start.4) | collective-permute-done | bytes 524320 | tf_op jit(solution)/shard_map/ppermute | solution.py:21
  93.8 4.2 %collective-permute-done.18.refs_8_ = bf16[2,64,2048]{2,1,0:T(8,128)(2,1)S(1)} collective-permute-done((bf16[2,64,2048]{2,1,0:T(8,128)(2,1)S(1)}, bf16[2,64,2048]{2,1,0:T(8,128)(2,1)S(1)}, u32[]{:S(2)}, u32[]{:S(2)}) %collective-permute-start.18) | collective-permute-done | bytes 524320 | tf_op jit(solution)/shard_map/ppermute | solution.py:21
  99.5 11.7 %shard_map.104 = (bf16[4,8,64,512]{3,2,1,0:T(8,128)(2,1)}, bf16[1024,256]{1,0:T(8,128)(2,1)}) custom-call(bf16[2,128,2048]{2,1,0:T(8,128)(2,1)} %copy-done.1, bf16[2,128,2048]{2,1,0:T(8,128)(2,1)} %collective-permute-done.11.refs_1_, bf16[2,128,2048]{2,1,0:T(8,128)(2,1)} %collective-permute-done.12.refs_2_, bf16[2,64,2048]{2,1,0:T(8,128)(2,1)} %copy-done.9, ...), custom_call_target="tpu_custom_call" | custom-call | flops 4294967296 | bytes 12582912 | tf_op jit(solution)/shard_map/pallas_call | solution.py:263
  111.2 3.6 %all-to-all-start.2 = ((bf16[4,8,64,512]{3,2,1,0:T(8,128)(2,1)}), bf16[4,8,64,512]{3,2,1,0:T(8,128)(2,1)S(1)}, u32[]{:S(2)}, u32[]{:S(2)}) async-start(bf16[4,8,64,512]{3,2,1,0:T(8,128)(2,1)} %get-tuple-element.19), calls=%async_computation.3 | async-start | bytes 4194304 | tf_op jit(solution)/shard_map/all_to_all | solution.py:62
  114.9 11.7 %shard_map.103 = (bf16[2048,512]{1,0:T(8,128)(2,1)}, bf16[1024,256]{1,0:T(8,128)(2,1)}) custom-call(bf16[2,128,2048]{2,1,0:T(8,128)(2,1)} %copy-done.1, bf16[2,128,2048]{2,1,0:T(8,128)(2,1)} %collective-permute-done.11.refs_1_, bf16[2,128,2048]{2,1,0:T(8,128)(2,1)} %collective-permute-done.12.refs_2_, bf16[2,64,2048]{2,1,0:T(8,128)(2,1)} %copy-done.9, ...), custom_call_target="tpu_custom_call" | custom-call | flops 4294967296 | bytes 12582912 | tf_op jit(solution)/shard_map/pallas_call | solution.py:263
  126.6 5.7 %shard_map.105 = (bf16[512,2048]{1,0:T(8,128)(2,1)}, bf16[512,2048]{1,0:T(8,128)(2,1)}) custom-call(bf16[1024,256]{1,0:T(8,128)(2,1)} %get-tuple-element.14.refs_0_, bf16[1024,256]{1,0:T(8,128)(2,1)} %get-tuple-element.15.refs_1_, bf16[8,4,64,512]{3,2,1,0:T(8,128)(2,1)} %bitcast.22, bf16[8,64,512]{2,1,0:T(8,128)(2,1)} %copy-done.2, ...), custom_call_target="tpu_custom_call" | custom-call | flops 2147483648 | bytes 12582912 | tf_op jit(solution)/shard_map/pallas_call | solution.py:263
  132.8 8.6 %shard_map.102 = (bf16[512,2048]{1,0:T(8,128)(2,1)}, bf16[512,2048]{1,0:T(8,128)(2,1)}) custom-call(bf16[1,512,2048]{2,1,0:T(8,128)(2,1)} %maximum_bitcast_fusion.refs_0_, bf16[1,512,2048]{2,1,0:T(8,128)(2,1)} %collective-permute-done.3.refs_1_, bf16[8,4,64,512]{3,2,1,0:T(8,128)(2,1)} %bitcast.23, bf16[8,64,512]{2,1,0:T(8,128)(2,1)} %copy-done.2, ...), custom_call_target="tpu_custom_call" | custom-call | flops 4294967296 | bytes 12582912 | tf_op jit(solution)/shard_map/pallas_call | solution.py:263
  143.1 6.7 %all-to-all-start.3 = ((bf16[8,64,512]{2,1,0:T(8,128)(2,1)}), bf16[8,64,512]{2,1,0:T(8,128)(2,1)S(1)}, u32[]{:S(2)}, u32[]{:S(2)}) async-start(bf16[8,64,512]{2,1,0:T(8,128)(2,1)} %reduce_sum.21), calls=%async_computation.4 | async-start | bytes 1048576 | tf_op jit(solution)/shard_map/all_to_all | solution.py:62
  149.8 23.6 %all-to-all-done.3 = bf16[8,64,512]{2,1,0:T(8,128)(2,1)S(1)} async-done(((bf16[8,64,512]{2,1,0:T(8,128)(2,1)}), bf16[8,64,512]{2,1,0:T(8,128)(2,1)S(1)}, u32[]{:S(2)}, u32[]{:S(2)}) %all-to-all-start.3) | async-done | bytes 524320 | tf_op jit(solution)/shard_map/all_to_all | solution.py:62
  177.0 3.5 %collective-permute-start.22 = (bf16[128,2048]{1,0:T(8,128)(2,1)S(1)}, bf16[128,2048]{1,0:T(8,128)(2,1)S(1)}, u32[]{:S(2)}, u32[]{:S(2)}) collective-permute-start(bf16[128,2048]{1,0:T(8,128)(2,1)S(1)} %get-tuple-element.22), channel_id=1, source_target_pairs={{0,6},{2,0},{4,2},{6,4},{1,7},{3,1},{5,3},{7,5},{8,14},{10,8},{12,... | collective-permute-start | bytes 1572872 | tf_op jit(solution)/shard_map/ppermute | solution.py:21
  180.5 4.3 %collective-permute-start.23 = (bf16[128,2048]{1,0:T(8,128)(2,1)S(1)}, bf16[128,2048]{1,0:T(8,128)(2,1)S(1)}, u32[]{:S(2)}, u32[]{:S(2)}) collective-permute-start(bf16[128,2048]{1,0:T(8,128)(2,1)S(1)} %get-tuple-element.21), channel_id=1, source_target_pairs={{0,4},{2,6},{4,0},{6,2},{1,5},{3,7},{5,1},{7,3},{8,12},{10,14},{12... | collective-permute-start | bytes 1572872 | tf_op jit(solution)/shard_map/ppermute | solution.py:21
  184.8 2.7 %add_convert_fusion.7 = (bf16[128,2048]{1,0:T(8,128)(2,1)S(1)}, bf16[128,2048]{1,0:T(8,128)(2,1)}, bf16[128,2048]{1,0:T(8,128)(2,1)S(1)}) fusion(bf16[512,2048]{1,0:T(8,128)(2,1)} %collective-permute-done.7, bf16[512,2048]{1,0:T(8,128)(2,1)S(1)} %copy-done), kind=kLoop, calls=%fused_computation.10 | loop fusion | flops 3145728 | bytes 4718592 | tf_op jit(solution)/shard_map/convert_element_type | solution.py:43
  189.6 3.5 %collective-permute-done.21 = bf16[128,2048]{1,0:T(8,128)(2,1)S(1)} collective-permute-done((bf16[128,2048]{1,0:T(8,128)(2,1)S(1)}, bf16[128,2048]{1,0:T(8,128)(2,1)S(1)}, u32[]{:S(2)}, u32[]{:S(2)}) %collective-permute-start.21) | collective-permute-done | bytes 524320 | tf_op jit(solution)/shard_map/ppermute | solution.py:21
  193.2 4.9 %collective-permute-start.9 = (bf16[128,2048]{1,0:T(8,128)(2,1)S(1)}, bf16[128,2048]{1,0:T(8,128)(2,1)}, u32[]{:S(2)}, u32[]{:S(2)}) collective-permute-start(bf16[128,2048]{1,0:T(8,128)(2,1)S(1)} %get-tuple-element.25), channel_id=1, source_target_pairs={{0,6},{2,0},{4,2},{6,4},{1,7},{3,1},{5,3},{7,5},{8,14},{10,8},{12,... | collective-permute-start | bytes 1572872 | tf_op jit(solution)/shard_map/ppermute | solution.py:21
  198.1 10.8 %collective-permute-done.23 = bf16[128,2048]{1,0:T(8,128)(2,1)S(1)} collective-permute-done((bf16[128,2048]{1,0:T(8,128)(2,1)S(1)}, bf16[128,2048]{1,0:T(8,128)(2,1)S(1)}, u32[]{:S(2)}, u32[]{:S(2)}) %collective-permute-start.23) | collective-permute-done | bytes 524320 | tf_op jit(solution)/shard_map/ppermute | solution.py:21
  212.3 10.8 %collective-permute-start.24 = (bf16[64,512]{1,0:T(8,128)(2,1)S(1)}, bf16[64,512]{1,0:T(8,128)(2,1)S(1)}, u32[]{:S(2)}, u32[]{:S(2)}) collective-permute-start(bf16[64,512]{1,0:T(8,128)(2,1)S(1)} %get-tuple-element.26), channel_id=1, source_target_pairs={{0,8},{8,16},{16,24},{24,0},{1,9},{9,17},{17,25},{25,1},{2,10},{10... | collective-permute-start | bytes 196616 | tf_op jit(solution)/shard_map/ppermute | solution.py:21
  223.1 2.8 %collective-permute-start.26 = (bf16[64,512]{1,0:T(8,128)(2,1)S(1)}, bf16[64,512]{1,0:T(8,128)(2,1)S(1)}, u32[]{:S(2)}, u32[]{:S(2)}) collective-permute-start(bf16[64,512]{1,0:T(8,128)(2,1)S(1)} %get-tuple-element.27), channel_id=1, source_target_pairs={{0,24},{8,0},{16,8},{24,16},{1,25},{9,1},{17,9},{25,17},{2,26},{10... | collective-permute-start | bytes 196616 | tf_op jit(solution)/shard_map/ppermute | solution.py:21
  228.5 2.7 %add_convert_fusion.4 = bf16[128,2048]{1,0:T(8,128)(2,1)} fusion(bf16[128,2048]{1,0:T(8,128)(2,1)} %collective-permute-done.10, bf16[128,2048]{1,0:T(8,128)(2,1)} %collective-permute-done.9, bf16[128,2048]{1,0:T(8,128)(2,1)} %collective-permute-done.8, bf16[512,2048]{1,0:T(8,128)(2,1)} %collective-permute-done.7, bf16[512,2048]{1,0:T(8,128)(2,1)S(1)} %copy-done), kind=kLoop, calls=%fused_computation.7 | loop fusion | flops 2621440 | bytes 3145728 | tf_op jit(solution)/shard_map/convert_element_type | solution.py:53
  (94 shorter events, 37.7 us)
Async XLA Ops:
  7.2 107.7 %all-gather.2.cloned.1.call-start = ((), (), s32[]{:S(2)}) async-start(), calls=%async_computation.5 | async-start | bytes 2359296 | tf_op jit(solution)/shard_map/all_gather | solution.py:317
  20.3 48.1 %collective-permute-start.11 = (bf16[2,128,2048]{2,1,0:T(8,128)(2,1)S(1)}, bf16[2,128,2048]{2,1,0:T(8,128)(2,1)}, u32[]{:S(2)}, u32[]{:S(2)}) collective-permute-start(bf16[2,128,2048]{2,1,0:T(8,128)(2,1)S(1)} %pad_maximum_fusion.refs_0_), channel_id=1, source_target_pairs={{0,2},{2,4},{4,6},{6,0},{1,3},{3,5},{5,7},{7,1},{8,10},{10,12},{12... | collective-permute-start | bytes 3145736 | tf_op jit(solution)/shard_map/ppermute | solution.py:21
  22.8 45.0 %all-to-all-start.1 = ((bf16[8,64,512]{2,1,0:T(8,128)(2,1)}), bf16[8,64,512]{2,1,0:T(8,128)(2,1)S(1)}, u32[]{:S(2)}, u32[]{:S(2)}) async-start(bf16[8,64,512]{2,1,0:T(8,128)(2,1)} %broadcast_in_dim.8), calls=%async_computation.1 | async-start | bytes 1048576 | tf_op jit(solution)/shard_map/all_to_all | solution.py:58
  31.3 39.2 %collective-permute-start.12 = (bf16[2,128,2048]{2,1,0:T(8,128)(2,1)S(1)}, bf16[2,128,2048]{2,1,0:T(8,128)(2,1)}, u32[]{:S(2)}, u32[]{:S(2)}) collective-permute-start(bf16[2,128,2048]{2,1,0:T(8,128)(2,1)S(1)} %pad_maximum_fusion.refs_0_), channel_id=1, source_target_pairs={{0,6},{2,0},{4,2},{6,4},{1,7},{3,1},{5,3},{7,5},{8,14},{10,8},{12,... | collective-permute-start | bytes 3145736 | tf_op jit(solution)/shard_map/ppermute | solution.py:21
  31.8 23.4 %collective-permute-start = (bf16[128,2048]{1,0:T(8,128)(2,1)S(1)}, bf16[128,2048]{1,0:T(8,128)(2,1)S(1)}, u32[]{:S(2)}, u32[]{:S(2)}) collective-permute-start(bf16[128,2048]{1,0:T(8,128)(2,1)S(1)} %copy-done.3), channel_id=1, source_target_pairs={{0,2},{2,4},{4,6},{6,0},{1,3},{3,5},{5,7},{7,1},{8,10},{10,12},{12... | collective-permute-start | bytes 1572872 | tf_op jit(solution)/shard_map/ppermute | solution.py:21
  33.3 34.5 %collective-permute-start.1 = (bf16[128,2048]{1,0:T(8,128)(2,1)S(1)}, bf16[128,2048]{1,0:T(8,128)(2,1)S(1)}, u32[]{:S(2)}, u32[]{:S(2)}) collective-permute-start(bf16[128,2048]{1,0:T(8,128)(2,1)S(1)} %copy-done.3), channel_id=1, source_target_pairs={{0,6},{2,0},{4,2},{6,4},{1,7},{3,1},{5,3},{7,5},{8,14},{10,8},{12,... | collective-permute-start | bytes 1572872 | tf_op jit(solution)/shard_map/ppermute | solution.py:21
  33.8 43.8 %collective-permute-start.15 = (bf16[2,128,2048]{2,1,0:T(8,128)(2,1)S(1)}, bf16[2,128,2048]{2,1,0:T(8,128)(2,1)}, u32[]{:S(2)}, u32[]{:S(2)}) collective-permute-start(bf16[2,128,2048]{2,1,0:T(8,128)(2,1)S(1)} %pad_maximum_fusion.refs_0_), channel_id=1, source_target_pairs={{0,1},{1,0},{2,3},{3,2},{4,5},{5,4},{6,7},{7,6},{8,9},{9,8},{10,11... | collective-permute-start | bytes 3145736 | tf_op jit(solution)/shard_map/ppermute | solution.py:21
  55.2 22.4 %collective-permute-start.2 = (bf16[128,2048]{1,0:T(8,128)(2,1)S(1)}, bf16[128,2048]{1,0:T(8,128)(2,1)}, u32[]{:S(2)}, u32[]{:S(2)}) collective-permute-start(bf16[128,2048]{1,0:T(8,128)(2,1)S(1)} %copy-done.3), channel_id=1, source_target_pairs={{0,4},{2,6},{4,0},{6,2},{1,5},{3,7},{5,1},{7,3},{8,12},{10,14},{12... | collective-permute-start | bytes 1572872 | tf_op jit(solution)/shard_map/ppermute | solution.py:21
  67.9 21.0 %collective-permute-start.4 = (bf16[8,64,512]{2,1,0:T(8,128)(2,1)S(1)}, bf16[8,64,512]{2,1,0:T(8,128)(2,1)S(1)}, u32[]{:S(2)}, u32[]{:S(2)}) collective-permute-start(bf16[8,64,512]{2,1,0:T(8,128)(2,1)S(1)} %all-to-all-done.1.refs_3_.refs_10_), channel_id=1, source_target_pairs={{0,8},{8,16},{16,24},{24,0},{1,9},{9,17},{17,25},{25,1},{2,10},{10... | collective-permute-start | bytes 1572872 | tf_op jit(solution)/shard_map/ppermute | solution.py:21
  68.4 20.5 %collective-permute-start.5 = (bf16[8,64,512]{2,1,0:T(8,128)(2,1)S(1)}, bf16[8,64,512]{2,1,0:T(8,128)(2,1)S(1)}, u32[]{:S(2)}, u32[]{:S(2)}) collective-permute-start(bf16[8,64,512]{2,1,0:T(8,128)(2,1)S(1)} %all-to-all-done.1.refs_3_.refs_10_), channel_id=1, source_target_pairs={{0,16},{8,24},{16,0},{24,8},{1,17},{9,25},{17,1},{25,9},{2,18},{10... | collective-permute-start | bytes 1572872 | tf_op jit(solution)/shard_map/ppermute | solution.py:21
  70.5 22.3 %collective-permute-start.6 = (bf16[8,64,512]{2,1,0:T(8,128)(2,1)S(1)}, bf16[8,64,512]{2,1,0:T(8,128)(2,1)S(1)}, u32[]{:S(2)}, u32[]{:S(2)}) collective-permute-start(bf16[8,64,512]{2,1,0:T(8,128)(2,1)S(1)} %all-to-all-done.1.refs_3_.refs_10_), channel_id=1, source_target_pairs={{0,24},{8,0},{16,8},{24,16},{1,25},{9,1},{17,9},{25,17},{2,26},{10... | collective-permute-start | bytes 1572872 | tf_op jit(solution)/shard_map/ppermute | solution.py:21
  92.8 40.0 %collective-permute-start.3 = (bf16[1,512,2048]{2,1,0:T(8,128)(2,1)}, bf16[1,512,2048]{2,1,0:T(8,128)(2,1)}, u32[]{:S(2)}, u32[]{:S(2)}) collective-permute-start(bf16[1,512,2048]{2,1,0:T(8,128)(2,1)} %maximum_bitcast_fusion.refs_0_), channel_id=1, source_target_pairs={{0,1},{1,0},{2,3},{3,2},{4,5},{5,4},{6,7},{7,6},{8,9},{9,8},{10,11... | collective-permute-start | bytes 6291464 | tf_op jit(solution)/shard_map/ppermute | solution.py:21
  111.2 30.7 %all-to-all-start.2 = ((bf16[4,8,64,512]{3,2,1,0:T(8,128)(2,1)}), bf16[4,8,64,512]{3,2,1,0:T(8,128)(2,1)S(1)}, u32[]{:S(2)}, u32[]{:S(2)}) async-start(bf16[4,8,64,512]{3,2,1,0:T(8,128)(2,1)} %get-tuple-element.19), calls=%async_computation.3 | async-start | bytes 4194304 | tf_op jit(solution)/shard_map/all_to_all | solution.py:62
  114.8 96.5 %reduce-scatter.2.cloned.1.call-start = ((), (), s32[]{:S(2)}) async-start(), calls=%async_computation.6 | async-start | bytes 2359296 | tf_op jit(solution)/shard_map/reduce_scatter | solution.py:324
  132.4 41.1 %collective-permute-start.20 = (bf16[512,2048]{1,0:T(8,128)(2,1)}, bf16[512,2048]{1,0:T(8,128)(2,1)}, u32[]{:S(2)}, u32[]{:S(2)}) collective-permute-start(bf16[512,2048]{1,0:T(8,128)(2,1)} %get-tuple-element.17), channel_id=1, source_target_pairs={{0,1},{1,0},{2,3},{3,2},{4,5},{5,4},{6,7},{7,6},{8,9},{9,8},{10,11... | collective-permute-start | bytes 6291464 | tf_op jit(solution)/shard_map/ppermute | solution.py:21
  141.4 43.4 %collective-permute-start.7 = (bf16[512,2048]{1,0:T(8,128)(2,1)}, bf16[512,2048]{1,0:T(8,128)(2,1)}, u32[]{:S(2)}, u32[]{:S(2)}) collective-permute-start(bf16[512,2048]{1,0:T(8,128)(2,1)} %get-tuple-element.13), channel_id=1, source_target_pairs={{0,1},{1,0},{2,3},{3,2},{4,5},{5,4},{6,7},{7,6},{8,9},{9,8},{10,11... | collective-permute-start | bytes 6291464 | tf_op jit(solution)/shard_map/ppermute | solution.py:21
  143.1 30.2 %all-to-all-start.3 = ((bf16[8,64,512]{2,1,0:T(8,128)(2,1)}), bf16[8,64,512]{2,1,0:T(8,128)(2,1)S(1)}, u32[]{:S(2)}, u32[]{:S(2)}) async-start(bf16[8,64,512]{2,1,0:T(8,128)(2,1)} %reduce_sum.21), calls=%async_computation.4 | async-start | bytes 1048576 | tf_op jit(solution)/shard_map/all_to_all | solution.py:62
  176.0 17.1 %collective-permute-start.21 = (bf16[128,2048]{1,0:T(8,128)(2,1)S(1)}, bf16[128,2048]{1,0:T(8,128)(2,1)S(1)}, u32[]{:S(2)}, u32[]{:S(2)}) collective-permute-start(bf16[128,2048]{1,0:T(8,128)(2,1)S(1)} %get-tuple-element.20), channel_id=1, source_target_pairs={{0,2},{2,4},{4,6},{6,0},{1,3},{3,5},{5,7},{7,1},{8,10},{10,12},{12... | collective-permute-start | bytes 1572872 | tf_op jit(solution)/shard_map/ppermute | solution.py:21
  177.0 21.1 %collective-permute-start.22 = (bf16[128,2048]{1,0:T(8,128)(2,1)S(1)}, bf16[128,2048]{1,0:T(8,128)(2,1)S(1)}, u32[]{:S(2)}, u32[]{:S(2)}) collective-permute-start(bf16[128,2048]{1,0:T(8,128)(2,1)S(1)} %get-tuple-element.22), channel_id=1, source_target_pairs={{0,6},{2,0},{4,2},{6,4},{1,7},{3,1},{5,3},{7,5},{8,14},{10,8},{12,... | collective-permute-start | bytes 1572872 | tf_op jit(solution)/shard_map/ppermute | solution.py:21
  180.5 28.4 %collective-permute-start.23 = (bf16[128,2048]{1,0:T(8,128)(2,1)S(1)}, bf16[128,2048]{1,0:T(8,128)(2,1)S(1)}, u32[]{:S(2)}, u32[]{:S(2)}) collective-permute-start(bf16[128,2048]{1,0:T(8,128)(2,1)S(1)} %get-tuple-element.21), channel_id=1, source_target_pairs={{0,4},{2,6},{4,0},{6,2},{1,5},{3,7},{5,1},{7,3},{8,12},{10,14},{12... | collective-permute-start | bytes 1572872 | tf_op jit(solution)/shard_map/ppermute | solution.py:21
  187.6 35.5 %collective-permute-start.10 = (bf16[128,2048]{1,0:T(8,128)(2,1)}, bf16[128,2048]{1,0:T(8,128)(2,1)}, u32[]{:S(2)}, u32[]{:S(2)}) collective-permute-start(bf16[128,2048]{1,0:T(8,128)(2,1)} %get-tuple-element.24), channel_id=1, source_target_pairs={{0,4},{2,6},{4,0},{6,2},{1,5},{3,7},{5,1},{7,3},{8,12},{10,14},{12... | collective-permute-start | bytes 1572872 | tf_op jit(solution)/shard_map/ppermute | solution.py:21
  187.6 38.3 %collective-permute-start.8 = (bf16[128,2048]{1,0:T(8,128)(2,1)S(1)}, bf16[128,2048]{1,0:T(8,128)(2,1)}, u32[]{:S(2)}, u32[]{:S(2)}) collective-permute-start(bf16[128,2048]{1,0:T(8,128)(2,1)S(1)} %get-tuple-element.23), channel_id=1, source_target_pairs={{0,2},{2,4},{4,6},{6,0},{1,3},{3,5},{5,7},{7,1},{8,10},{10,12},{12... | collective-permute-start | bytes 1572872 | tf_op jit(solution)/shard_map/ppermute | solution.py:21
  193.2 35.4 %collective-permute-start.9 = (bf16[128,2048]{1,0:T(8,128)(2,1)S(1)}, bf16[128,2048]{1,0:T(8,128)(2,1)}, u32[]{:S(2)}, u32[]{:S(2)}) collective-permute-start(bf16[128,2048]{1,0:T(8,128)(2,1)S(1)} %get-tuple-element.25), channel_id=1, source_target_pairs={{0,6},{2,0},{4,2},{6,4},{1,7},{3,1},{5,3},{7,5},{8,14},{10,8},{12,... | collective-permute-start | bytes 1572872 | tf_op jit(solution)/shard_map/ppermute | solution.py:21
  212.3 19.0 %collective-permute-start.24 = (bf16[64,512]{1,0:T(8,128)(2,1)S(1)}, bf16[64,512]{1,0:T(8,128)(2,1)S(1)}, u32[]{:S(2)}, u32[]{:S(2)}) collective-permute-start(bf16[64,512]{1,0:T(8,128)(2,1)S(1)} %get-tuple-element.26), channel_id=1, source_target_pairs={{0,8},{8,16},{16,24},{24,0},{1,9},{9,17},{17,25},{25,1},{2,10},{10... | collective-permute-start | bytes 196616 | tf_op jit(solution)/shard_map/ppermute | solution.py:21
  (21 other events, 241.0 us)
Sparse Core Ops, SparseCore 0:
  19.1 49.0 all-gather.1
  126.8 56.6 reduce-scatter.1
